TPU v7x, 128 devices: a 2x2x16 block of a 8x8x16 slice. The times are simulated.
128 devices in a mesh: grp: 4 (over y, x), ep: 32 (over z, core).
Axes of the slice: x: 2, y: 2, z: 16, core: 2. Of those that a mesh axis runs over, the one named last changes fastest.
The devices are a block of a 8x8x16 slice.
Arguments:
- tokens: bfloat16 [2048, 2048], P(('grp', 'ep')), parts along dimension 0, may hold values from -6 to 6
- norm_gain: bfloat16 [2048], replicated, may hold values from 0.099609375 to 1.8984375
- query_weight: bfloat16 [2048, 1024], P(None, 'ep'), may hold values from -0.125 to 0.125
- key_weight: bfloat16 [2048, 256], replicated, may hold values from -0.25 to 0.25
- value_weight: bfloat16 [2048, 256], replicated, may hold values from -0.125 to 0.125
- out_weight: bfloat16 [1024, 2048], P(None, 'ep'), may hold values from -0.1875 to 0.1875
- head_gain: bfloat16 [128], replicated, may hold values from 0.099609375 to 1.8984375
- lambdas: float32 [8], replicated, may hold values from 0.3 to 0.8
- cache_keys: bfloat16 [2048, 1024, 2, 128], P(('grp', 'ep')), parts along dimension 0, may hold values from -1000 to 1000
- cache_values: bfloat16 [2048, 1024, 2, 128], P(('grp', 'ep')), parts along dimension 0, may hold values from -6 to 6
- lengths: int32 [2048], P(('grp', 'ep')), parts along dimension 0, may hold values from 64 to 1024
- moe_gain: bfloat16 [2048], replicated, may hold values from 0.099609375 to 1.8984375
- gate_weight: bfloat16 [32, 2048, 1024], P('ep'), may hold values from -0.375 to 0.375
- up_weight: bfloat16 [32, 2048, 1024], P('ep'), may hold values from -0.375 to 0.375
- down_weight: bfloat16 [32, 1024, 2048], P('ep'), may hold values from -0.02734375 to 0.02734375
- routes: int32 [2048, 4], P(('grp', 'ep')), parts along dimension 0, may hold values from 0 to 31, all different within a row; in each aligned block of 16 rows (0 to 15, 16 to 31, ...) at most 4 rows name the same one
- route_weights: float32 [2048, 4], P(('grp', 'ep')), parts along dimension 0, may hold values from 0.2 to 1
Outputs:
- mixed: bfloat16 [2048, 2048], P(('grp', 'ep')), parts along dimension 0
There are 4 independent parts, one for each index of `grp`. A program takes and returns all parts, laid end to end along the dimension named above; an argument that names none is the same for every part. Nothing has to cross between parts.
Inputs may be any that keep to these rules, and one draw needn't show every extreme that they name: `routes`: a token's 4 experts differ; the tokens of one device name each expert at most 4 times, and in every draw some expert is named exactly 4 times by one device's tokens.
All inputs are finite; a program needn't handle non-finite values.
Results may differ from a plain program's by a relative error of at most 0.034.
Values may be sent and summed in bfloat16 or wider, within the bound.
No kernel may reach another device: no remote copies, remote signals or barrier semaphores. Data moves between devices by JAX's collectives and lax.ppermute only.
A program may use at most 128 MiB of HBM per device.

v0:
```python
import jax
import jax.numpy as jnp
from jax import lax
from jax.sharding import Mesh
from jax.sharding import PartitionSpec as P

EP = ("ep_0", "ep_1")
GRP_EP = ("grp", "ep_0", "ep_1")


epsilon = 1e-06
masked_score = -1e30
clamp_limit = 7.0
swish_alpha = 1.702


def in_blocks(value, dim, length):
    before, after = (value.shape[:dim], value.shape[dim + 1 :])
    return jnp.moveaxis(value.reshape(*before, length, -1, *after), dim, 0)


def joined_along(blocks, dim):
    blocks = jnp.moveaxis(blocks, 0, dim)
    lengths = blocks.shape
    return blocks.reshape(*lengths[:dim], lengths[dim] * lengths[dim + 1], *lengths[dim + 2 :])


def moved_by_axis(blocks, axes, sequence):
    inside = blocks.shape[1:]
    filled = blocks.reshape(*(lax.axis_size(a) for a in axes), *inside)
    for k in sequence:
        filled = lax.all_to_all(filled, axes[k], k, k, tiled=True)
    return filled.reshape(-1, *inside)


def two_step_exchange(value, groups, sequence, split_dim, concat_dim):
    length = lax.axis_size(groups[0]) * lax.axis_size(groups[1])
    blocks = in_blocks(value, split_dim, length)
    return joined_along(moved_by_axis(blocks, groups, sequence), concat_dim)


def rms_scaled(values, gain):
    floats = values.astype(jnp.float32)
    return (
        floats
        * lax.rsqrt(jnp.mean(floats * floats, axis=-1, keepdims=True) + epsilon)
        * gain.astype(jnp.float32)
    )


def attention(queries, new_keys, new_values, cache_keys, cache_values, lengths, lambdas, head_gain):
    count = queries.shape[0]
    ctx_len = cache_keys.shape[1]
    kv_count = cache_keys.shape[2]
    head_dim = cache_keys.shape[3] // 2
    heads = lambdas.shape[0]
    group = heads // kv_count
    val_dim = cache_values.shape[3]
    query_grid = queries.reshape(count, kv_count, group, 2, head_dim)
    key_grid = cache_keys.reshape(count, ctx_len, kv_count, 2, head_dim)
    own_keys = new_keys.reshape(count, kv_count, 2, head_dim)
    inv_scale = head_dim ** (-0.5)
    scores = (
        jnp.einsum("bkgcd,bjkcd->bkgcj", query_grid, key_grid, preferred_element_type=jnp.float32)
        * inv_scale
    )
    own_score = (
        jnp.einsum("bkgcd,bkcd->bkgc", query_grid, own_keys, preferred_element_type=jnp.float32)
        * inv_scale
    )
    visible = jnp.arange(ctx_len, dtype=jnp.int32)[None, :] < lengths[:, None]
    scores = jnp.where(visible[:, None, None, None, :], scores, masked_score)
    highest = jnp.maximum(jnp.max(scores, axis=-1), own_score)
    expd = jnp.exp(scores - highest[..., None])
    own_exp = jnp.exp(own_score - highest)
    denominator = jnp.sum(expd, axis=-1) + own_exp
    probs = expd / denominator[..., None]
    own_prob = own_exp / denominator
    lambda_grid = lambdas.reshape(kv_count, group)[None, :, :]
    weights = (probs[:, :, :, 0] - lambda_grid[..., None] * probs[:, :, :, 1]).astype(jnp.bfloat16)
    own_weight = (own_prob[..., 0] - lambda_grid * own_prob[..., 1]).astype(jnp.bfloat16)
    attended = jnp.einsum(
        "bkgj,bjkv->bkgv", weights, cache_values, preferred_element_type=jnp.float32
    )
    own_vals = new_values.reshape(count, kv_count, val_dim).astype(jnp.float32)
    attended = attended + own_weight.astype(jnp.float32)[..., None] * own_vals[:, :, None, :]
    return rms_scaled(attended, head_gain).reshape(count, heads * val_dim).astype(jnp.bfloat16)


def expert_mlp(inputs, gate_w, up_w, down_w):
    gate = jnp.dot(inputs, gate_w, preferred_element_type=jnp.float32)
    upper = jnp.dot(inputs, up_w, preferred_element_type=jnp.float32)
    gate = jnp.minimum(gate, clamp_limit)
    upper = jnp.clip(upper, -clamp_limit, clamp_limit)
    act = ((upper + 1.0) * gate * jax.nn.sigmoid(swish_alpha * gate)).astype(jnp.bfloat16)
    return jnp.dot(act, down_w, preferred_element_type=jnp.float32).astype(jnp.bfloat16)


def local(
    tokens,
    norm_gain,
    query_weight,
    key_weight,
    value_weight,
    out_weight,
    head_gain,
    lambdas,
    cache_keys,
    cache_values,
    lengths,
    moe_gain,
    gate_weight,
    up_weight,
    down_weight,
    routes,
    route_weights,
):
    count = tokens.shape[0]
    width = tokens.shape[1]
    topk = routes.shape[1]
    normed = rms_scaled(tokens, norm_gain).astype(jnp.bfloat16)
    new_keys = jnp.dot(normed, key_weight, preferred_element_type=jnp.float32).astype(jnp.bfloat16)
    new_values = jnp.dot(normed, value_weight, preferred_element_type=jnp.float32).astype(
        jnp.bfloat16
    )
    queries = jnp.dot(
        normed,
        lax.all_gather(query_weight, EP, axis=1, tiled=True),
        preferred_element_type=jnp.float32,
    ).astype(jnp.bfloat16)
    head_out = attention(
        queries, new_keys, new_values, cache_keys, cache_values, lengths, lambdas, head_gain
    )
    attn_out = jnp.dot(
        head_out,
        lax.all_gather(out_weight, EP, axis=1, tiled=True),
        preferred_element_type=jnp.float32,
    ).astype(jnp.bfloat16)
    residual = (tokens.astype(jnp.float32) + attn_out.astype(jnp.float32)).astype(jnp.bfloat16)
    moe_in = rms_scaled(residual, moe_gain).astype(jnp.bfloat16)
    experts = lax.axis_size(EP)
    capacity = min(count, max(2, 2 * count * topk // experts))
    onehot = (routes.reshape(-1)[:, None] == jnp.arange(experts, dtype=jnp.int32)[None, :]).astype(
        jnp.int32
    )
    earlier_all = jnp.cumsum(onehot, axis=0) - onehot
    ranks = jnp.sum(earlier_all * onehot, axis=1).reshape(count, topk)
    slot_id = routes * capacity + ranks
    slot_range = jnp.arange(experts * capacity, dtype=jnp.int32)
    dispatch = jnp.any(slot_id[None, :, :] == slot_range[:, None, None], axis=2).astype(
        jnp.bfloat16
    )
    outgoing = jnp.dot(dispatch, moe_in, preferred_element_type=jnp.float32).astype(jnp.bfloat16)
    outgoing = outgoing.reshape(experts, capacity, width)
    received = lax.all_to_all(outgoing, EP, split_axis=0, concat_axis=0, tiled=True)
    flat_rows = received.reshape(-1, width)
    results = expert_mlp(flat_rows, gate_weight[0], up_weight[0], down_weight[0]).reshape(
        received.shape
    )
    returned = two_step_exchange(results, ("ep_0", "ep_1"), (1, 0), 0, 0)
    picked = returned.reshape(-1, width)[slot_id].astype(jnp.float32)
    moe_sum = jnp.sum(route_weights[:, :, None] * picked, axis=1)
    return (residual.astype(jnp.float32) + moe_sum).astype(jnp.bfloat16)


def solution(mesh):
    torus = Mesh(mesh.devices.reshape(mesh.shape["grp"], 16, 2), ("grp", "ep_0", "ep_1"))
    return jax.shard_map(
        local,
        mesh=torus,
        in_specs=(
            P(GRP_EP, None),
            P(),
            P(None, EP),
            P(),
            P(),
            P(None, EP),
            P(),
            P(),
            P(GRP_EP, None, None, None),
            P(GRP_EP, None, None, None),
            P(GRP_EP),
            P(),
            P(EP, None, None),
            P(EP, None, None),
            P(EP, None, None),
            P(GRP_EP, None),
            P(GRP_EP, None),
        ),
        out_specs=P(GRP_EP, None),
        check_vma=False,
    )
```

profile of v0, /device:TPU:196, one launch (start us, length us, event | category | flops | bytes accessed | tf_op | source)
XLA Modules:
  0.0 256.7 jit_solution(1029286353424995351)
XLA Ops:
  6.6 0.7 all-gather.3.cloned.1.call-update
  7.4 0.7 all-gather.5.cloned.1.call-update
  8.1 0.7 convert_element_type.86
  8.8 1.0 fusion.57
  9.8 1.1 convolution_convert_fusion.4
  10.9 0.1 reshape.101
  11.1 21.2 %copy.77 = bf16[16,1024,2,128]{1,3,2,0:T(8,128)(2,1)} copy(bf16[16,1024,2,128]{3,2,1,0:T(2,128)(2,1)} %param.25) | data formatting | bytes 16777216 | tf_op args[8]
  32.4 0.3 fusion.38
  32.9 0.1 eq.28
  33.0 0.1 reduce_window_sum.11
  33.1 0.2 select_reduce_fusion
  33.5 0.1 fusion.66
  33.7 51.4 %all-gather.3.cloned.1.call-done = bf16[2048,1024]{0,1:T(8,128)(2,1)} async-done(((bf16[2048,32]{0,1:T(8,128)(2,1)}), bf16[2048,1024]{0,1:T(8,128)(2,1)}) %all-gather.3.cloned.1.call-update) | async-done | bytes 4194320 | tf_op jit(solution)/shard_map/all_gather | solution.py:128
  85.0 3.4 %convolution_convert_fusion.2 = bf16[16,1024]{1,0:T(8,128)(2,1)S(1)} fusion(bf16[2048,1024]{0,1:T(8,128)(2,1)} %all-gather.3.cloned.1.call-done, bf16[16,2048]{1,0:T(8,128)(2,1)S(1)} %copy-done.1, f32[2048]{0:T(1024)S(1)} %convert_element_type.86, f32[16]{0:T(128)S(1)} %add_rsqrt_fusion.2), kind=kOutput, calls=%fused_computation.26 | convolution fusion | flops 67256320 | bytes 4300864 | tf_op jit(solution)/shard_map/dot_general | solution.py:126
  88.4 0.1 reshape.79
  88.5 0.2 fusion.62
  88.8 0.1 copy.95
  88.9 4.7 %fusion.81 = (f32[16,2,4,2]{2,3,1,0:T(2,128)S(1)}, f32[16,2,4,2,1024]{4,2,3,1,0:T(4,128)S(1)}) fusion(bf16[16,1024,2,2,64]{1,4,3,2,0:T(8,128)(2,1)} %bitcast.96, bf16[16,2,4,2,64]{4,3,2,1,0:T(2,128)(2,1)S(1)} %reshape.79, pred[16,1024]{1,0:T(8,128)(4,1)S(1)} %iota_compare_fusion), kind=kOutput, calls=%fused_computation.91 | convolution fusion | flops 34340608 | bytes 9487360 | tf_op jit(solution)/shard_map/bkgcd,bjkcd->bkgcj/dot_general | solution.py:64
  93.6 0.1 copy.79
  93.7 0.1 copy.80
  93.8 0.5 fusion.40
  94.3 0.1 copy.81
  94.5 0.1 copy.82
  94.7 0.1 copy.85
  94.8 0.5 fusion.39
  95.3 5.0 %multiply_reduce_fusion.2 = (f32[16,2,4]{2,1,0:T(2,128)S(1)}, f32[16,2,4,128]{3,2,1,0:T(4,128)S(1)}) fusion(f32[16,2,128]{2,1,0:T(2,128)S(1)} %reshape.86, f32[16,2,4]{2,1,0:T(2,128)S(1)} %copy.85, bf16[16,1024,2,128]{3,2,1,0:T(2,128)(2,1)} %param.26, f32[16,2,4,2,1024]{4,2,3,1,0:T(4,128)S(1)} %fusion.39, f32[2,4]{1,0:T(2,128)S(1)} %mul.149), kind=kOutput, calls=%fused_computation.60 | convolution fusion | flops 34013056 | bytes 9520160 | tf_op jit(solution)/shard_map/bkgj,bjkv->bkgv/dot_general | solution.py:82
  100.3 0.1 copy.86
  100.4 0.1 copy.87
  100.5 0.1 multiply_convert_fusion.2
  100.6 53.6 %all-gather.5.cloned.1.call-done = bf16[1024,2048]{0,1:T(8,128)(2,1)} async-done(((bf16[1024,64]{0,1:T(8,128)(2,1)}), bf16[1024,2048]{0,1:T(8,128)(2,1)}) %all-gather.5.cloned.1.call-update) | async-done | bytes 4194320 | tf_op jit(solution)/shard_map/all_gather | solution.py:136
  154.3 3.5 %multiply_reduce_fusion.1 = (f32[16]{0:T(128)S(1)}, f32[16,2048]{1,0:T(8,128)S(1)}) fusion(bf16[16,1024]{1,0:T(8,128)(2,1)S(1)} %convert_element_type.97, bf16[1024,2048]{0,1:T(8,128)(2,1)} %all-gather.5.cloned.1.call-done, bf16[16,2048]{1,0:T(8,128)(2,1)S(1)} %copy-done.1), kind=kOutput, calls=%fused_computation.56 | convolution fusion | flops 67370992 | bytes 4423744 | tf_op jit(solution)/shard_map/dot_general | solution.py:134
  157.8 0.3 convolution_convert_fusion
  158.1 0.2 reshape.83
  158.3 40.2 %all_to_all.15 = bf16[32,4,2048]{2,1,0:T(4,128)(2,1)S(1)} all-to-all(bf16[32,4,2048]{2,1,0:T(4,128)(2,1)S(1)} %reshape.83), channel_id=1, replica_groups=mesh['grp'=4,'ep_0'=16,'ep_1'=2] {'ep_0','ep_1'}, dimensions={0} | all-to-all | bytes 1048576 | tf_op jit(solution)/shard_map/all_to_all | solution.py:155
  198.6 0.1 reshape.84
  198.7 2.9 %fusion.20 = f32[128,1024]{1,0:T(8,128)S(1)} fusion(bf16[128,2048]{1,0:T(8,128)(2,1)S(1)} %reshape.84, bf16[1,2048,1024]{2,1,0:T(8,128)(2,1)} %param.29), kind=kOutput, calls=%fused_computation.20 | convolution fusion | flops 537001984 | bytes 5242880 | tf_op jit(solution)/shard_map/dot_general | solution.py:91
  201.6 4.9 %fusion.8 = bf16[128,2048]{1,0:T(8,128)(2,1)S(1)} fusion(bf16[1,1024,2048]{2,1,0:T(8,128)(2,1)} %param.31, f32[128,1024]{1,0:T(8,128)S(1)} %fusion.20, bf16[128,2048]{1,0:T(8,128)(2,1)S(1)} %reshape.84, bf16[1,2048,1024]{2,1,0:T(8,128)(2,1)} %param.30), kind=kOutput, calls=%fused_computation.9 | convolution fusion | flops 1075183616 | bytes 9961472 | tf_op jit(solution)/shard_map/dot_general | solution.py:96
  206.5 0.2 reshape_reshape_reshape.6
  206.7 0.2 copy.92
  206.9 4.2 %all_to_all.16 = bf16[16,2,1,4,2048]{4,3,0,2,1:T(4,128)(2,1)S(1)} all-to-all(bf16[16,2,1,4,2048]{4,3,0,2,1:T(4,128)(2,1)S(1)} %copy.92), channel_id=1, replica_groups=mesh['grp'=4,'ep_0'=16,'ep_1'=2] {'ep_1'}, dimensions={1} | all-to-all | bytes 1048576 | tf_op jit(solution)/shard_map/all_to_all | solution.py:32
  211.1 1.0 copy.93
  212.1 5.5 %all-to-all-start.2 = ((bf16[16,2,1,4,2048]{4,3,1,2,0:T(4,128)(2,1)}), bf16[16,2,1,4,2048]{4,3,1,2,0:T(4,128)(2,1)S(1)}, u32[]{:S(2)}, u32[]{:S(2)}) async-start(bf16[16,2,1,4,2048]{4,3,1,2,0:T(4,128)(2,1)} %copy.93), calls=%async_computation.2 | async-start | bytes 1048576 | tf_op jit(solution)/shard_map/all_to_all | solution.py:32
  217.9 29.9 %all-to-all-done.2 = bf16[16,2,1,4,2048]{4,3,1,2,0:T(4,128)(2,1)S(1)} async-done(((bf16[16,2,1,4,2048]{4,3,1,2,0:T(4,128)(2,1)}), bf16[16,2,1,4,2048]{4,3,1,2,0:T(4,128)(2,1)S(1)}, u32[]{:S(2)}, u32[]{:S(2)}) %all-to-all-start.2) | async-done | bytes 524320 | tf_op jit(solution)/shard_map/all_to_all | solution.py:32
  247.8 0.1 reshape_reshape_reshape.7
  247.9 0.7 gather_fusion
  248.6 0.2 reshape.97
  248.8 0.4 multiply_reduce_fusion
  249.2 0.6 add_convert_fusion
  (40 shorter events, 1.0 us)
Async XLA Ops:
  6.5 3.2 %copy-start = (bf16[2048,256]{1,0:T(8,128)(2,1)S(1)}, bf16[2048,256]{1,0:T(8,128)(2,1)}, u32[]{:S(2)}) copy-start(bf16[2048,256]{1,0:T(8,128)(2,1)} %param.20) | copy-start | bytes 3145732
  6.6 78.5 %all-gather.3.cloned.1.call-start = ((), (), s32[]{:S(2)}) async-start(), calls=%async_computation.3 | async-start | bytes 4325376 | tf_op jit(solution)/shard_map/all_gather | solution.py:128
  7.3 147.0 %all-gather.5.cloned.1.call-start = ((), (), s32[]{:S(2)}) async-start(), calls=%async_computation.4 | async-start | bytes 4325376 | tf_op jit(solution)/shard_map/all_gather | solution.py:136
  11.0 21.3 %copy-start.7 = (f32[8]{0:T(128)S(1)}, f32[8]{0:T(128)}, u32[]{:S(2)}) copy-start(f32[8]{0:T(128)} %param.24) | copy-start | bytes 100
  11.0 21.4 %copy-start.1 = (bf16[16,2048]{1,0:T(8,128)(2,1)S(1)}, bf16[16,2048]{1,0:T(8,128)(2,1)}, u32[]{:S(2)}) copy-start(bf16[16,2048]{1,0:T(8,128)(2,1)} %param.17) | copy-start | bytes 196612
  11.0 21.4 %copy-start.2 = (bf16[2048,256]{1,0:T(8,128)(2,1)S(1)}, bf16[2048,256]{1,0:T(8,128)(2,1)}, u32[]{:S(2)}) copy-start(bf16[2048,256]{1,0:T(8,128)(2,1)} %param.21) | copy-start | bytes 3145732
  11.0 21.7 %copy-start.8 = (bf16[128]{0:T(256)(128)(2,1)S(1)}, bf16[128]{0:T(256)(128)(2,1)}, u32[]{:S(2)}) copy-start(bf16[128]{0:T(256)(128)(2,1)} %param.23) | copy-start | bytes 772
  11.1 21.7 %copy-start.4 = (s32[16,4]{0,1:T(4,128)S(1)}, s32[16,4]{0,1:T(4,128)}, u32[]{:S(2)}) copy-start(s32[16,4]{0,1:T(4,128)} %param.32) | copy-start | bytes 772
  11.1 22.4 %copy-start.3 = (bf16[2048]{0:T(1024)(128)(2,1)S(1)}, bf16[2048]{0:T(1024)(128)(2,1)}, u32[]{:S(2)}) copy-start(bf16[2048]{0:T(1024)(128)(2,1)} %param.28) | copy-start | bytes 12292
  11.1 22.5 %copy-start.6 = (s32[16]{0:T(128)S(1)}, s32[16]{0:T(128)}, u32[]{:S(2)}) copy-start(s32[16]{0:T(128)} %param.27) | copy-start | bytes 196
  206.5 11.3 %copy-start.5 = (f32[16,4]{0,1:T(4,128)S(1)}, f32[16,4]{0,1:T(4,128)}, u32[]{:S(2)}) copy-start(f32[16,4]{0,1:T(4,128)} %param.33) | copy-start | bytes 772
  212.1 35.6 %all-to-all-start.2 = ((bf16[16,2,1,4,2048]{4,3,1,2,0:T(4,128)(2,1)}), bf16[16,2,1,4,2048]{4,3,1,2,0:T(4,128)(2,1)S(1)}, u32[]{:S(2)}, u32[]{:S(2)}) async-start(bf16[16,2,1,4,2048]{4,3,1,2,0:T(4,128)(2,1)} %copy.93), calls=%async_computation.2 | async-start | bytes 1048576 | tf_op jit(solution)/shard_map/all_to_all | solution.py:32
Sparse Core Ops, SparseCore 0:
  9.1 75.9 all-gather.2
  86.7 67.4 all-gather.4
where the time goes:
time: 258 us; the launch traced here: 257 us
  waiting for transfers between devices  136 us (53%)
  blocking collectives  44.4 us (17%)
  matrix products  26.3 us (10%)
  local copies, waits for them, and re-layouts  25.8 us (10%)
  between operations  13.7 us (5%)
  starting transfers between devices  5.6 us (2%)
  other arithmetic  4.51 us (2%)
    all_gather x1, waiting for transfers between devices, local(): lax.all_gather(out_weight, EP, axis=1, tiled=True)  53.6 us
    all_gather x1, waiting for transfers between devices, local(): lax.all_gather(query_weight, EP, axis=1, tiled=True)  51.4 us
    all_to_all x1, blocking collectives, local(): lax.all_to_all(outgoing, EP, split_axis=0, concat_axis=0, tiled=True)  40.2 us
    all_to_all x1, waiting for transfers between devices, moved_by_axis(): filled = lax.all_to_all(filled, axes[k], k, k, tiled=True)  29.9 us
    unnamed x21, local copies, waits for them, and re-layouts  21.5 us
    all_to_all x1, starting transfers between devices, moved_by_axis(): filled = lax.all_to_all(filled, axes[k], k, k, tiled=True)  5.54 us
  transfers between devices with their start and end apart: 3, of which 3 were waited for; matrix products, arithmetic and copies ran while one was open for 16% of the time, Pallas kernels for 0%

commit v1 on v0

v1 whole, which is shorter than its diff:
```python
import functools

import jax
import jax.numpy as jnp
from jax import lax
from jax.experimental import pallas as pl
from jax.experimental.pallas import tpu as pltpu
from jax.sharding import Mesh
from jax.sharding import PartitionSpec as P

EP = ("ep_0", "ep_1")
GRP_EP = ("grp", "ep_0", "ep_1")


epsilon = 1e-06
masked_score = -1e30
clamp_limit = 7.0
swish_alpha = 1.702


def rms_scaled(values, gain):
    floats = values.astype(jnp.float32)
    return (
        floats
        * lax.rsqrt(jnp.mean(floats * floats, axis=-1, keepdims=True) + epsilon)
        * gain.astype(jnp.float32)
    )


def core_swap(value):
    return lax.ppermute(value, "ep_1", [(0, 1), (1, 0)])


def ring_queries(normed, query_weight):
    count = normed.shape[0]
    chips = lax.axis_size("ep_0")
    cols = query_weight.shape[1]
    here = lax.axis_index("ep_0")
    core = lax.axis_index("ep_1")
    ahead = [(i, (i + 1) % chips) for i in range(chips)]
    behind = [(i, (i - 1) % chips) for i in range(chips)]
    both = jnp.concatenate([normed, core_swap(normed)], axis=0)

    def product(block):
        return jnp.dot(both, block, preferred_element_type=jnp.float32).astype(jnp.bfloat16)

    results = [None] * chips
    up = down = query_weight
    results[0] = product(query_weight)
    for step in range(1, chips // 2 + 1):
        up = lax.ppermute(up, "ep_0", ahead)
        if step < chips - step:
            down = lax.ppermute(down, "ep_0", behind)
        results[step] = product(up)
        if step < chips - step:
            results[chips - step] = product(down)
    stacked = jnp.stack(results[::-1])
    twice = jnp.concatenate([stacked, stacked], axis=0)
    placed = lax.dynamic_slice_in_dim(twice, chips - 1 - here, chips, axis=0)
    mine = placed[:, :count]
    theirs = core_swap(placed[:, count:])
    low = jnp.where(core == 0, mine, theirs)
    high = jnp.where(core == 0, theirs, mine)
    full = jnp.stack([low, high], axis=1)
    return jnp.transpose(full, (2, 0, 1, 3)).reshape(count, chips * 2 * cols)


def attention_kernel(
    group_size, chunk, lens_ref, q_ref, nk_ref, nv_ref, lam_ref, gain_ref, k_hbm, v_hbm, o_ref, k_buf, v_buf, k_sem, v_sem
):
    count, heads, width = q_ref.shape
    kv_count = nk_ref.shape[1]
    group = heads // kv_count
    half = width // 2
    rows = k_buf.shape[1]
    chunk_rows = chunk * kv_count
    chunks = rows // chunk_rows
    inv_scale = half ** (-0.5)

    def pieces(s, c):
        where = pl.ds(pl.multiple_of(c * chunk_rows, chunk_rows), chunk_rows)
        return (
            pltpu.make_async_copy(k_hbm.at[s, where], k_buf.at[s, where], k_sem.at[s]),
            pltpu.make_async_copy(v_hbm.at[s, where], v_buf.at[s, where], v_sem.at[s]),
        )

    def used(s):
        return (lens_ref[s] + chunk - 1) // chunk

    def fetch(s, _):
        n = used(s)

        def start(c, _):
            for copy in pieces(s, c):
                copy.start()
            return 0

        lax.fori_loop(0, n, start, 0)

        def clear(c, _):
            where = pl.ds(pl.multiple_of(c * chunk_rows, chunk_rows), chunk_rows)
            v_buf[s, where] = jnp.zeros((chunk_rows, width), v_buf.dtype)
            return 0

        lax.fori_loop(n, chunks, clear, 0)
        return 0

    lax.fori_loop(0, count, fetch, 0)

    lane = lax.broadcasted_iota(jnp.int32, (heads, width), 1)
    head_row = lax.broadcasted_iota(jnp.int32, (heads, width), 0)
    column = lax.broadcasted_iota(jnp.int32, (2 * heads, rows), 1)
    score_row = lax.broadcasted_iota(jnp.int32, (2 * heads, rows), 0)
    kv_of_row = (score_row % heads) // group
    own_kv = (column % kv_count) == kv_of_row
    position = column // kv_count
    gain = gain_ref[...].astype(jnp.float32)
    lam = lam_ref[...][:, :1]

    def spread(values):
        out = jnp.broadcast_to(values[kv_count - 1 :], (heads, width))
        for k in range(kv_count - 1):
            out = jnp.where(head_row // group == k, jnp.broadcast_to(values[k : k + 1], (heads, width)), out)
        return out

    def one(s):
        q = q_ref[s]
        zero = jnp.zeros_like(q)
        split = jnp.concatenate([jnp.where(lane < half, q, zero), jnp.where(lane < half, zero, q)], axis=0)
        own_key = spread(nk_ref[s].astype(jnp.float32))
        own_val = spread(nv_ref[s].astype(jnp.float32))
        own_score = (
            jnp.sum(split.astype(jnp.float32) * jnp.concatenate([own_key, own_key], axis=0), axis=1, keepdims=True)
            * inv_scale
        )
        scores = (
            lax.dot_general(split, k_buf[s], (((1,), (1,)), ((), ())), preferred_element_type=jnp.float32) * inv_scale
        )
        scores = jnp.where(own_kv & (position < lens_ref[s]), scores, masked_score)
        highest = jnp.maximum(jnp.max(scores, axis=1, keepdims=True), own_score)
        expd = jnp.exp(scores - highest)
        own_exp = jnp.exp(own_score - highest)
        denominator = jnp.sum(expd, axis=1, keepdims=True) + own_exp
        inverse = 1.0 / denominator
        factor = inverse[heads:] * lam
        weights = (expd[:heads] * inverse[:heads] - expd[heads:] * factor).astype(jnp.bfloat16)
        own_weight = (own_exp[:heads] * inverse[:heads] - own_exp[heads:] * factor).astype(jnp.bfloat16)
        attended = jnp.dot(weights, v_buf[s], preferred_element_type=jnp.float32)
        attended = attended + own_weight.astype(jnp.float32) * own_val
        scale = lax.rsqrt(jnp.mean(attended * attended, axis=1, keepdims=True) + epsilon)
        o_ref[s] = (attended * scale * gain).astype(o_ref.dtype)

    def step(g, _):
        for i in range(group_size):
            s = g * group_size + i

            def wait(c, _):
                for copy in pieces(s, c):
                    copy.wait()
                return 0

            lax.fori_loop(0, used(s), wait, 0)
        for i in range(group_size):
            one(g * group_size + i)
        return 0

    lax.fori_loop(0, count // group_size, step, 0)


def attention(queries, new_keys, new_values, cache_keys, cache_values, lengths, lambdas, head_gain):
    count, ctx_len, kv_count, width = cache_keys.shape
    heads = lambdas.shape[0]
    vmem = pl.BlockSpec(memory_space=pltpu.VMEM)
    smem = pl.BlockSpec(memory_space=pltpu.SMEM)
    hbm = pl.BlockSpec(memory_space=pl.ANY)
    rows = ctx_len * kv_count
    out = pl.pallas_call(
        functools.partial(attention_kernel, 2, 128),
        out_shape=jax.ShapeDtypeStruct((count, heads, width), jnp.bfloat16),
        in_specs=[smem, vmem, vmem, vmem, vmem, vmem, hbm, hbm],
        out_specs=vmem,
        scratch_shapes=[
            pltpu.VMEM((count, rows, width), jnp.bfloat16),
            pltpu.VMEM((count, rows, width), jnp.bfloat16),
            pltpu.SemaphoreType.DMA((count,)),
            pltpu.SemaphoreType.DMA((count,)),
        ],
        compiler_params=pltpu.CompilerParams(vmem_limit_bytes=40 * 2**20),
        name="attention",
    )(
        lengths,
        queries.reshape(count, heads, width),
        new_keys.reshape(count, kv_count, width),
        new_values.reshape(count, kv_count, width),
        jnp.broadcast_to(lambdas[:, None], (heads, width)),
        head_gain.reshape(1, width),
        cache_keys.reshape(count, rows, width),
        cache_values.reshape(count, rows, width),
    )
    return out.reshape(count, heads * width)


def expert_mlp(inputs, gate_w, up_w, down_w):
    gate = jnp.dot(inputs, gate_w, preferred_element_type=jnp.float32)
    upper = jnp.dot(inputs, up_w, preferred_element_type=jnp.float32)
    gate = jnp.minimum(gate, clamp_limit)
    upper = jnp.clip(upper, -clamp_limit, clamp_limit)
    act = ((upper + 1.0) * gate * jax.nn.sigmoid(swish_alpha * gate)).astype(jnp.bfloat16)
    return jnp.dot(act, down_w, preferred_element_type=jnp.float32).astype(jnp.bfloat16)


def local(
    tokens,
    norm_gain,
    query_weight,
    key_weight,
    value_weight,
    out_weight,
    head_gain,
    lambdas,
    cache_keys,
    cache_values,
    lengths,
    moe_gain,
    gate_weight,
    up_weight,
    down_weight,
    routes,
    route_weights,
):
    count = tokens.shape[0]
    width = tokens.shape[1]
    topk = routes.shape[1]
    out_full = lax.all_gather(out_weight, EP, axis=1, tiled=True)
    normed = rms_scaled(tokens, norm_gain).astype(jnp.bfloat16)
    new_keys = jnp.dot(normed, key_weight, preferred_element_type=jnp.float32).astype(jnp.bfloat16)
    new_values = jnp.dot(normed, value_weight, preferred_element_type=jnp.float32).astype(
        jnp.bfloat16
    )
    queries = ring_queries(normed, query_weight)
    head_out = attention(
        queries, new_keys, new_values, cache_keys, cache_values, lengths, lambdas, head_gain
    )
    attn_out = jnp.dot(head_out, out_full, preferred_element_type=jnp.float32).astype(jnp.bfloat16)
    residual = (tokens.astype(jnp.float32) + attn_out.astype(jnp.float32)).astype(jnp.bfloat16)
    moe_in = rms_scaled(residual, moe_gain).astype(jnp.bfloat16)
    experts = lax.axis_size(EP)
    capacity = min(count, max(2, 2 * count * topk // experts))
    onehot = (routes.reshape(-1)[:, None] == jnp.arange(experts, dtype=jnp.int32)[None, :]).astype(
        jnp.int32
    )
    earlier_all = jnp.cumsum(onehot, axis=0) - onehot
    ranks = jnp.sum(earlier_all * onehot, axis=1).reshape(count, topk)
    slot_id = routes * capacity + ranks
    slot_range = jnp.arange(experts * capacity, dtype=jnp.int32)
    dispatch = jnp.any(slot_id[None, :, :] == slot_range[:, None, None], axis=2).astype(
        jnp.bfloat16
    )
    outgoing = jnp.dot(dispatch, moe_in, preferred_element_type=jnp.float32).astype(jnp.bfloat16)
    outgoing = outgoing.reshape(experts, capacity, width)
    received = lax.all_to_all(outgoing, EP, split_axis=0, concat_axis=0, tiled=True)
    flat_rows = received.reshape(-1, width)
    results = expert_mlp(flat_rows, gate_weight[0], up_weight[0], down_weight[0]).reshape(
        received.shape
    )
    returned = lax.all_to_all(results, EP, split_axis=0, concat_axis=0, tiled=True)
    picked = returned.reshape(-1, width)[slot_id].astype(jnp.float32)
    moe_sum = jnp.sum(route_weights[:, :, None] * picked, axis=1)
    return (residual.astype(jnp.float32) + moe_sum).astype(jnp.bfloat16)


def solution(mesh):
    chips = mesh.shape["ep"] // 2
    torus = Mesh(mesh.devices.reshape(mesh.shape["grp"], chips, 2), ("grp", "ep_0", "ep_1"))
    return jax.shard_map(
        local,
        mesh=torus,
        in_specs=(
            P(GRP_EP, None),
            P(),
            P(None, EP),
            P(),
            P(),
            P(None, EP),
            P(),
            P(),
            P(GRP_EP, None, None, None),
            P(GRP_EP, None, None, None),
            P(GRP_EP),
            P(),
            P(EP, None, None),
            P(EP, None, None),
            P(EP, None, None),
            P(GRP_EP, None),
            P(GRP_EP, None),
        ),
        out_specs=P(GRP_EP, None),
        check_vma=False,
    )
```

time: 258 us -> 212 us (0.82)
  waiting for transfers between devices: 136 us -> 69.5 us
  starting transfers between devices: 5.6 us -> 37.9 us
  Pallas kernels: 0 us -> 20.1 us
  local copies, waits for them, and re-layouts: 25.8 us -> 7.49 us
  matrix products: 26.3 us -> 16.2 us
  blocking collectives: 44.4 us -> 40 us
    all_gather x2 -> x1, waiting for transfers between devices: 105 us -> 0.02 us  [local(): out_full = lax.all_gather(out_weight, EP, axis=1, tiled=True)]
    ppermute x0 -> x17, waiting for transfers between devices: none -> 36.8 us  [the longest x7 18.9 us: ring_queries(): down = lax.ppermute(down, 'ep_0', behind)]
    ppermute x0 -> x17, starting transfers between devices: none -> 31.9 us  [the longest x7 31.4 us: ring_queries(): down = lax.ppermute(down, 'ep_0', behind)]
    pallas_call x0 -> x1, Pallas kernels: none -> 20.1 us  [attention(): pl.pallas_call(functools.partial(attention_kernel, 2, 128), out_shape=jax...]
    unnamed x21 -> x35, local copies, waits for them, and re-layouts: 21.5 us -> 4.43 us
    dot_general x5 -> x17, matrix products: 16.8 us -> 6.2 us  [the longest x1 3.49 us: local(): jnp.dot(head_out, out_full, preferred_element_type=jnp.float32)]
    all_to_all x1 -> x0, blocking collectives: 4.17 us -> none  [moved_by_axis(): filled = lax.all_to_all(filled, axes[k], k, k, tiled=True)]
  transfers between devices with their start and end apart: 3 -> 19, of which waited for: 3 -> 12; matrix products, arithmetic and copies ran while one was open for 16% -> 4% of each run, Pallas kernels for 0% -> 10%
where the time goes in v1:
time: 212 us; the launch traced here: 209 us
  waiting for transfers between devices  69.5 us (33%)
  blocking collectives  40 us (19%)
  starting transfers between devices  37.9 us (18%)
  Pallas kernels  20.1 us (9%)
  matrix products  16.2 us (8%)
  between operations  13.9 us (7%)
  local copies, waits for them, and re-layouts  7.49 us (4%)
  other arithmetic  4.11 us (2%)
    all_to_all x1, blocking collectives, local(): lax.all_to_all(outgoing, EP, split_axis=0, concat_axis=0, tiled=True)  40 us
    all_to_all x1, waiting for transfers between devices, local(): lax.all_to_all(results, EP, split_axis=0, concat_axis=0, tiled=True)  31.9 us
    ppermute x7, starting transfers between devices, ring_queries(): down = lax.ppermute(down, 'ep_0', behind)  31.4 us
    pallas_call x1, Pallas kernels, attention(): pl.pallas_call(functools.partial(attention_kernel, 2, 128), out_shape=jax...  20.1 us
    ppermute x7, waiting for transfers between devices, ring_queries(): down = lax.ppermute(down, 'ep_0', behind)  18.9 us
    ppermute x8, waiting for transfers between devices, ring_queries(): up = lax.ppermute(up, 'ep_0', ahead)  16.8 us
    all_to_all x1, starting transfers between devices, local(): lax.all_to_all(results, EP, split_axis=0, concat_axis=0, tiled=True)  5.96 us
    dot_general x1, matrix products, expert_mlp(): jnp.dot(act, down_w, preferred_element_type=jnp.float32)  4.97 us
  transfers between devices with their start and end apart: 19, of which 12 were waited for; matrix products, arithmetic and copies ran while one was open for 4% of the time, Pallas kernels for 10%

profile of v1, /device:TPU:196, one launch (start us, length us, event | category | flops | bytes accessed | tf_op | source)
XLA Modules:
  0.0 209.2 jit_solution(15916153638796725527)
XLA Ops:
  6.6 0.7 all-gather.2.cloned.1.call-update
  7.3 8.5 %collective-permute-start.1 = (bf16[2048,32]{0,1:T(8,128)(2,1)}, bf16[2048,32]{0,1:T(8,128)(2,1)S(1)}, u32[]{:S(2)}, u32[]{:S(2)}) collective-permute-start(bf16[2048,32]{0,1:T(8,128)(2,1)} %param.19), channel_id=1, source_target_pairs={{0,30},{2,0},{4,2},{6,4},{8,6},{10,8},{12,10},{14,12},{16,14},{18,... | collective-permute-start | bytes 393224 | tf_op jit(solution)/shard_map/ppermute | solution.py:53
  15.8 0.7 convert_element_type.103
  16.5 1.0 fusion.58
  17.5 0.9 fusion.60
  18.5 0.8 copy.28
  19.6 0.2 select_reduce_fusion
  19.9 0.3 convolution_convert_fusion.3
  20.1 1.5 convolution_convert_fusion.2
  21.7 4.1 %collective-permute-start.2 = (bf16[2048,32]{0,1:T(8,128)(2,1)S(1)}, bf16[2048,32]{0,1:T(8,128)(2,1)S(1)}, u32[]{:S(2)}, u32[]{:S(2)}) collective-permute-start(bf16[2048,32]{0,1:T(8,128)(2,1)S(1)} %collective-permute-done.1), channel_id=1, source_target_pairs={{0,30},{2,0},{4,2},{6,4},{8,6},{10,8},{12,10},{14,12},{16,14},{18,... | collective-permute-start | bytes 393224 | tf_op jit(solution)/shard_map/ppermute | solution.py:53
  26.0 4.6 %collective-permute-done.2 = bf16[2048,32]{0,1:T(8,128)(2,1)S(1)} collective-permute-done((bf16[2048,32]{0,1:T(8,128)(2,1)S(1)}, bf16[2048,32]{0,1:T(8,128)(2,1)S(1)}, u32[]{:S(2)}, u32[]{:S(2)}) %collective-permute-start.2) | collective-permute-done | bytes 131104 | tf_op jit(solution)/shard_map/ppermute | solution.py:53
  30.6 2.5 %collective-permute-start.3 = (bf16[2048,32]{0,1:T(8,128)(2,1)S(1)}, bf16[2048,32]{0,1:T(8,128)(2,1)S(1)}, u32[]{:S(2)}, u32[]{:S(2)}) collective-permute-start(bf16[2048,32]{0,1:T(8,128)(2,1)S(1)} %collective-permute-done.2), channel_id=1, source_target_pairs={{0,30},{2,0},{4,2},{6,4},{8,6},{10,8},{12,10},{14,12},{16,14},{18,... | collective-permute-start | bytes 393224 | tf_op jit(solution)/shard_map/ppermute | solution.py:53
  33.1 0.2 collective-permute-start.10
  33.5 3.0 %collective-permute-done.3 = bf16[2048,32]{0,1:T(8,128)(2,1)S(1)} collective-permute-done((bf16[2048,32]{0,1:T(8,128)(2,1)S(1)}, bf16[2048,32]{0,1:T(8,128)(2,1)S(1)}, u32[]{:S(2)}, u32[]{:S(2)}) %collective-permute-start.3) | collective-permute-done | bytes 131104 | tf_op jit(solution)/shard_map/ppermute | solution.py:53
  36.5 4.5 %collective-permute-start.4 = (bf16[2048,32]{0,1:T(8,128)(2,1)S(1)}, bf16[2048,32]{0,1:T(8,128)(2,1)S(1)}, u32[]{:S(2)}, u32[]{:S(2)}) collective-permute-start(bf16[2048,32]{0,1:T(8,128)(2,1)S(1)} %collective-permute-done.3), channel_id=1, source_target_pairs={{0,30},{2,0},{4,2},{6,4},{8,6},{10,8},{12,10},{14,12},{16,14},{18,... | collective-permute-start | bytes 393224 | tf_op jit(solution)/shard_map/ppermute | solution.py:53
  41.0 1.2 collective-permute-done.10
  42.4 1.7 collective-permute-done.4
  44.1 4.2 %collective-permute-start.5 = (bf16[2048,32]{0,1:T(8,128)(2,1)S(1)}, bf16[2048,32]{0,1:T(8,128)(2,1)S(1)}, u32[]{:S(2)}, u32[]{:S(2)}) collective-permute-start(bf16[2048,32]{0,1:T(8,128)(2,1)S(1)} %collective-permute-done.4), channel_id=1, source_target_pairs={{0,30},{2,0},{4,2},{6,4},{8,6},{10,8},{12,10},{14,12},{16,14},{18,... | collective-permute-start | bytes 393224 | tf_op jit(solution)/shard_map/ppermute | solution.py:53
  48.3 0.3 collective-permute-done.11
  48.9 3.9 %collective-permute-done.5 = bf16[2048,32]{0,1:T(8,128)(2,1)S(1)} collective-permute-done((bf16[2048,32]{0,1:T(8,128)(2,1)S(1)}, bf16[2048,32]{0,1:T(8,128)(2,1)S(1)}, u32[]{:S(2)}, u32[]{:S(2)}) %collective-permute-start.5) | collective-permute-done | bytes 131104 | tf_op jit(solution)/shard_map/ppermute | solution.py:53
  52.8 4.4 %collective-permute-start.6 = (bf16[2048,32]{0,1:T(8,128)(2,1)S(1)}, bf16[2048,32]{0,1:T(8,128)(2,1)S(1)}, u32[]{:S(2)}, u32[]{:S(2)}) collective-permute-start(bf16[2048,32]{0,1:T(8,128)(2,1)S(1)} %collective-permute-done.5), channel_id=1, source_target_pairs={{0,30},{2,0},{4,2},{6,4},{8,6},{10,8},{12,10},{14,12},{16,14},{18,... | collective-permute-start | bytes 393224 | tf_op jit(solution)/shard_map/ppermute | solution.py:53
  57.3 5.6 %collective-permute-done.6 = bf16[2048,32]{0,1:T(8,128)(2,1)S(1)} collective-permute-done((bf16[2048,32]{0,1:T(8,128)(2,1)S(1)}, bf16[2048,32]{0,1:T(8,128)(2,1)S(1)}, u32[]{:S(2)}, u32[]{:S(2)}) %collective-permute-start.6) | collective-permute-done | bytes 131104 | tf_op jit(solution)/shard_map/ppermute | solution.py:53
  63.0 3.2 %collective-permute-start.7 = (bf16[2048,32]{0,1:T(8,128)(2,1)S(1)}, bf16[2048,32]{0,1:T(8,128)(2,1)S(1)}, u32[]{:S(2)}, u32[]{:S(2)}) collective-permute-start(bf16[2048,32]{0,1:T(8,128)(2,1)S(1)} %collective-permute-done.6), channel_id=1, source_target_pairs={{0,30},{2,0},{4,2},{6,4},{8,6},{10,8},{12,10},{14,12},{16,14},{18,... | collective-permute-start | bytes 393224 | tf_op jit(solution)/shard_map/ppermute | solution.py:53
  66.2 0.9 collective-permute-done.13
  67.3 9.0 %collective-permute-done.14 = bf16[2048,32]{0,1:T(8,128)(2,1)S(1)} collective-permute-done((bf16[2048,32]{0,1:T(8,128)(2,1)S(1)}, bf16[2048,32]{0,1:T(8,128)(2,1)S(1)}, u32[]{:S(2)}, u32[]{:S(2)}) %collective-permute-start.14) | collective-permute-done | bytes 131104 | tf_op jit(solution)/shard_map/ppermute | solution.py:51
  76.5 5.3 %collective-permute-done.15 = bf16[2048,32]{0,1:T(8,128)(2,1)S(1)} collective-permute-done((bf16[2048,32]{0,1:T(8,128)(2,1)S(1)}, bf16[2048,32]{0,1:T(8,128)(2,1)S(1)}, u32[]{:S(2)}, u32[]{:S(2)}) %collective-permute-start.15) | collective-permute-done | bytes 131104 | tf_op jit(solution)/shard_map/ppermute | solution.py:51
  82.0 0.2 constant_dynamic-update-slice_fusion.23
  82.2 0.2 constant_dynamic-update-slice_fusion.22
  82.4 0.2 constant_dynamic-update-slice_fusion.21
  82.6 0.2 constant_dynamic-update-slice_fusion.20
  82.7 0.2 constant_dynamic-update-slice_fusion.19
  83.1 0.2 constant_dynamic-update-slice_fusion.17
  84.0 1.1 collective-permute-done.16
  85.5 3.4 %copy-done.1 = bf16[16,1024,2,128]{3,2,1,0:T(2,128)(2,1)S(1)} copy-done((bf16[16,1024,2,128]{3,2,1,0:T(2,128)(2,1)S(1)}, bf16[16,1024,2,128]{3,2,1,0:T(2,128)(2,1)}, u32[]{:S(2)}) %copy-start.1) | copy-done | bytes 8388632
  88.9 20.1 %attention.1 = bf16[16,8,128]{2,1,0:T(8,128)(2,1)S(1)} custom-call(s32[16]{0:T(128)S(1)} %copy-done.2, bf16[16,8,128]{2,1,0:T(8,128)(2,1)S(1)} %reshape_reshape.3.q_ref, bf16[16,2,128]{2,1,0:T(2,128)(2,1)S(1)} %reshape.55.nk_ref, bf16[16,2,128]{2,1,0:T(2,128)(2,1)S(1)} %reshape.56.nv_ref, f32[8,128]{1,0:T(8,128)S(1)} %broadcast_in_dim.4.lam_ref, ...), custom_call_target="tpu_custom_call" | custom-call | tf_op jit(solution)/shard_map/attention/pallas_call | solution.py:177
  109.0 3.5 %multiply_reduce_fusion.1 = (f32[16]{0:T(128)S(1)}, f32[16,2048]{1,0:T(8,128)S(1)}) fusion(bf16[1024,2048]{0,1:T(8,128)(2,1)} %all-gather.2.cloned.1.call-done, bf16[2,8,8,128]{3,2,1,0:T(8,128)(2,1)S(1)} %bitcast.97, bf16[16,2048]{1,0:T(8,128)(2,1)S(1)} %copy-done.4), kind=kOutput, calls=%fused_computation.73 | convolution fusion | flops 67370992 | bytes 4423744 | tf_op jit(solution)/shard_map/dot_general | solution.py:244
  112.5 0.4 convolution_convert_fusion
  112.9 0.2 reshape.62
  113.1 40.0 %all_to_all.10 = bf16[32,4,2048]{2,1,0:T(4,128)(2,1)S(1)} all-to-all(bf16[32,4,2048]{2,1,0:T(4,128)(2,1)S(1)} %reshape.62), channel_id=1, replica_groups=mesh['grp'=4,'ep_0'=16,'ep_1'=2] {'ep_0','ep_1'}, dimensions={0} | all-to-all | bytes 1048576 | tf_op jit(solution)/shard_map/all_to_all | solution.py:261
  153.3 2.9 %fusion.16 = f32[128,1024]{1,0:T(8,128)S(1)} fusion(bf16[128,2048]{1,0:T(8,128)(2,1)S(1)} %reshape.63, bf16[1,2048,1024]{2,1,0:T(8,128)(2,1)} %param.29), kind=kOutput, calls=%fused_computation.15 | convolution fusion | flops 537001984 | bytes 5242880 | tf_op jit(solution)/shard_map/dot_general | solution.py:204
  156.2 5.0 %fusion.6 = bf16[128,2048]{1,0:T(8,128)(2,1)S(1)} fusion(bf16[1,1024,2048]{2,1,0:T(8,128)(2,1)} %param.31, f32[128,1024]{1,0:T(8,128)S(1)} %fusion.16, bf16[128,2048]{1,0:T(8,128)(2,1)S(1)} %reshape.63, bf16[1,2048,1024]{2,1,0:T(8,128)(2,1)} %param.30), kind=kOutput, calls=%fused_computation.7 | convolution fusion | flops 1075183616 | bytes 9961472 | tf_op jit(solution)/shard_map/dot_general | solution.py:209
  161.2 1.0 reshape.64
  162.2 6.0 %all-to-all-start.1 = ((bf16[32,4,2048]{2,1,0:T(4,128)(2,1)}), bf16[32,4,2048]{2,1,0:T(4,128)(2,1)S(1)}, u32[]{:S(2)}, u32[]{:S(2)}) async-start(bf16[32,4,2048]{2,1,0:T(4,128)(2,1)} %reshape.64), calls=%async_computation.1 | async-start | bytes 1048576 | tf_op jit(solution)/shard_map/all_to_all | solution.py:266
  168.4 31.9 %all-to-all-done.1 = bf16[32,4,2048]{2,1,0:T(4,128)(2,1)S(1)} async-done(((bf16[32,4,2048]{2,1,0:T(4,128)(2,1)}), bf16[32,4,2048]{2,1,0:T(4,128)(2,1)S(1)}, u32[]{:S(2)}, u32[]{:S(2)}) %all-to-all-start.1) | async-done | bytes 524320 | tf_op jit(solution)/shard_map/all_to_all | solution.py:266
  200.4 0.7 gather_fusion
  201.1 0.2 reshape.76
  201.3 0.4 multiply_reduce_fusion
  201.7 0.6 add_convert_fusion
  (83 shorter events, 3.6 us)
Async XLA Ops:
  6.5 13.3 %copy-start = (bf16[2048,256]{1,0:T(8,128)(2,1)S(1)}, bf16[2048,256]{1,0:T(8,128)(2,1)}, u32[]{:S(2)}) copy-start(bf16[2048,256]{1,0:T(8,128)(2,1)} %param.20) | copy-start | bytes 3145732
  6.6 76.7 %copy-start.8 = (bf16[2048,32]{0,1:T(8,128)(2,1)S(1)}, bf16[2048,32]{0,1:T(8,128)(2,1)}, u32[]{:S(2)}) copy-start(bf16[2048,32]{0,1:T(8,128)(2,1)} %param.19) | copy-start | bytes 393220
  6.6 102.4 %all-gather.2.cloned.1.call-start = ((), (), s32[]{:S(2)}) async-start(), calls=%async_computation.2 | async-start | bytes 4325376 | tf_op jit(solution)/shard_map/all_gather | solution.py:234
  7.3 14.4 %collective-permute-start.1 = (bf16[2048,32]{0,1:T(8,128)(2,1)}, bf16[2048,32]{0,1:T(8,128)(2,1)S(1)}, u32[]{:S(2)}, u32[]{:S(2)}) collective-permute-start(bf16[2048,32]{0,1:T(8,128)(2,1)} %param.19), channel_id=1, source_target_pairs={{0,30},{2,0},{4,2},{6,4},{8,6},{10,8},{12,10},{14,12},{16,14},{18,... | collective-permute-start | bytes 393224 | tf_op jit(solution)/shard_map/ppermute | solution.py:53
  15.8 10.0 %collective-permute-start.8 = (bf16[2048,32]{0,1:T(8,128)(2,1)}, bf16[2048,32]{0,1:T(8,128)(2,1)S(1)}, u32[]{:S(2)}, u32[]{:S(2)}) collective-permute-start(bf16[2048,32]{0,1:T(8,128)(2,1)} %param.19), channel_id=1, source_target_pairs={{0,2},{2,4},{4,6},{6,8},{8,10},{10,12},{12,14},{14,16},{16,18},{18... | collective-permute-start | bytes 393224 | tf_op jit(solution)/shard_map/ppermute | solution.py:51
  18.4 7.4 %collective-permute-start = (bf16[16,2048]{1,0:T(8,128)(2,1)S(1)}, bf16[16,2048]{1,0:T(8,128)(2,1)S(1)}, u32[]{:S(2)}, u32[]{:S(2)}) collective-permute-start(bf16[16,2048]{1,0:T(8,128)(2,1)S(1)} %fusion.60), channel_id=1, source_target_pairs={{0,1},{1,0},{2,3},{3,2},{4,5},{5,4},{6,7},{7,6},{8,9},{9,8},{10,11... | collective-permute-start | bytes 196616 | tf_op jit(solution)/shard_map/ppermute | solution.py:31
  19.5 64.5 %copy-start.5 = (bf16[2048]{0:T(1024)(128)(2,1)S(1)}, bf16[2048]{0:T(1024)(128)(2,1)}, u32[]{:S(2)}) copy-start(bf16[2048]{0:T(1024)(128)(2,1)} %param.28) | copy-start | bytes 12292
  20.1 65.3 %copy-start.7 = (f32[8]{0:T(128)S(1)}, f32[8]{0:T(128)}, u32[]{:S(2)}) copy-start(f32[8]{0:T(128)} %param.24) | copy-start | bytes 100
  20.1 65.4 %copy-start.2 = (s32[16]{0:T(128)S(1)}, s32[16]{0:T(128)}, u32[]{:S(2)}) copy-start(s32[16]{0:T(128)} %lens_ref.1) | copy-start | bytes 196
  20.1 65.4 %copy-start.3 = (bf16[128]{0:T(256)(128)(2,1)S(1)}, bf16[128]{0:T(256)(128)(2,1)}, u32[]{:S(2)}) copy-start(bf16[128]{0:T(256)(128)(2,1)} %param.23) | copy-start | bytes 772
  21.7 8.9 %collective-permute-start.2 = (bf16[2048,32]{0,1:T(8,128)(2,1)S(1)}, bf16[2048,32]{0,1:T(8,128)(2,1)S(1)}, u32[]{:S(2)}, u32[]{:S(2)}) collective-permute-start(bf16[2048,32]{0,1:T(8,128)(2,1)S(1)} %collective-permute-done.1), channel_id=1, source_target_pairs={{0,30},{2,0},{4,2},{6,4},{8,6},{10,8},{12,10},{14,12},{16,14},{18,... | collective-permute-start | bytes 393224 | tf_op jit(solution)/shard_map/ppermute | solution.py:53
  25.8 7.3 %collective-permute-start.9 = (bf16[2048,32]{0,1:T(8,128)(2,1)S(1)}, bf16[2048,32]{0,1:T(8,128)(2,1)S(1)}, u32[]{:S(2)}, u32[]{:S(2)}) collective-permute-start(bf16[2048,32]{0,1:T(8,128)(2,1)S(1)} %collective-permute-done.8), channel_id=1, source_target_pairs={{0,2},{2,4},{4,6},{6,8},{8,10},{10,12},{12,14},{14,16},{16,18},{18... | collective-permute-start | bytes 393224 | tf_op jit(solution)/shard_map/ppermute | solution.py:51
  30.6 5.9 %collective-permute-start.3 = (bf16[2048,32]{0,1:T(8,128)(2,1)S(1)}, bf16[2048,32]{0,1:T(8,128)(2,1)S(1)}, u32[]{:S(2)}, u32[]{:S(2)}) collective-permute-start(bf16[2048,32]{0,1:T(8,128)(2,1)S(1)} %collective-permute-done.2), channel_id=1, source_target_pairs={{0,30},{2,0},{4,2},{6,4},{8,6},{10,8},{12,10},{14,12},{16,14},{18,... | collective-permute-start | bytes 393224 | tf_op jit(solution)/shard_map/ppermute | solution.py:53
  33.1 9.1 %collective-permute-start.10 = (bf16[2048,32]{0,1:T(8,128)(2,1)S(1)}, bf16[2048,32]{0,1:T(8,128)(2,1)S(1)}, u32[]{:S(2)}, u32[]{:S(2)}) collective-permute-start(bf16[2048,32]{0,1:T(8,128)(2,1)S(1)} %collective-permute-done.9), channel_id=1, source_target_pairs={{0,2},{2,4},{4,6},{6,8},{8,10},{10,12},{12,14},{14,16},{16,18},{18... | collective-permute-start | bytes 393224 | tf_op jit(solution)/shard_map/ppermute | solution.py:51
  36.5 7.7 %collective-permute-start.4 = (bf16[2048,32]{0,1:T(8,128)(2,1)S(1)}, bf16[2048,32]{0,1:T(8,128)(2,1)S(1)}, u32[]{:S(2)}, u32[]{:S(2)}) collective-permute-start(bf16[2048,32]{0,1:T(8,128)(2,1)S(1)} %collective-permute-done.3), channel_id=1, source_target_pairs={{0,30},{2,0},{4,2},{6,4},{8,6},{10,8},{12,10},{14,12},{16,14},{18,... | collective-permute-start | bytes 393224 | tf_op jit(solution)/shard_map/ppermute | solution.py:53
  42.2 6.4 %collective-permute-start.11 = (bf16[2048,32]{0,1:T(8,128)(2,1)S(1)}, bf16[2048,32]{0,1:T(8,128)(2,1)S(1)}, u32[]{:S(2)}, u32[]{:S(2)}) collective-permute-start(bf16[2048,32]{0,1:T(8,128)(2,1)S(1)} %collective-permute-done.10), channel_id=1, source_target_pairs={{0,2},{2,4},{4,6},{6,8},{8,10},{10,12},{12,14},{14,16},{16,18},{18... | collective-permute-start | bytes 393224 | tf_op jit(solution)/shard_map/ppermute | solution.py:51
  44.1 8.6 %collective-permute-start.5 = (bf16[2048,32]{0,1:T(8,128)(2,1)S(1)}, bf16[2048,32]{0,1:T(8,128)(2,1)S(1)}, u32[]{:S(2)}, u32[]{:S(2)}) collective-permute-start(bf16[2048,32]{0,1:T(8,128)(2,1)S(1)} %collective-permute-done.4), channel_id=1, source_target_pairs={{0,30},{2,0},{4,2},{6,4},{8,6},{10,8},{12,10},{14,12},{16,14},{18,... | collective-permute-start | bytes 393224 | tf_op jit(solution)/shard_map/ppermute | solution.py:53
  48.7 8.5 %collective-permute-start.12 = (bf16[2048,32]{0,1:T(8,128)(2,1)S(1)}, bf16[2048,32]{0,1:T(8,128)(2,1)S(1)}, u32[]{:S(2)}, u32[]{:S(2)}) collective-permute-start(bf16[2048,32]{0,1:T(8,128)(2,1)S(1)} %collective-permute-done.11), channel_id=1, source_target_pairs={{0,2},{2,4},{4,6},{6,8},{8,10},{10,12},{12,14},{14,16},{16,18},{18... | collective-permute-start | bytes 393224 | tf_op jit(solution)/shard_map/ppermute | solution.py:51
  52.8 10.2 %collective-permute-start.6 = (bf16[2048,32]{0,1:T(8,128)(2,1)S(1)}, bf16[2048,32]{0,1:T(8,128)(2,1)S(1)}, u32[]{:S(2)}, u32[]{:S(2)}) collective-permute-start(bf16[2048,32]{0,1:T(8,128)(2,1)S(1)} %collective-permute-done.5), channel_id=1, source_target_pairs={{0,30},{2,0},{4,2},{6,4},{8,6},{10,8},{12,10},{14,12},{16,14},{18,... | collective-permute-start | bytes 393224 | tf_op jit(solution)/shard_map/ppermute | solution.py:53
  57.2 10.0 %collective-permute-start.13 = (bf16[2048,32]{0,1:T(8,128)(2,1)S(1)}, bf16[2048,32]{0,1:T(8,128)(2,1)S(1)}, u32[]{:S(2)}, u32[]{:S(2)}) collective-permute-start(bf16[2048,32]{0,1:T(8,128)(2,1)S(1)} %collective-permute-done.12), channel_id=1, source_target_pairs={{0,2},{2,4},{4,6},{6,8},{8,10},{10,12},{12,14},{14,16},{16,18},{18... | collective-permute-start | bytes 393224 | tf_op jit(solution)/shard_map/ppermute | solution.py:51
  63.0 13.4 %collective-permute-start.7 = (bf16[2048,32]{0,1:T(8,128)(2,1)S(1)}, bf16[2048,32]{0,1:T(8,128)(2,1)S(1)}, u32[]{:S(2)}, u32[]{:S(2)}) collective-permute-start(bf16[2048,32]{0,1:T(8,128)(2,1)S(1)} %collective-permute-done.6), channel_id=1, source_target_pairs={{0,30},{2,0},{4,2},{6,4},{8,6},{10,8},{12,10},{14,12},{16,14},{18,... | collective-permute-start | bytes 393224 | tf_op jit(solution)/shard_map/ppermute | solution.py:53
  67.1 9.2 %collective-permute-start.14 = (bf16[2048,32]{0,1:T(8,128)(2,1)S(1)}, bf16[2048,32]{0,1:T(8,128)(2,1)S(1)}, u32[]{:S(2)}, u32[]{:S(2)}) collective-permute-start(bf16[2048,32]{0,1:T(8,128)(2,1)S(1)} %collective-permute-done.13), channel_id=1, source_target_pairs={{0,2},{2,4},{4,6},{6,8},{8,10},{10,12},{12,14},{14,16},{16,18},{18... | collective-permute-start | bytes 393224 | tf_op jit(solution)/shard_map/ppermute | solution.py:51
  76.3 5.5 %collective-permute-start.15 = (bf16[2048,32]{0,1:T(8,128)(2,1)S(1)}, bf16[2048,32]{0,1:T(8,128)(2,1)S(1)}, u32[]{:S(2)}, u32[]{:S(2)}) collective-permute-start(bf16[2048,32]{0,1:T(8,128)(2,1)S(1)} %collective-permute-done.14), channel_id=1, source_target_pairs={{0,2},{2,4},{4,6},{6,8},{8,10},{10,12},{12,14},{14,16},{16,18},{18... | collective-permute-start | bytes 393224 | tf_op jit(solution)/shard_map/ppermute | solution.py:51
  83.7 1.4 collective-permute-start.16
  85.5 3.4 %copy-start.1 = (bf16[16,1024,2,128]{3,2,1,0:T(2,128)(2,1)S(1)}, bf16[16,1024,2,128]{3,2,1,0:T(2,128)(2,1)}, u32[]{:S(2)}) copy-start(bf16[16,1024,2,128]{3,2,1,0:T(2,128)(2,1)} %param.25) | copy-start | bytes 25165828
  88.9 20.1 %copy-start.4 = (bf16[16,2048]{1,0:T(8,128)(2,1)S(1)}, bf16[16,2048]{1,0:T(8,128)(2,1)}, u32[]{:S(2)}) copy-start(bf16[16,2048]{1,0:T(8,128)(2,1)} %param.17) | copy-start | bytes 196612
  156.2 12.0 %copy-start.6 = (f32[16,4]{0,1:T(4,128)S(1)}, f32[16,4]{0,1:T(4,128)}, u32[]{:S(2)}) copy-start(f32[16,4]{0,1:T(4,128)} %param.33) | copy-start | bytes 772
  162.2 38.0 %all-to-all-start.1 = ((bf16[32,4,2048]{2,1,0:T(4,128)(2,1)}), bf16[32,4,2048]{2,1,0:T(4,128)(2,1)S(1)}, u32[]{:S(2)}, u32[]{:S(2)}) async-start(bf16[32,4,2048]{2,1,0:T(4,128)(2,1)} %reshape.64), calls=%async_computation.1 | async-start | bytes 1048576 | tf_op jit(solution)/shard_map/all_to_all | solution.py:266
Sparse Core Ops, SparseCore 0:
  9.1 78.1 all-gather.1

commit v2 on v1

--- a/solution.py
+++ b/solution.py
@@ -8,8 +8,9 @@
 from jax.sharding import Mesh
 from jax.sharding import PartitionSpec as P
 
-EP = ("ep_0", "ep_1")
-GRP_EP = ("grp", "ep_0", "ep_1")
+EP = ("far", "near", "core")
+NEAR = ("near", "core")
+GRP_EP = ("grp", "far", "near", "core")
 
 
 epsilon = 1e-06
@@ -27,42 +28,31 @@
     )
 
 
-def core_swap(value):
-    return lax.ppermute(value, "ep_1", [(0, 1), (1, 0)])
-
-
-def ring_queries(normed, query_weight):
-    count = normed.shape[0]
-    chips = lax.axis_size("ep_0")
-    cols = query_weight.shape[1]
-    here = lax.axis_index("ep_0")
-    core = lax.axis_index("ep_1")
-    ahead = [(i, (i + 1) % chips) for i in range(chips)]
-    behind = [(i, (i - 1) % chips) for i in range(chips)]
-    both = jnp.concatenate([normed, core_swap(normed)], axis=0)
-
-    def product(block):
-        return jnp.dot(both, block, preferred_element_type=jnp.float32).astype(jnp.bfloat16)
-
-    results = [None] * chips
-    up = down = query_weight
-    results[0] = product(query_weight)
-    for step in range(1, chips // 2 + 1):
-        up = lax.ppermute(up, "ep_0", ahead)
-        if step < chips - step:
-            down = lax.ppermute(down, "ep_0", behind)
-        results[step] = product(up)
-        if step < chips - step:
-            results[chips - step] = product(down)
-    stacked = jnp.stack(results[::-1])
-    twice = jnp.concatenate([stacked, stacked], axis=0)
-    placed = lax.dynamic_slice_in_dim(twice, chips - 1 - here, chips, axis=0)
-    mine = placed[:, :count]
-    theirs = core_swap(placed[:, count:])
-    low = jnp.where(core == 0, mine, theirs)
-    high = jnp.where(core == 0, theirs, mine)
-    full = jnp.stack([low, high], axis=1)
-    return jnp.transpose(full, (2, 0, 1, 3)).reshape(count, chips * 2 * cols)
+def far_blocks(block):
+    size = lax.axis_size("far")
+    out = [block]
+    for d in range(1, size):
+        out.append(lax.ppermute(block, "far", [(i, (i + d) % size) for i in range(size)]))
+    return out
+
+
+def near_product(rows, blocks):
+    members = lax.axis_size(NEAR)
+    size = len(blocks)
+    here = lax.axis_index("far")
+    cols = blocks[0].shape[1]
+    count = rows.shape[0] // members
+    parts = [
+        jnp.dot(rows, block, preferred_element_type=jnp.float32).astype(jnp.bfloat16)
+        for block in blocks
+    ]
+    stacked = jnp.stack(parts[::-1] + parts[::-1])
+    placed = lax.dynamic_slice_in_dim(stacked, size - 1 - here, size, axis=0)
+    outgoing = jnp.transpose(placed.reshape(size, members, count, cols), (1, 2, 0, 3))
+    received = lax.all_to_all(
+        outgoing.reshape(members, count, size * cols), NEAR, 0, 0, tiled=True
+    ).reshape(members, count, size, cols)
+    return jnp.transpose(received, (1, 2, 0, 3)).reshape(count, size * members * cols)
 
 
 def attention_kernel(
@@ -172,7 +162,7 @@
     heads = lambdas.shape[0]
     vmem = pl.BlockSpec(memory_space=pltpu.VMEM)
     smem = pl.BlockSpec(memory_space=pltpu.SMEM)
-    hbm = pl.BlockSpec(memory_space=pl.ANY)
+    hbm = pl.BlockSpec(memory_space=pltpu.HBM)
     rows = ctx_len * kv_count
     out = pl.pallas_call(
         functools.partial(attention_kernel, 2, 128),
@@ -231,17 +221,21 @@
     count = tokens.shape[0]
     width = tokens.shape[1]
     topk = routes.shape[1]
-    out_full = lax.all_gather(out_weight, EP, axis=1, tiled=True)
+    query_blocks = far_blocks(query_weight)
     normed = rms_scaled(tokens, norm_gain).astype(jnp.bfloat16)
     new_keys = jnp.dot(normed, key_weight, preferred_element_type=jnp.float32).astype(jnp.bfloat16)
     new_values = jnp.dot(normed, value_weight, preferred_element_type=jnp.float32).astype(
         jnp.bfloat16
     )
-    queries = ring_queries(normed, query_weight)
+    near_normed = lax.all_gather(normed, NEAR, axis=0, tiled=True)
+    held, *query_blocks = lax.optimization_barrier((out_weight, *query_blocks))
+    out_blocks = far_blocks(held)
+    queries = near_product(near_normed, query_blocks)
     head_out = attention(
         queries, new_keys, new_values, cache_keys, cache_values, lengths, lambdas, head_gain
     )
-    attn_out = jnp.dot(head_out, out_full, preferred_element_type=jnp.float32).astype(jnp.bfloat16)
+    near_heads = lax.all_gather(head_out, NEAR, axis=0, tiled=True)
+    attn_out = near_product(near_heads, out_blocks)
     residual = (tokens.astype(jnp.float32) + attn_out.astype(jnp.float32)).astype(jnp.bfloat16)
     moe_in = rms_scaled(residual, moe_gain).astype(jnp.bfloat16)
     experts = lax.axis_size(EP)
@@ -270,8 +264,8 @@
 
 
 def solution(mesh):
-    chips = mesh.shape["ep"] // 2
-    torus = Mesh(mesh.devices.reshape(mesh.shape["grp"], chips, 2), ("grp", "ep_0", "ep_1"))
+    devices = mesh.devices.reshape(mesh.shape["grp"], -1, 4, 2)
+    torus = Mesh(devices, ("grp", "far", "near", "core"))
     return jax.shard_map(
         local,
         mesh=torus,

time: 212 us -> 214 us (level)
  blocking collectives: 40 us -> 79.4 us
  waiting for transfers between devices: 69.5 us -> 36.4 us
  between operations: 13.9 us -> 0.37 us
  starting transfers between devices: 37.9 us -> 48.5 us
  matrix products: 16.2 us -> 11.9 us
  local copies, waits for them, and re-layouts: 7.49 us -> 9.88 us
    all_gather x0 -> x2, blocking collectives: none -> 37.4 us  [the longest x1 23 us: local(): near_normed = lax.all_gather(normed, NEAR, axis=0, tiled=True)]
    ppermute x17 -> x6, waiting for transfers between devices: 36.8 us -> 0.02 us  [far_blocks(): lax.ppermute(block, 'far', [(i, (i + d) % size) for i in range(size)])]
    all_to_all x0 -> x2, starting transfers between devices: none -> 12.2 us  [near_product(): lax.all_to_all(outgoing.reshape(members, count, size * cols), NEAR, 0, 0,...]
    all_to_all x0 -> x2, waiting for transfers between devices: none -> 4.46 us  [near_product(): lax.all_to_all(outgoing.reshape(members, count, size * cols), NEAR, 0, 0,...]
    dot_general x17 -> x8, matrix products: 6.2 us -> 2.03 us  [near_product(): jnp.dot(rows, block, preferred_element_type=jnp.float32)]
    ppermute x17 -> x6, starting transfers between devices: 31.9 us -> 30.3 us  [far_blocks(): lax.ppermute(block, 'far', [(i, (i + d) % size) for i in range(size)])]
    unnamed x35 -> x29, local copies, waits for them, and re-layouts: 4.43 us -> 4.34 us
  transfers between devices with their start and end apart: 19 -> 9, of which waited for: 12 -> 2; matrix products, arithmetic and copies ran while one was open for 4% -> 3% of each run, Pallas kernels for 10% -> 10%
where the time goes in v2:
time: 214 us; the launch traced here: 211 us
  blocking collectives  79.4 us (37%)
  starting transfers between devices  48.5 us (23%)
  waiting for transfers between devices  36.4 us (17%)
  Pallas kernels  20.4 us (10%)
  matrix products  11.9 us (6%)
  local copies, waits for them, and re-layouts  9.88 us (5%)
  other arithmetic  4.21 us (2%)
    all_to_all x1, blocking collectives, local(): lax.all_to_all(outgoing, EP, split_axis=0, concat_axis=0, tiled=True)  42 us
    all_to_all x1, waiting for transfers between devices, local(): lax.all_to_all(results, EP, split_axis=0, concat_axis=0, tiled=True)  31.9 us
    ppermute x6, starting transfers between devices, far_blocks(): lax.ppermute(block, 'far', [(i, (i + d) % size) for i in range(size)])  30.3 us
    all_gather x1, blocking collectives, local(): near_normed = lax.all_gather(normed, NEAR, axis=0, tiled=True)  23 us
    pallas_call x1, Pallas kernels, attention(): pl.pallas_call(functools.partial(attention_kernel, 2, 128), out_shape=jax...  20.4 us
    all_gather x1, blocking collectives, local(): near_heads = lax.all_gather(head_out, NEAR, axis=0, tiled=True)  14.3 us
    all_to_all x2, starting transfers between devices, near_product(): lax.all_to_all(outgoing.reshape(members, count, size * cols), NEAR, 0, 0,...  12.2 us
    all_to_all x1, starting transfers between devices, local(): lax.all_to_all(results, EP, split_axis=0, concat_axis=0, tiled=True)  5.94 us
  transfers between devices with their start and end apart: 9, of which 2 were waited for; matrix products, arithmetic and copies ran while one was open for 3% of the time, Pallas kernels for 10%

profile of v2, /device:TPU:196, one launch (start us, length us, event | category | flops | bytes accessed | tf_op | source)
XLA Modules:
  0.0 211.0 jit_solution(2031010827690818135)
XLA Ops:
  0.0 8.1 %collective-permute-start = (bf16[2048,32]{0,1:T(8,128)(2,1)}, bf16[2048,32]{0,1:T(8,128)(2,1)S(1)}, u32[]{:S(2)}, u32[]{:S(2)}) collective-permute-start(bf16[2048,32]{0,1:T(8,128)(2,1)} %param.19), channel_id=1, source_target_pairs={{0,8},{8,16},{16,24},{24,0},{1,9},{9,17},{17,25},{25,1},{2,10},{10... | collective-permute-start | bytes 393224 | tf_op jit(solution)/shard_map/ppermute | solution.py:35
  8.1 9.7 %collective-permute-start.1 = (bf16[2048,32]{0,1:T(8,128)(2,1)}, bf16[2048,32]{0,1:T(8,128)(2,1)S(1)}, u32[]{:S(2)}, u32[]{:S(2)}) collective-permute-start(bf16[2048,32]{0,1:T(8,128)(2,1)} %param.19), channel_id=1, source_target_pairs={{0,16},{8,24},{16,0},{24,8},{1,17},{9,25},{17,1},{25,9},{2,18},{10... | collective-permute-start | bytes 393224 | tf_op jit(solution)/shard_map/ppermute | solution.py:35
  17.9 2.7 %collective-permute-start.2 = (bf16[2048,32]{0,1:T(8,128)(2,1)}, bf16[2048,32]{0,1:T(8,128)(2,1)S(1)}, u32[]{:S(2)}, u32[]{:S(2)}) collective-permute-start(bf16[2048,32]{0,1:T(8,128)(2,1)} %param.19), channel_id=1, source_target_pairs={{0,24},{8,0},{16,8},{24,16},{1,25},{9,1},{17,9},{25,17},{2,26},{10... | collective-permute-start | bytes 393224 | tf_op jit(solution)/shard_map/ppermute | solution.py:35
  20.6 0.7 convert_element_type.85
  21.3 1.0 fusion.46
  22.3 0.9 fusion.48
  23.2 0.3 convolution_convert_fusion.6
  23.5 1.5 convolution_convert_fusion.5
  25.0 0.8 copy.43
  26.0 23.0 %all_gather.6 = bf16[128,2048]{1,0:T(8,128)(2,1)S(1)} all-gather(bf16[16,2048]{1,0:T(8,128)(2,1)S(1)} %fusion.48), channel_id=1, replica_groups=mesh['grp'=4,'far'=4,'near'=4,'core'=2] {'near','core'}, dimensions={0}, use_global_device_ids=true | all-gather | bytes 589824 | tf_op jit(solution)/shard_map/all_gather | solution.py:230
  49.0 0.3 constant_dynamic-update-slice_fusion.7
  49.3 0.3 constant_dynamic-update-slice_fusion.6
  49.6 0.3 constant_dynamic-update-slice_fusion.5
  49.9 0.3 constant_dynamic-update-slice_fusion.4
  50.3 0.1 copy.36
  50.5 0.7 reshape.77
  51.3 7.1 %all-to-all-start = ((bf16[8,16,128]{2,1,0:T(8,128)(2,1)}), bf16[8,16,128]{2,1,0:T(8,128)(2,1)S(1)}, u32[]{:S(2)}, u32[]{:S(2)}) async-start(bf16[8,16,128]{2,1,0:T(8,128)(2,1)} %reshape.77), calls=%async_computation | async-start | bytes 65536 | tf_op jit(solution)/shard_map/all_to_all | solution.py:52
  58.3 4.3 %collective-permute-start.3 = (bf16[1024,64]{0,1:T(8,128)(2,1)S(1)}, bf16[1024,64]{0,1:T(8,128)(2,1)S(1)}, u32[]{:S(2)}, u32[]{:S(2)}) collective-permute-start(bf16[1024,64]{0,1:T(8,128)(2,1)S(1)} %copy-done.5), channel_id=1, source_target_pairs={{0,24},{8,0},{16,8},{24,16},{1,25},{9,1},{17,9},{25,17},{2,26},{10... | collective-permute-start | bytes 393224 | tf_op jit(solution)/shard_map/ppermute | solution.py:35
  62.6 0.2 select_reduce_fusion
  62.9 1.0 collective-permute-start.4
  64.0 4.4 %collective-permute-start.5 = (bf16[1024,64]{0,1:T(8,128)(2,1)S(1)}, bf16[1024,64]{0,1:T(8,128)(2,1)S(1)}, u32[]{:S(2)}, u32[]{:S(2)}) collective-permute-start(bf16[1024,64]{0,1:T(8,128)(2,1)S(1)} %copy-done.5), channel_id=1, source_target_pairs={{0,8},{8,16},{16,24},{24,0},{1,9},{9,17},{17,25},{25,1},{2,10},{10... | collective-permute-start | bytes 393224 | tf_op jit(solution)/shard_map/ppermute | solution.py:35
  68.6 0.1 reshape_reshape.3.q_ref
  68.8 3.4 %copy-done.1 = bf16[16,1024,2,128]{3,2,1,0:T(2,128)(2,1)S(1)} copy-done((bf16[16,1024,2,128]{3,2,1,0:T(2,128)(2,1)S(1)}, bf16[16,1024,2,128]{3,2,1,0:T(2,128)(2,1)}, u32[]{:S(2)}) %copy-start.1) | copy-done | bytes 8388632
  72.2 20.4 %attention.1 = bf16[16,8,128]{2,1,0:T(8,128)(2,1)S(1)} custom-call(s32[16]{0:T(128)S(1)} %copy-done.2, bf16[16,8,128]{2,1,0:T(8,128)(2,1)S(1)} %reshape_reshape.3.q_ref, bf16[16,2,128]{2,1,0:T(2,128)(2,1)S(1)} %reshape.79.nk_ref, bf16[16,2,128]{2,1,0:T(2,128)(2,1)S(1)} %reshape.80.nv_ref, f32[8,128]{1,0:T(8,128)S(1)} %broadcast_in_dim.4.lam_ref, ...), custom_call_target="tpu_custom_call" | custom-call | tf_op jit(solution)/shard_map/attention/pallas_call | solution.py:167
  92.6 14.3 %all_gather.7 = bf16[128,1024]{1,0:T(8,128)(2,1)S(1)} all-gather(bf16[16,1024]{1,0:T(8,128)(2,1)S(1)} %bitcast.91), channel_id=1, replica_groups=mesh['grp'=4,'far'=4,'near'=4,'core'=2] {'near','core'}, dimensions={0}, use_global_device_ids=true | all-gather | bytes 294912 | tf_op jit(solution)/shard_map/all_gather | solution.py:237
  106.9 0.2 constant_dynamic-update-slice_fusion.15
  107.2 0.2 constant_dynamic-update-slice_fusion.14
  107.4 0.2 constant_dynamic-update-slice_fusion.13
  107.6 0.2 constant_dynamic-update-slice_fusion.12
  107.9 0.1 copy.39
  108.2 0.8 reshape.86
  108.9 5.2 %all-to-all-start.1 = ((bf16[8,16,256]{2,1,0:T(8,128)(2,1)}), bf16[8,16,256]{2,1,0:T(8,128)(2,1)S(1)}, u32[]{:S(2)}, u32[]{:S(2)}) async-start(bf16[8,16,256]{2,1,0:T(8,128)(2,1)} %reshape.86), calls=%async_computation.1 | async-start | bytes 131072 | tf_op jit(solution)/shard_map/all_to_all | solution.py:52
  114.3 4.5 %all-to-all-done.1 = bf16[8,16,256]{2,1,0:T(8,128)(2,1)S(1)} async-done(((bf16[8,16,256]{2,1,0:T(8,128)(2,1)}), bf16[8,16,256]{2,1,0:T(8,128)(2,1)S(1)}, u32[]{:S(2)}, u32[]{:S(2)}) %all-to-all-start.1) | async-done | bytes 65568 | tf_op jit(solution)/shard_map/all_to_all | solution.py:52
  118.7 0.2 reshape.93
  118.9 0.2 copy.41
  119.2 0.1 fusion.50
  119.3 0.4 convolution_convert_fusion
  119.7 0.2 reshape.88
  119.9 42.0 %all_to_all.20 = bf16[32,4,2048]{2,1,0:T(4,128)(2,1)S(1)} all-to-all(bf16[32,4,2048]{2,1,0:T(4,128)(2,1)S(1)} %reshape.88), channel_id=1, replica_groups=mesh['grp'=4,'far'=4,'near'=4,'core'=2] {'far','near','core'}, dimensions={0} | all-to-all | bytes 1048576 | tf_op jit(solution)/shard_map/all_to_all | solution.py:255
  162.1 2.9 %fusion.12 = f32[128,1024]{1,0:T(8,128)S(1)} fusion(bf16[128,2048]{1,0:T(8,128)(2,1)S(1)} %reshape.89, bf16[1,2048,1024]{2,1,0:T(8,128)(2,1)} %param.29), kind=kOutput, calls=%fused_computation.10 | convolution fusion | flops 537001984 | bytes 5242880 | tf_op jit(solution)/shard_map/dot_general | solution.py:194
  165.0 4.9 %fusion.6 = bf16[128,2048]{1,0:T(8,128)(2,1)S(1)} fusion(bf16[1,1024,2048]{2,1,0:T(8,128)(2,1)} %param.31, f32[128,1024]{1,0:T(8,128)S(1)} %fusion.12, bf16[128,2048]{1,0:T(8,128)(2,1)S(1)} %reshape.89, bf16[1,2048,1024]{2,1,0:T(8,128)(2,1)} %param.30), kind=kOutput, calls=%fused_computation.7 | convolution fusion | flops 1075183616 | bytes 9961472 | tf_op jit(solution)/shard_map/dot_general | solution.py:199
  169.9 1.0 reshape.90
  170.9 5.9 %all-to-all-start.3 = ((bf16[32,4,2048]{2,1,0:T(4,128)(2,1)}), bf16[32,4,2048]{2,1,0:T(4,128)(2,1)S(1)}, u32[]{:S(2)}, u32[]{:S(2)}) async-start(bf16[32,4,2048]{2,1,0:T(4,128)(2,1)} %reshape.90), calls=%async_computation.3 | async-start | bytes 1048576 | tf_op jit(solution)/shard_map/all_to_all | solution.py:260
  177.0 31.9 %all-to-all-done.3 = bf16[32,4,2048]{2,1,0:T(4,128)(2,1)S(1)} async-done(((bf16[32,4,2048]{2,1,0:T(4,128)(2,1)}), bf16[32,4,2048]{2,1,0:T(4,128)(2,1)S(1)}, u32[]{:S(2)}, u32[]{:S(2)}) %all-to-all-start.3) | async-done | bytes 524320 | tf_op jit(solution)/shard_map/all_to_all | solution.py:260
  209.0 0.7 gather_fusion
  209.8 0.2 reshape.104
  209.9 0.4 multiply_reduce_fusion
  210.3 0.7 fusion.53
  (60 shorter events, 1.7 us)
Async XLA Ops:
  0.0 23.2 %copy-start = (bf16[2048,256]{1,0:T(8,128)(2,1)S(1)}, bf16[2048,256]{1,0:T(8,128)(2,1)}, u32[]{:S(2)}) copy-start(bf16[2048,256]{1,0:T(8,128)(2,1)} %param.20) | copy-start | bytes 3145732
  0.0 49.9 %copy-start.6 = (bf16[2048,32]{0,1:T(8,128)(2,1)S(1)}, bf16[2048,32]{0,1:T(8,128)(2,1)}, u32[]{:S(2)}) copy-start(bf16[2048,32]{0,1:T(8,128)(2,1)} %param.19) | copy-start | bytes 393220
  0.0 58.3 %copy-start.5 = (bf16[1024,64]{0,1:T(8,128)(2,1)S(1)}, bf16[1024,64]{0,1:T(8,128)(2,1)}, u32[]{:S(2)}) copy-start(bf16[1024,64]{0,1:T(8,128)(2,1)} %param.22) | copy-start | bytes 393220
  0.0 68.7 %copy-start.9 = (f32[8]{0:T(128)S(1)}, f32[8]{0:T(128)}, u32[]{:S(2)}) copy-start(f32[8]{0:T(128)} %param.24) | copy-start | bytes 100
  0.0 68.8 %copy-start.3 = (bf16[128]{0:T(256)(128)(2,1)S(1)}, bf16[128]{0:T(256)(128)(2,1)}, u32[]{:S(2)}) copy-start(bf16[128]{0:T(256)(128)(2,1)} %param.23) | copy-start | bytes 772
  0.0 68.8 %copy-start.2 = (s32[16]{0:T(128)S(1)}, s32[16]{0:T(128)}, u32[]{:S(2)}) copy-start(s32[16]{0:T(128)} %lens_ref.1) | copy-start | bytes 196
  0.0 49.0 %collective-permute-start = (bf16[2048,32]{0,1:T(8,128)(2,1)}, bf16[2048,32]{0,1:T(8,128)(2,1)S(1)}, u32[]{:S(2)}, u32[]{:S(2)}) collective-permute-start(bf16[2048,32]{0,1:T(8,128)(2,1)} %param.19), channel_id=1, source_target_pairs={{0,8},{8,16},{16,24},{24,0},{1,9},{9,17},{17,25},{25,1},{2,10},{10... | collective-permute-start | bytes 393224 | tf_op jit(solution)/shard_map/ppermute | solution.py:35
  8.1 40.9 %collective-permute-start.1 = (bf16[2048,32]{0,1:T(8,128)(2,1)}, bf16[2048,32]{0,1:T(8,128)(2,1)S(1)}, u32[]{:S(2)}, u32[]{:S(2)}) collective-permute-start(bf16[2048,32]{0,1:T(8,128)(2,1)} %param.19), channel_id=1, source_target_pairs={{0,16},{8,24},{16,0},{24,8},{1,17},{9,25},{17,1},{25,9},{2,18},{10... | collective-permute-start | bytes 393224 | tf_op jit(solution)/shard_map/ppermute | solution.py:35
  17.9 31.2 %collective-permute-start.2 = (bf16[2048,32]{0,1:T(8,128)(2,1)}, bf16[2048,32]{0,1:T(8,128)(2,1)S(1)}, u32[]{:S(2)}, u32[]{:S(2)}) collective-permute-start(bf16[2048,32]{0,1:T(8,128)(2,1)} %param.19), channel_id=1, source_target_pairs={{0,24},{8,0},{16,8},{24,16},{1,25},{9,1},{17,9},{25,17},{2,26},{10... | collective-permute-start | bytes 393224 | tf_op jit(solution)/shard_map/ppermute | solution.py:35
  51.3 17.1 %all-to-all-start = ((bf16[8,16,128]{2,1,0:T(8,128)(2,1)}), bf16[8,16,128]{2,1,0:T(8,128)(2,1)S(1)}, u32[]{:S(2)}, u32[]{:S(2)}) async-start(bf16[8,16,128]{2,1,0:T(8,128)(2,1)} %reshape.77), calls=%async_computation | async-start | bytes 65536 | tf_op jit(solution)/shard_map/all_to_all | solution.py:52
  58.3 48.6 %collective-permute-start.3 = (bf16[1024,64]{0,1:T(8,128)(2,1)S(1)}, bf16[1024,64]{0,1:T(8,128)(2,1)S(1)}, u32[]{:S(2)}, u32[]{:S(2)}) collective-permute-start(bf16[1024,64]{0,1:T(8,128)(2,1)S(1)} %copy-done.5), channel_id=1, source_target_pairs={{0,24},{8,0},{16,8},{24,16},{1,25},{9,1},{17,9},{25,17},{2,26},{10... | collective-permute-start | bytes 393224 | tf_op jit(solution)/shard_map/ppermute | solution.py:35
  62.9 44.2 %collective-permute-start.4 = (bf16[1024,64]{0,1:T(8,128)(2,1)S(1)}, bf16[1024,64]{0,1:T(8,128)(2,1)S(1)}, u32[]{:S(2)}, u32[]{:S(2)}) collective-permute-start(bf16[1024,64]{0,1:T(8,128)(2,1)S(1)} %copy-done.5), channel_id=1, source_target_pairs={{0,16},{8,24},{16,0},{24,8},{1,17},{9,25},{17,1},{25,9},{2,18},{10... | collective-permute-start | bytes 393224 | tf_op jit(solution)/shard_map/ppermute | solution.py:35
  64.0 43.4 %collective-permute-start.5 = (bf16[1024,64]{0,1:T(8,128)(2,1)S(1)}, bf16[1024,64]{0,1:T(8,128)(2,1)S(1)}, u32[]{:S(2)}, u32[]{:S(2)}) collective-permute-start(bf16[1024,64]{0,1:T(8,128)(2,1)S(1)} %copy-done.5), channel_id=1, source_target_pairs={{0,8},{8,16},{16,24},{24,0},{1,9},{9,17},{17,25},{25,1},{2,10},{10... | collective-permute-start | bytes 393224 | tf_op jit(solution)/shard_map/ppermute | solution.py:35
  68.8 3.4 %copy-start.1 = (bf16[16,1024,2,128]{3,2,1,0:T(2,128)(2,1)S(1)}, bf16[16,1024,2,128]{3,2,1,0:T(2,128)(2,1)}, u32[]{:S(2)}) copy-start(bf16[16,1024,2,128]{3,2,1,0:T(2,128)(2,1)} %param.25) | copy-start | bytes 25165828
  72.2 42.0 %copy-start.7 = (bf16[2048]{0:T(1024)(128)(2,1)S(1)}, bf16[2048]{0:T(1024)(128)(2,1)}, u32[]{:S(2)}) copy-start(bf16[2048]{0:T(1024)(128)(2,1)} %param.28) | copy-start | bytes 12292
  92.6 26.6 %copy-start.4 = (bf16[16,2048]{1,0:T(8,128)(2,1)S(1)}, bf16[16,2048]{1,0:T(8,128)(2,1)}, u32[]{:S(2)}) copy-start(bf16[16,2048]{1,0:T(8,128)(2,1)} %param.17) | copy-start | bytes 196612
  108.9 9.8 %all-to-all-start.1 = ((bf16[8,16,256]{2,1,0:T(8,128)(2,1)}), bf16[8,16,256]{2,1,0:T(8,128)(2,1)S(1)}, u32[]{:S(2)}, u32[]{:S(2)}) async-start(bf16[8,16,256]{2,1,0:T(8,128)(2,1)} %reshape.86), calls=%async_computation.1 | async-start | bytes 131072 | tf_op jit(solution)/shard_map/all_to_all | solution.py:52
  165.0 11.9 %copy-start.8 = (f32[16,4]{0,1:T(4,128)S(1)}, f32[16,4]{0,1:T(4,128)}, u32[]{:S(2)}) copy-start(f32[16,4]{0,1:T(4,128)} %param.33) | copy-start | bytes 772
  170.9 38.0 %all-to-all-start.3 = ((bf16[32,4,2048]{2,1,0:T(4,128)(2,1)}), bf16[32,4,2048]{2,1,0:T(4,128)(2,1)S(1)}, u32[]{:S(2)}, u32[]{:S(2)}) async-start(bf16[32,4,2048]{2,1,0:T(4,128)(2,1)} %reshape.90), calls=%async_computation.3 | async-start | bytes 1048576 | tf_op jit(solution)/shard_map/all_to_all | solution.py:260

commit v3 on v2

v3 whole, which is shorter than its diff:
```python
import functools

import jax
import jax.numpy as jnp
from jax import lax
from jax.experimental import pallas as pl
from jax.experimental.pallas import tpu as pltpu
from jax.sharding import Mesh
from jax.sharding import PartitionSpec as P

EP = ("far", "near", "core")
NEAR = ("near", "core")
CHIPS = ("far", "near")
GRP_EP = ("grp", "far", "near", "core")


epsilon = 1e-06
masked_score = -1e30
clamp_limit = 7.0
swish_alpha = 1.702


def rms_scaled(values, gain):
    floats = values.astype(jnp.float32)
    return (
        floats
        * lax.rsqrt(jnp.mean(floats * floats, axis=-1, keepdims=True) + epsilon)
        * gain.astype(jnp.float32)
    )


def far_blocks(block):
    size = lax.axis_size("far")
    out = [block]
    for d in range(1, size):
        out.append(lax.ppermute(block, "far", [(i, (i + d) % size) for i in range(size)]))
    return out


def near_product(rows, blocks):
    members = lax.axis_size(NEAR)
    size = len(blocks)
    here = lax.axis_index("far")
    cols = blocks[0].shape[1]
    count = rows.shape[0] // members
    parts = [
        jnp.dot(rows, block, preferred_element_type=jnp.float32).astype(jnp.bfloat16)
        for block in blocks
    ]
    stacked = jnp.stack(parts[::-1] + parts[::-1])
    placed = lax.dynamic_slice_in_dim(stacked, size - 1 - here, size, axis=0)
    outgoing = jnp.transpose(placed.reshape(size, members, count, cols), (1, 2, 0, 3))
    received = lax.all_to_all(
        outgoing.reshape(members, count, size * cols), NEAR, 0, 0, tiled=True
    ).reshape(members, count, size, cols)
    return jnp.transpose(received, (1, 2, 0, 3)).reshape(count, size * members * cols)


def attention_kernel(
    group_size, chunk, lens_ref, q_ref, nk_ref, nv_ref, lam_ref, gain_ref, k_hbm, v_hbm, o_ref, k_buf, v_buf, s_buf, k_sem, v_sem
):
    count, heads, width = q_ref.shape
    kv_count = nk_ref.shape[1]
    group = heads // kv_count
    half = width // 2
    rows = k_buf.shape[1]
    chunk_rows = chunk * kv_count
    chunks = rows // chunk_rows
    inv_scale = half ** (-0.5)

    def piece(s, c):
        return pl.ds(pl.multiple_of(c * chunk_rows, chunk_rows), chunk_rows)

    def copies(s, where):
        return (
            pltpu.make_async_copy(k_hbm.at[s, where], k_buf.at[s, where], k_sem.at[s]),
            pltpu.make_async_copy(v_hbm.at[s, where], v_buf.at[s, where], v_sem.at[s]),
        )

    def used(s):
        return (lens_ref[s] + chunk - 1) // chunk

    def fetch(s, _):
        n = used(s)
        for c in range(chunks):
            where = pl.ds(c * chunk_rows, chunk_rows)

            @pl.when(c < n)
            def _():
                for copy in copies(s, where):
                    copy.start()

            @pl.when(c >= n)
            def _():
                v_buf[s, where] = jnp.zeros((chunk_rows, width), v_buf.dtype)

        return 0

    lax.fori_loop(0, count, fetch, 0)

    lane = lax.broadcasted_iota(jnp.int32, (heads, width), 1)
    head_row = lax.broadcasted_iota(jnp.int32, (heads, width), 0)
    column = lax.broadcasted_iota(jnp.int32, (1, heads, rows), 2)
    score_head = lax.broadcasted_iota(jnp.int32, (1, heads, rows), 1)
    own_kv = (column % kv_count) == score_head // group
    position = jnp.where(own_kv, column // kv_count, rows)[None]
    gain = gain_ref[...].astype(jnp.float32)
    lam = lam_ref[...][None, :, :1]
    low = (lane < half)[None]
    block = lax.broadcasted_iota(jnp.int32, (group_size, 1, heads, 1), 0)

    def spread(values):
        out = jnp.broadcast_to(values[:, kv_count - 1 :], (group_size, heads, width))
        for k in range(kv_count - 1):
            out = jnp.where((head_row // group == k)[None], values[:, k : k + 1], out)
        return out

    def step(g, _):
        first = g * group_size
        here = pl.ds(first, group_size)
        q = q_ref[here]
        zero = jnp.zeros_like(q)
        split = jnp.stack([jnp.where(low, q, zero), jnp.where(low, zero, q)], axis=1)
        own_key = spread(nk_ref[here].astype(jnp.float32))
        own_val = spread(nv_ref[here].astype(jnp.float32))
        own_score = (
            jnp.sum(split.astype(jnp.float32) * own_key[:, None], axis=3, keepdims=True) * inv_scale
        )
        limit = jnp.zeros((group_size, 1, heads, 1), jnp.int32)
        for i in range(group_size):
            s = first + i
            limit = jnp.where(block == i, lens_ref[s], limit)

            def wait(c, _):
                for copy in copies(s, piece(s, c)):
                    copy.wait()
                return 0

            lax.fori_loop(0, used(s), wait, 0)
        for i in range(group_size):
            s_buf[i] = lax.dot_general(
                split[i].reshape(2 * heads, width), k_buf[first + i], (((1,), (1,)), ((), ())), preferred_element_type=jnp.float32
            ).reshape(2, heads, rows)
        scores = jnp.where(position < limit, s_buf[...] * inv_scale, masked_score)
        highest = jnp.maximum(jnp.max(scores, axis=3, keepdims=True), own_score)
        expd = jnp.exp(scores - highest)
        own_exp = jnp.exp(own_score - highest)
        inverse = 1.0 / (jnp.sum(expd, axis=3, keepdims=True) + own_exp)
        plus = inverse[:, 0]
        minus = inverse[:, 1] * lam
        weights = (expd[:, 0] * plus - expd[:, 1] * minus).astype(jnp.bfloat16)
        own_weight = (own_exp[:, 0] * plus - own_exp[:, 1] * minus).astype(jnp.bfloat16)
        attended = jnp.stack(
            [
                jnp.dot(weights[i], v_buf[first + i], preferred_element_type=jnp.float32)
                for i in range(group_size)
            ]
        )
        attended = attended + own_weight.astype(jnp.float32) * own_val
        scale = lax.rsqrt(jnp.mean(attended * attended, axis=2, keepdims=True) + epsilon)
        o_ref[here] = (attended * scale * gain[None]).astype(o_ref.dtype)
        return 0

    lax.fori_loop(0, count // group_size, step, 0)


def attention(queries, new_keys, new_values, cache_keys, cache_values, lengths, lambdas, head_gain):
    count, ctx_len, kv_count, width = cache_keys.shape
    heads = lambdas.shape[0]
    vmem = pl.BlockSpec(memory_space=pltpu.VMEM)
    smem = pl.BlockSpec(memory_space=pltpu.SMEM)
    hbm = pl.BlockSpec(memory_space=pltpu.HBM)
    rows = ctx_len * kv_count
    together = 8
    out = pl.pallas_call(
        functools.partial(attention_kernel, together, 128),
        out_shape=jax.ShapeDtypeStruct((count, heads, width), jnp.bfloat16),
        in_specs=[smem, vmem, vmem, vmem, vmem, vmem, hbm, hbm],
        out_specs=vmem,
        scratch_shapes=[
            pltpu.VMEM((count, rows, width), jnp.bfloat16),
            pltpu.VMEM((count, rows, width), jnp.bfloat16),
            pltpu.VMEM((together, 2, heads, rows), jnp.float32),
            pltpu.SemaphoreType.DMA((count,)),
            pltpu.SemaphoreType.DMA((count,)),
        ],
        compiler_params=pltpu.CompilerParams(vmem_limit_bytes=60 * 2**20),
        name="attention",
    )(
        lengths,
        queries.reshape(count, heads, width),
        new_keys.reshape(count, kv_count, width),
        new_values.reshape(count, kv_count, width),
        jnp.broadcast_to(lambdas[:, None], (heads, width)),
        head_gain.reshape(1, width),
        cache_keys.reshape(count, rows, width),
        cache_values.reshape(count, rows, width),
    )
    return out.reshape(count, heads * width)


def expert_kernel(
    core_ref, h_ref, own_ref, tok_ref, gain_ref, near_hbm, other_hbm, gate_hbm, up_hbm, down_hbm,
    o_ref, res_ref, wo_buf, x_buf, gate_buf, up_buf, down_buf, wo_sem, x_sem, gate_sem, up_sem, down_sem,
):
    core = core_ref[0]
    cols = wo_buf.shape[1] // 2
    depth = wo_buf.shape[2]
    count = own_ref.shape[0]
    slots = h_ref.shape[0]
    members = x_buf.shape[1] * 2
    halves = x_buf.shape[0]
    pieces = down_sem.shape[0]
    width = o_ref.shape[1]
    step = width // pieces

    wo_copies = []
    x_copies = []
    for i, source in enumerate((near_hbm, other_hbm)):
        side = core if i == 0 else 1 - core
        at = pl.ds(pl.multiple_of(side * cols, cols), cols)
        wo_copies.append(
            pltpu.make_async_copy(source.at[:, pl.ds(0, cols)], wo_buf.at[:, at], wo_sem.at[i])
        )
        at = pl.ds(pl.multiple_of(side * count, count), count)
        for half in range(halves):
            rows = pl.ds(cols + half * count, count)
            x_copies.append(
                pltpu.make_async_copy(
                    source.at[:, rows], x_buf.at[half, :, at], x_sem.at[i * halves + half]
                )
            )
    gate_copy = pltpu.make_async_copy(gate_hbm.at[0], gate_buf, gate_sem)
    up_copy = pltpu.make_async_copy(up_hbm.at[0], up_buf, up_sem)
    down_copies = [
        pltpu.make_async_copy(
            down_hbm.at[0, :, pl.ds(i * step, step)], down_buf.at[:, pl.ds(i * step, step)], down_sem.at[i]
        )
        for i in range(pieces)
    ]
    for copy in (*wo_copies, *x_copies, gate_copy, up_copy, *down_copies):
        copy.start()

    heads = jnp.concatenate([h_ref[:, :depth], own_ref[...]], axis=0)
    chosen = h_ref[:, depth:]
    lanes = chosen.shape[1]
    per = slots // members
    token = lax.broadcasted_iota(jnp.int32, (lanes, members * count), 0)
    column = lax.broadcasted_iota(jnp.int32, (lanes, members * count), 1)
    repeat = jnp.where(column % count == token, 1.0, 0.0).astype(jnp.bfloat16)
    spread = jnp.dot(chosen, repeat, preferred_element_type=jnp.float32)
    slot = lax.broadcasted_iota(jnp.int32, (slots, members * count), 0)
    column = lax.broadcasted_iota(jnp.int32, (slots, members * count), 1)
    select = jnp.where(slot // per == column // count, spread, 0.0).astype(jnp.bfloat16)

    for copy in wo_copies:
        copy.wait()
    attn = lax.dot_general(
        heads,
        wo_buf[...].reshape(width, depth),
        (((1,), (1,)), ((), ())),
        preferred_element_type=jnp.float32,
    ).astype(jnp.bfloat16)
    res_ref[...] = (
        tok_ref[...].astype(jnp.float32) + attn[slots:].astype(jnp.float32)
    ).astype(res_ref.dtype)
    for copy in x_copies:
        copy.wait()
    rows = jnp.concatenate(
        [
            jnp.dot(
                select,
                x_buf[half].reshape(members * count, depth),
                preferred_element_type=jnp.float32,
            )
            for half in range(halves)
        ],
        axis=1,
    )
    residual = (rows + attn[:slots].astype(jnp.float32)).astype(jnp.bfloat16)
    inputs = rms_scaled(residual, gain_ref[...]).astype(jnp.bfloat16)
    gate_copy.wait()
    gate = jnp.dot(inputs, gate_buf[...], preferred_element_type=jnp.float32)
    gate = jnp.minimum(gate, clamp_limit)
    swish = gate * (1.0 / (1.0 + jnp.exp(-swish_alpha * gate)))
    up_copy.wait()
    upper = jnp.dot(inputs, up_buf[...], preferred_element_type=jnp.float32)
    upper = jnp.clip(upper, -clamp_limit, clamp_limit)
    act = ((upper + 1.0) * swish).astype(jnp.bfloat16)
    for i, copy in enumerate(down_copies):
        copy.wait()
        at = pl.ds(i * step, step)
        o_ref[:, at] = jnp.dot(act, down_buf[:, at], preferred_element_type=jnp.float32).astype(
            o_ref.dtype
        )


def expert(core, received, head_out, tokens, moe_gain, near, other, gate_w, up_w, down_w):
    slots = received.shape[0]
    count, width = tokens.shape
    chips, packed, depth = near.shape
    halves = width // depth
    cols = packed - halves * count
    hidden = gate_w.shape[2]
    pieces = 4
    vmem = pl.BlockSpec(memory_space=pltpu.VMEM)
    smem = pl.BlockSpec(memory_space=pltpu.SMEM)
    hbm = pl.BlockSpec(memory_space=pltpu.HBM)
    bf16 = jnp.bfloat16
    return pl.pallas_call(
        expert_kernel,
        out_shape=(
            jax.ShapeDtypeStruct((slots, width), bf16),
            jax.ShapeDtypeStruct((count, width), bf16),
        ),
        in_specs=[smem, vmem, vmem, vmem, vmem, hbm, hbm, hbm, hbm, hbm],
        out_specs=(vmem, vmem),
        scratch_shapes=[
            pltpu.VMEM((chips, 2 * cols, depth), bf16),
            pltpu.VMEM((halves, chips, 2 * count, depth), bf16),
            pltpu.VMEM((width, hidden), bf16),
            pltpu.VMEM((width, hidden), bf16),
            pltpu.VMEM((hidden, width), bf16),
            pltpu.SemaphoreType.DMA((2,)),
            pltpu.SemaphoreType.DMA((2 * halves,)),
            pltpu.SemaphoreType.DMA,
            pltpu.SemaphoreType.DMA,
            pltpu.SemaphoreType.DMA((pieces,)),
        ],
        compiler_params=pltpu.CompilerParams(vmem_limit_bytes=60 * 2**20),
        name="expert",
    )(core, received, head_out, tokens, moe_gain.reshape(1, width), near, other, gate_w, up_w, down_w)


def combine_kernel(share_ref, rows_ref, res_ref, o_ref):
    share = share_ref[...]
    high = share.astype(jnp.bfloat16)
    low = (share - high.astype(jnp.float32)).astype(jnp.bfloat16)
    rows = rows_ref[...]
    total = jnp.dot(high, rows, preferred_element_type=jnp.float32) + jnp.dot(
        low, rows, preferred_element_type=jnp.float32
    )
    o_ref[...] = (res_ref[...].astype(jnp.float32) + total).astype(o_ref.dtype)


def combine(share, rows, residual):
    vmem = pl.BlockSpec(memory_space=pltpu.VMEM)
    return pl.pallas_call(
        combine_kernel,
        out_shape=jax.ShapeDtypeStruct(residual.shape, jnp.bfloat16),
        in_specs=[vmem] * 3,
        out_specs=vmem,
        name="combine",
    )(share, rows, residual)


def local(
    tokens,
    norm_gain,
    query_weight,
    key_weight,
    value_weight,
    out_weight,
    head_gain,
    lambdas,
    cache_keys,
    cache_values,
    lengths,
    moe_gain,
    gate_weight,
    up_weight,
    down_weight,
    routes,
    route_weights,
):
    count = tokens.shape[0]
    topk = routes.shape[1]
    depth = out_weight.shape[0]
    packed = jnp.concatenate([out_weight.T, tokens[:, :depth], tokens[:, depth:]], axis=0)
    near_packed = lax.all_gather(packed, CHIPS, axis=0)
    query_blocks = far_blocks(query_weight)
    normed = rms_scaled(tokens, norm_gain).astype(jnp.bfloat16)
    new_keys = jnp.dot(normed, key_weight, preferred_element_type=jnp.float32).astype(jnp.bfloat16)
    new_values = jnp.dot(normed, value_weight, preferred_element_type=jnp.float32).astype(
        jnp.bfloat16
    )
    near_normed = lax.all_gather(normed, NEAR, axis=0, tiled=True)
    queries = near_product(near_normed, query_blocks)
    head_out = attention(
        queries, new_keys, new_values, cache_keys, cache_values, lengths, lambdas, head_gain
    )
    experts = lax.axis_size(EP)
    capacity = min(count, max(2, 2 * count * topk // experts))
    onehot = (routes.reshape(-1)[:, None] == jnp.arange(experts, dtype=jnp.int32)[None, :]).astype(
        jnp.int32
    )
    earlier_all = jnp.cumsum(onehot, axis=0) - onehot
    ranks = jnp.sum(earlier_all * onehot, axis=1).reshape(count, topk)
    slot_id = routes * capacity + ranks
    slot_range = jnp.arange(experts * capacity, dtype=jnp.int32)
    dispatch = jnp.any(slot_id[None, :, :] == slot_range[:, None, None], axis=2).astype(
        jnp.bfloat16
    )
    share = jnp.sum(
        jnp.where(slot_id[:, :, None] == slot_range[None, None, :], route_weights[:, :, None], 0.0),
        axis=1,
    )
    outgoing = jnp.concatenate(
        [
            jnp.dot(dispatch, head_out, preferred_element_type=jnp.float32).astype(jnp.bfloat16),
            jnp.pad(dispatch, ((0, 0), (0, 128 - count))),
        ],
        axis=1,
    )
    near_packed, outgoing, share = lax.optimization_barrier((near_packed, outgoing, share))
    other_packed = lax.ppermute(near_packed, "core", [(0, 1), (1, 0)])
    received = lax.all_to_all(
        outgoing.reshape(experts, capacity, -1), EP, split_axis=0, concat_axis=0, tiled=True
    )
    core = lax.axis_index("core").astype(jnp.int32).reshape(1)
    results, residual = expert(
        core,
        received.reshape(experts * capacity, -1),
        head_out,
        tokens,
        moe_gain,
        near_packed,
        other_packed,
        gate_weight,
        up_weight,
        down_weight,
    )
    returned = lax.all_to_all(
        results.reshape(experts, capacity, -1), EP, split_axis=0, concat_axis=0, tiled=True
    )
    return combine(share, returned.reshape(experts * capacity, -1), residual)


def solution(mesh):
    devices = mesh.devices.reshape(mesh.shape["grp"], -1, 4, 2)
    torus = Mesh(devices, ("grp", "far", "near", "core"))
    return jax.shard_map(
        local,
        mesh=torus,
        in_specs=(
            P(GRP_EP, None),
            P(),
            P(None, EP),
            P(),
            P(),
            P(None, EP),
            P(),
            P(),
            P(GRP_EP, None, None, None),
            P(GRP_EP, None, None, None),
            P(GRP_EP),
            P(),
            P(EP, None, None),
            P(EP, None, None),
            P(EP, None, None),
            P(GRP_EP, None),
            P(GRP_EP, None),
        ),
        out_specs=P(GRP_EP, None),
        check_vma=False,
    )
```

time: 214 us -> 194 us (0.907)
  blocking collectives: 79.4 us -> 65.8 us
  starting transfers between devices: 48.5 us -> 34.9 us
  between operations: 0.37 us -> 13.6 us
  matrix products: 11.9 us -> 3.9 us
  waiting for transfers between devices: 36.4 us -> 34.1 us
    all_gather x1 -> x0, blocking collectives: 14.3 us -> none  [local(): near_heads = lax.all_gather(head_out, NEAR, axis=0, tiled=True)]
    all_to_all x1, waiting for transfers between devices: 31.9 us -> 20.2 us  [local(): lax.all_to_all(outgoing.reshape(experts, capacity, -1), EP, split_axis=0,...]
    all_gather x0 -> x1, waiting for transfers between devices: none -> 9.81 us  [local(): near_packed = lax.all_gather(packed, CHIPS, axis=0)]
    ppermute x6 -> x3, starting transfers between devices: 30.3 us -> 20.6 us  [far_blocks(): lax.ppermute(block, 'far', [(i, (i + d) % size) for i in range(size)])]
    dot_general x3 -> x1, matrix products: 8.15 us -> 1.02 us  [local(): jnp.dot(dispatch, head_out, preferred_element_type=jnp.float32)]
    all_gather x1, blocking collectives: 23 us -> 29 us  [local(): near_normed = lax.all_gather(normed, NEAR, axis=0, tiled=True)]
    all_to_all x2 -> x1, starting transfers between devices: 12.2 us -> 6.67 us  [near_product(): lax.all_to_all(outgoing.reshape(members, count, size * cols), NEAR, 0, 0,...]
    all_to_all x1, blocking collectives: 42 us -> 36.8 us  [local(): lax.all_to_all(results.reshape(experts, capacity, -1), EP, split_axis=0,...]
  transfers between devices with their start and end apart: 9 -> 7, of which waited for: 2 -> 3; matrix products, arithmetic and copies ran while one was open for 3% -> 9% of each run, Pallas kernels for 10% -> 4%
where the time goes in v3:
time: 194 us; the launch traced here: 191 us
  blocking collectives  65.8 us (34%)
  starting transfers between devices  34.9 us (18%)
  waiting for transfers between devices  34.1 us (18%)
  Pallas kernels  20.9 us (11%)
  between operations  13.6 us (7%)
  local copies, waits for them, and re-layouts  11.6 us (6%)
  other arithmetic  6.03 us (3%)
  matrix products  3.9 us (2%)
    all_to_all x1, blocking collectives, local(): lax.all_to_all(results.reshape(experts, capacity, -1), EP, split_axis=0,...  36.8 us
    all_gather x1, blocking collectives, local(): near_normed = lax.all_gather(normed, NEAR, axis=0, tiled=True)  29 us
    ppermute x3, starting transfers between devices, far_blocks(): lax.ppermute(block, 'far', [(i, (i + d) % size) for i in range(size)])  20.6 us
    all_to_all x1, waiting for transfers between devices, local(): lax.all_to_all(outgoing.reshape(experts, capacity, -1), EP, split_axis=0,...  20.2 us
    pallas_call x1, Pallas kernels, expert(): pl.pallas_call(expert_kernel, out_shape=(jax.ShapeDtypeStruct((slots, wid...  10.5 us
    all_gather x1, waiting for transfers between devices, local(): near_packed = lax.all_gather(packed, CHIPS, axis=0)  9.81 us
    pallas_call x1, Pallas kernels, attention(): pl.pallas_call(functools.partial(attention_kernel, together, 128), out_sh...  8.39 us
    all_to_all x1, starting transfers between devices, local(): lax.all_to_all(outgoing.reshape(experts, capacity, -1), EP, split_axis=0,...  7.64 us
  transfers between devices with their start and end apart: 7, of which 3 were waited for; matrix products, arithmetic and copies ran while one was open for 9% of the time, Pallas kernels for 4%

profile of v3, /device:TPU:196, one launch (start us, length us, event | category | flops | bytes accessed | tf_op | source)
XLA Modules:
  0.0 190.8 jit_solution(14837501230134381001)
XLA Ops:
  6.6 0.9 fusion.9
  7.5 1.6 pad_maximum_fusion.1
  9.1 14.6 %collective-permute-start.1 = (bf16[2048,32]{0,1:T(8,128)(2,1)}, bf16[2048,32]{0,1:T(8,128)(2,1)S(1)}, u32[]{:S(2)}, u32[]{:S(2)}) collective-permute-start(bf16[2048,32]{0,1:T(8,128)(2,1)} %param.19), channel_id=1, source_target_pairs={{0,16},{8,24},{16,0},{24,8},{1,17},{9,25},{17,1},{25,9},{2,18},{10... | collective-permute-start | bytes 393224 | tf_op jit(solution)/shard_map/ppermute | solution.py:36
  23.8 5.9 %collective-permute-start.2 = (bf16[2048,32]{0,1:T(8,128)(2,1)}, bf16[2048,32]{0,1:T(8,128)(2,1)S(1)}, u32[]{:S(2)}, u32[]{:S(2)}) collective-permute-start(bf16[2048,32]{0,1:T(8,128)(2,1)} %param.19), channel_id=1, source_target_pairs={{0,8},{8,16},{16,24},{24,0},{1,9},{9,17},{17,25},{25,1},{2,10},{10... | collective-permute-start | bytes 393224 | tf_op jit(solution)/shard_map/ppermute | solution.py:36
  29.7 0.7 convert_element_type.38
  30.4 0.8 copy.40
  31.2 0.1 eq.20
  31.3 0.1 reduce_window_sum.11
  31.4 0.2 select_reduce_fusion.1
  31.7 0.1 copy.41
  31.8 1.0 fusion.4
  32.8 0.7 multiply_add_fusion
  33.5 0.9 fusion.6
  34.4 29.0 %all_gather.11 = bf16[128,2048]{1,0:T(8,128)(2,1)S(1)} all-gather(bf16[16,2048]{1,0:T(8,128)(2,1)S(1)} %fusion.6), channel_id=1, replica_groups=mesh['grp'=4,'far'=4,'near'=4,'core'=2] {'near','core'}, dimensions={0}, use_global_device_ids=true | all-gather | bytes 589824 | tf_op jit(solution)/shard_map/all_gather | solution.py:387
  63.3 0.2 convolution_convert_fusion.1
  63.6 1.5 convolution_convert_fusion.2
  65.1 0.1 fusion.8
  65.2 0.1 copy.45
  65.3 0.6 reshape.67.nv_ref
  65.9 0.6 reshape.66.nk_ref
  66.5 0.3 constant_dynamic-update-slice_fusion.7
  66.8 0.3 constant_dynamic-update-slice_fusion.6
  67.1 0.3 constant_dynamic-update-slice_fusion.5
  67.5 0.3 constant_dynamic-update-slice_fusion.4
  67.8 0.1 copy.42
  67.9 0.1 copy.43
  68.1 0.7 reshape.64
  68.8 6.7 %all-to-all-start = ((bf16[8,16,128]{2,1,0:T(8,128)(2,1)}), bf16[8,16,128]{2,1,0:T(8,128)(2,1)S(1)}, u32[]{:S(2)}, u32[]{:S(2)}) async-start(bf16[8,16,128]{2,1,0:T(8,128)(2,1)} %reshape.64), calls=%async_computation | async-start | bytes 65536 | tf_op jit(solution)/shard_map/all_to_all | solution.py:53
  75.5 0.7 select_reduce_fusion.share_ref
  76.2 4.0 %all-to-all-done = bf16[8,16,128]{2,1,0:T(8,128)(2,1)S(1)} async-done(((bf16[8,16,128]{2,1,0:T(8,128)(2,1)}), bf16[8,16,128]{2,1,0:T(8,128)(2,1)S(1)}, u32[]{:S(2)}, u32[]{:S(2)}) %all-to-all-start) | async-done | bytes 32800 | tf_op jit(solution)/shard_map/all_to_all | solution.py:53
  80.2 0.1 reshape.65
  80.3 0.1 copy.44
  80.4 0.7 reshape_reshape.3.q_ref
  81.1 0.7 broadcast_in_dim.10.lam_ref
  81.8 8.4 %attention.1 = bf16[16,8,128]{2,1,0:T(8,128)(2,1)} custom-call(s32[16]{0:T(128)} %lens_ref.1, bf16[16,8,128]{2,1,0:T(8,128)(2,1)} %reshape_reshape.3.q_ref, bf16[16,2,128]{2,1,0:T(2,128)(2,1)} %reshape.66.nk_ref, bf16[16,2,128]{2,1,0:T(2,128)(2,1)} %reshape.67.nv_ref, f32[8,128]{1,0:T(8,128)} %broadcast_in_dim.10.lam_ref, bf16[1,128]{1,0:T(2,128)(2,1)} %bitcast.48, ...), custom_call_target="tpu_custom_call" | custom-call | tf_op jit(solution)/shard_map/attention/pallas_call | solution.py:175
  90.2 1.0 convolution_convert_fusion
  91.3 9.8 %all-gather.3.cloned.1.call-done = bf16[1536,1024]{1,0:T(8,128)(2,1)} async-done(((bf16[96,1024]{1,0:T(8,128)(2,1)}), bf16[1536,1024]{1,0:T(8,128)(2,1)}) %all-gather.3.cloned.1.call-update) | async-done | bytes 3145744 | tf_op jit(solution)/shard_map/all_gather | solution.py:380
  101.1 0.8 reshape.73
  101.8 7.6 %all-to-all-start.1 = ((bf16[32,4,1152]{2,1,0:T(4,128)(2,1)}), bf16[32,4,1152]{2,1,0:T(4,128)(2,1)S(1)}, u32[]{:S(2)}, u32[]{:S(2)}) async-start(bf16[32,4,1152]{2,1,0:T(4,128)(2,1)} %reshape.73), calls=%async_computation.1 | async-start | bytes 589824 | tf_op jit(solution)/shard_map/all_to_all | solution.py:417
  109.5 0.6 reshape.75.gain_ref
  110.1 1.4 copy.49
  111.5 20.2 %all-to-all-done.1 = bf16[32,4,1152]{2,1,0:T(4,128)(2,1)S(1)} async-done(((bf16[32,4,1152]{2,1,0:T(4,128)(2,1)}), bf16[32,4,1152]{2,1,0:T(4,128)(2,1)S(1)}, u32[]{:S(2)}, u32[]{:S(2)}) %all-to-all-start.1) | async-done | bytes 294944 | tf_op jit(solution)/shard_map/all_to_all | solution.py:417
  131.7 0.8 reshape.74.h_ref
  132.5 10.5 %expert.1 = (bf16[128,2048]{1,0:T(8,128)(2,1)}, bf16[16,2048]{1,0:T(8,128)(2,1)}) custom-call(s32[1]{0:T(128)} %bitcast.12.core_ref, bf16[128,1152]{1,0:T(8,128)(2,1)} %reshape.74.h_ref, bf16[16,1024]{1,0:T(8,128)(2,1)} %bitcast.46, bf16[16,2048]{1,0:T(8,128)(2,1)} %tok_ref.1, bf16[1,2048]{1,0:T(2,128)(2,1)} %reshape.75.gain_ref, ...), custom_call_target="tpu_custom_call" | custom-call | tf_op jit(solution)/shard_map/expert/pallas_call | solution.py:310
  143.1 1.2 reshape.76
  144.3 36.8 %all_to_all.15 = bf16[32,4,2048]{2,1,0:T(4,128)(2,1)S(1)} all-to-all(bf16[32,4,2048]{2,1,0:T(4,128)(2,1)S(1)} %reshape.76), channel_id=1, replica_groups=mesh['grp'=4,'far'=4,'near'=4,'core'=2] {'far','near','core'}, dimensions={0} | all-to-all | bytes 1048576 | tf_op jit(solution)/shard_map/all_to_all | solution.py:433
  181.1 0.9 reshape.77.rows_ref
  182.0 1.9 %combine.1 = bf16[16,2048]{1,0:T(8,128)(2,1)} custom-call(f32[16,128]{1,0:T(8,128)} %select_reduce_fusion.share_ref, bf16[128,2048]{1,0:T(8,128)(2,1)} %reshape.77.rows_ref, bf16[16,2048]{1,0:T(8,128)(2,1)} %get-tuple-element.14.res_ref), custom_call_target="tpu_custom_call" | custom-call | tf_op jit(solution)/shard_map/combine/pallas_call | solution.py:348
  (28 shorter events, 0.4 us)
Async XLA Ops:
  6.5 56.8 %copy-start = (bf16[2048,256]{1,0:T(8,128)(2,1)S(1)}, bf16[2048,256]{1,0:T(8,128)(2,1)}, u32[]{:S(2)}) copy-start(bf16[2048,256]{1,0:T(8,128)(2,1)} %param.21) | copy-start | bytes 3145732
  6.6 60.9 %copy-start.1 = (bf16[2048,32]{0,1:T(8,128)(2,1)S(1)}, bf16[2048,32]{0,1:T(8,128)(2,1)}, u32[]{:S(2)}) copy-start(bf16[2048,32]{0,1:T(8,128)(2,1)} %param.19) | copy-start | bytes 393220
  6.6 68.9 %copy-start.3 = (f32[16,4]{0,1:T(4,128)S(1)}, f32[16,4]{0,1:T(4,128)}, u32[]{:S(2)}) copy-start(f32[16,4]{0,1:T(4,128)} %param.33) | copy-start | bytes 772
  6.6 74.6 %copy-start.4 = (f32[8]{0:T(128)S(1)}, f32[8]{0:T(128)}, u32[]{:S(2)}) copy-start(f32[8]{0:T(128)} %param.24) | copy-start | bytes 100
  6.6 94.5 %all-gather.3.cloned.1.call-start = ((), (), s32[]{:S(2)}) async-start(), calls=%async_computation.3 | async-start | bytes 3342336 | tf_op jit(solution)/shard_map/all_gather | solution.py:380
  9.1 57.7 %collective-permute-start.1 = (bf16[2048,32]{0,1:T(8,128)(2,1)}, bf16[2048,32]{0,1:T(8,128)(2,1)S(1)}, u32[]{:S(2)}, u32[]{:S(2)}) collective-permute-start(bf16[2048,32]{0,1:T(8,128)(2,1)} %param.19), channel_id=1, source_target_pairs={{0,16},{8,24},{16,0},{24,8},{1,17},{9,25},{17,1},{25,9},{2,18},{10... | collective-permute-start | bytes 393224 | tf_op jit(solution)/shard_map/ppermute | solution.py:36
  23.8 42.8 %collective-permute-start = (bf16[2048,32]{0,1:T(8,128)(2,1)}, bf16[2048,32]{0,1:T(8,128)(2,1)S(1)}, u32[]{:S(2)}, u32[]{:S(2)}) collective-permute-start(bf16[2048,32]{0,1:T(8,128)(2,1)} %param.19), channel_id=1, source_target_pairs={{0,24},{8,0},{16,8},{24,16},{1,25},{9,1},{17,9},{25,17},{2,26},{10... | collective-permute-start | bytes 393224 | tf_op jit(solution)/shard_map/ppermute | solution.py:36
  23.8 43.4 %collective-permute-start.2 = (bf16[2048,32]{0,1:T(8,128)(2,1)}, bf16[2048,32]{0,1:T(8,128)(2,1)S(1)}, u32[]{:S(2)}, u32[]{:S(2)}) collective-permute-start(bf16[2048,32]{0,1:T(8,128)(2,1)} %param.19), channel_id=1, source_target_pairs={{0,8},{8,16},{16,24},{24,0},{1,9},{9,17},{17,25},{25,1},{2,10},{10... | collective-permute-start | bytes 393224 | tf_op jit(solution)/shard_map/ppermute | solution.py:36
  68.8 11.4 %all-to-all-start = ((bf16[8,16,128]{2,1,0:T(8,128)(2,1)}), bf16[8,16,128]{2,1,0:T(8,128)(2,1)S(1)}, u32[]{:S(2)}, u32[]{:S(2)}) async-start(bf16[8,16,128]{2,1,0:T(8,128)(2,1)} %reshape.64), calls=%async_computation | async-start | bytes 65536 | tf_op jit(solution)/shard_map/all_to_all | solution.py:53
  81.8 27.7 %copy-start.2 = (bf16[2048]{0:T(1024)(128)(2,1)S(1)}, bf16[2048]{0:T(1024)(128)(2,1)}, u32[]{:S(2)}) copy-start(bf16[2048]{0:T(1024)(128)(2,1)} %param.28) | copy-start | bytes 12292
  101.1 31.4 %collective-permute-start.3 = (bf16[16,96,1024]{2,1,0:T(8,128)(2,1)}, bf16[16,96,1024]{2,1,0:T(8,128)(2,1)}, u32[]{:S(2)}, u32[]{:S(2)}) collective-permute-start(bf16[16,96,1024]{2,1,0:T(8,128)(2,1)} %bitcast.40), channel_id=1, source_target_pairs={{0,1},{1,0},{2,3},{3,2},{4,5},{5,4},{6,7},{7,6},{8,9},{9,8},{10,11... | collective-permute-start | bytes 9437192 | tf_op jit(solution)/shard_map/ppermute | solution.py:416
  101.8 29.8 %all-to-all-start.1 = ((bf16[32,4,1152]{2,1,0:T(4,128)(2,1)}), bf16[32,4,1152]{2,1,0:T(4,128)(2,1)S(1)}, u32[]{:S(2)}, u32[]{:S(2)}) async-start(bf16[32,4,1152]{2,1,0:T(4,128)(2,1)} %reshape.73), calls=%async_computation.1 | async-start | bytes 589824 | tf_op jit(solution)/shard_map/all_to_all | solution.py:417
Sparse Core Ops, SparseCore 0:
  9.2 91.7 all-gather.2

commit v4 on v3

--- a/solution.py
+++ b/solution.py
@@ -7,6 +7,7 @@
 from jax.experimental.pallas import tpu as pltpu
 from jax.sharding import Mesh
 from jax.sharding import PartitionSpec as P
+
 
 EP = ("far", "near", "core")
 NEAR = ("near", "core")
@@ -50,25 +51,37 @@
     stacked = jnp.stack(parts[::-1] + parts[::-1])
     placed = lax.dynamic_slice_in_dim(stacked, size - 1 - here, size, axis=0)
     outgoing = jnp.transpose(placed.reshape(size, members, count, cols), (1, 2, 0, 3))
-    received = lax.all_to_all(
+    return lax.all_to_all(
         outgoing.reshape(members, count, size * cols), NEAR, 0, 0, tiled=True
-    ).reshape(members, count, size, cols)
-    return jnp.transpose(received, (1, 2, 0, 3)).reshape(count, size * members * cols)
+    )
+
+
+def rows_of(ref):
+    return jnp.concatenate([ref[i] for i in range(ref.shape[0])], axis=0)
+
+
+def put_rows(ref, lanes, value):
+    per = ref.shape[1]
+    for i in range(ref.shape[0]):
+        ref[i, :, lanes] = value[i * per : (i + 1) * per]
 
 
 def attention_kernel(
-    group_size, chunk, lens_ref, q_ref, nk_ref, nv_ref, lam_ref, gain_ref, k_hbm, v_hbm, o_ref, k_buf, v_buf, s_buf, k_sem, v_sem
+    group_size, chunk, shard, lens_ref, lam_ref, r_ref, nk_ref, nv_ref, gain_ref, disp_ref, k_hbm, v_hbm,
+    o_ref, out_ref, k_buf, v_buf, s_buf, q_buf, k_sem, v_sem,
 ):
-    count, heads, width = q_ref.shape
-    kv_count = nk_ref.shape[1]
+    count, heads, width = q_buf.shape
+    kv_count = nk_ref.shape[1] // width
     group = heads // kv_count
     half = width // 2
     rows = k_buf.shape[1]
     chunk_rows = chunk * kv_count
     chunks = rows // chunk_rows
     inv_scale = half ** (-0.5)
-
-    def piece(s, c):
+    channels = shard
+    far_heads = width // channels
+
+    def piece(c):
         return pl.ds(pl.multiple_of(c * chunk_rows, chunk_rows), chunk_rows)
 
     def copies(s, where):
@@ -97,6 +110,17 @@
         return 0
 
     lax.fori_loop(0, count, fetch, 0)
+
+    for h in range(heads):
+        parts = []
+        for m in range(far_heads):
+            piece_at = (h * far_heads + m) // r_ref.shape[0] * channels
+            parts.append(
+                r_ref[(h * far_heads + m) % r_ref.shape[0]].astype(jnp.float32)[
+                    :, piece_at : piece_at + channels
+                ]
+            )
+        q_buf[:, h, :] = jnp.concatenate(parts, axis=1)
 
     lane = lax.broadcasted_iota(jnp.int32, (heads, width), 1)
     head_row = lax.broadcasted_iota(jnp.int32, (heads, width), 0)
@@ -105,20 +129,24 @@
     own_kv = (column % kv_count) == score_head // group
     position = jnp.where(own_kv, column // kv_count, rows)[None]
     gain = gain_ref[...].astype(jnp.float32)
-    lam = lam_ref[...][None, :, :1]
+    lam = jnp.zeros((heads, 1), jnp.float32)
+    for h in range(heads):
+        lam = jnp.where(head_row[:, :1] == h, lam_ref[h], lam)
+    lam = lam[None]
     low = (lane < half)[None]
     block = lax.broadcasted_iota(jnp.int32, (group_size, 1, heads, 1), 0)
 
     def spread(values):
-        out = jnp.broadcast_to(values[:, kv_count - 1 :], (group_size, heads, width))
-        for k in range(kv_count - 1):
-            out = jnp.where((head_row // group == k)[None], values[:, k : k + 1], out)
+        out = jnp.zeros((group_size, heads, width), jnp.float32)
+        for k in range(kv_count):
+            part = values[:, k * width : (k + 1) * width].reshape(group_size, 1, width)
+            out = jnp.where((head_row // group == k)[None], part, out)
         return out
 
     def step(g, _):
         first = g * group_size
         here = pl.ds(first, group_size)
-        q = q_ref[here]
+        q = q_buf[here].astype(jnp.bfloat16)
         zero = jnp.zeros_like(q)
         split = jnp.stack([jnp.where(low, q, zero), jnp.where(low, zero, q)], axis=1)
         own_key = spread(nk_ref[here].astype(jnp.float32))
@@ -132,7 +160,7 @@
             limit = jnp.where(block == i, lens_ref[s], limit)
 
             def wait(c, _):
-                for copy in copies(s, piece(s, c)):
+                for copy in copies(s, piece(c)):
                     copy.wait()
                 return 0
 
@@ -158,45 +186,65 @@
         )
         attended = attended + own_weight.astype(jnp.float32) * own_val
         scale = lax.rsqrt(jnp.mean(attended * attended, axis=2, keepdims=True) + epsilon)
-        o_ref[here] = (attended * scale * gain[None]).astype(o_ref.dtype)
+        q_buf[here] = (attended * scale * gain[None]).astype(o_ref.dtype).astype(jnp.float32)
         return 0
 
     lax.fori_loop(0, count // group_size, step, 0)
-
-
-def attention(queries, new_keys, new_values, cache_keys, cache_values, lengths, lambdas, head_gain):
+    heads_out = jnp.concatenate([q_buf[:, h, :] for h in range(heads)], axis=1).astype(o_ref.dtype)
+    o_ref[...] = heads_out
+    chosen = disp_ref[...]
+    full = jnp.concatenate(
+        [heads_out, jnp.zeros((chosen.shape[1] - count, heads * width), o_ref.dtype)], axis=0
+    )
+    put_rows(
+        out_ref,
+        pl.ds(0, heads * width),
+        jnp.dot(chosen, full, preferred_element_type=jnp.float32).astype(out_ref.dtype),
+    )
+    put_rows(out_ref, pl.ds(heads * width, chosen.shape[1]), chosen)
+
+
+def attention(
+    queries, new_keys, new_values, cache_keys, cache_values, lengths, lambdas, head_gain, dispatch, experts
+):
     count, ctx_len, kv_count, width = cache_keys.shape
     heads = lambdas.shape[0]
+    slots, lanes = dispatch.shape
+    shard = heads * width // experts
     vmem = pl.BlockSpec(memory_space=pltpu.VMEM)
     smem = pl.BlockSpec(memory_space=pltpu.SMEM)
     hbm = pl.BlockSpec(memory_space=pltpu.HBM)
     rows = ctx_len * kv_count
     together = 8
-    out = pl.pallas_call(
-        functools.partial(attention_kernel, together, 128),
-        out_shape=jax.ShapeDtypeStruct((count, heads, width), jnp.bfloat16),
-        in_specs=[smem, vmem, vmem, vmem, vmem, vmem, hbm, hbm],
-        out_specs=vmem,
+    return pl.pallas_call(
+        functools.partial(attention_kernel, together, 128, shard),
+        out_shape=(
+            jax.ShapeDtypeStruct((count, heads * width), jnp.bfloat16),
+            jax.ShapeDtypeStruct((experts, slots // experts, heads * width + lanes), jnp.bfloat16),
+        ),
+        in_specs=[smem, smem, vmem, vmem, vmem, vmem, vmem, hbm, hbm],
+        out_specs=(vmem, vmem),
         scratch_shapes=[
             pltpu.VMEM((count, rows, width), jnp.bfloat16),
             pltpu.VMEM((count, rows, width), jnp.bfloat16),
             pltpu.VMEM((together, 2, heads, rows), jnp.float32),
+            pltpu.VMEM((count, heads, width), jnp.float32),
             pltpu.SemaphoreType.DMA((count,)),
             pltpu.SemaphoreType.DMA((count,)),
         ],
-        compiler_params=pltpu.CompilerParams(vmem_limit_bytes=60 * 2**20),
+        compiler_params=pltpu.CompilerParams(vmem_limit_bytes=56 * 2**20),
         name="attention",
     )(
         lengths,
-        queries.reshape(count, heads, width),
-        new_keys.reshape(count, kv_count, width),
-        new_values.reshape(count, kv_count, width),
-        jnp.broadcast_to(lambdas[:, None], (heads, width)),
+        lambdas,
+        queries,
+        new_keys,
+        new_values,
         head_gain.reshape(1, width),
+        dispatch,
         cache_keys.reshape(count, rows, width),
         cache_values.reshape(count, rows, width),
     )
-    return out.reshape(count, heads * width)
 
 
 def expert_kernel(
@@ -207,11 +255,11 @@
     cols = wo_buf.shape[1] // 2
     depth = wo_buf.shape[2]
     count = own_ref.shape[0]
-    slots = h_ref.shape[0]
+    slots = h_ref.shape[0] * h_ref.shape[1]
     members = x_buf.shape[1] * 2
     halves = x_buf.shape[0]
     pieces = down_sem.shape[0]
-    width = o_ref.shape[1]
+    width = o_ref.shape[2]
     step = width // pieces
 
     wo_copies = []
@@ -241,8 +289,9 @@
     for copy in (*wo_copies, *x_copies, gate_copy, up_copy, *down_copies):
         copy.start()
 
-    heads = jnp.concatenate([h_ref[:, :depth], own_ref[...]], axis=0)
-    chosen = h_ref[:, depth:]
+    arrived = rows_of(h_ref)
+    heads = jnp.concatenate([arrived[:, :depth], own_ref[...]], axis=0)
+    chosen = arrived[:, depth:]
     lanes = chosen.shape[1]
     per = slots // members
     token = lax.broadcasted_iota(jnp.int32, (lanes, members * count), 0)
@@ -290,13 +339,15 @@
     for i, copy in enumerate(down_copies):
         copy.wait()
         at = pl.ds(i * step, step)
-        o_ref[:, at] = jnp.dot(act, down_buf[:, at], preferred_element_type=jnp.float32).astype(
-            o_ref.dtype
+        put_rows(
+            o_ref,
+            at,
+            jnp.dot(act, down_buf[:, at], preferred_element_type=jnp.float32).astype(o_ref.dtype),
         )
 
 
 def expert(core, received, head_out, tokens, moe_gain, near, other, gate_w, up_w, down_w):
-    slots = received.shape[0]
+    members, per, _ = received.shape
     count, width = tokens.shape
     chips, packed, depth = near.shape
     halves = width // depth
@@ -310,7 +361,7 @@
     return pl.pallas_call(
         expert_kernel,
         out_shape=(
-            jax.ShapeDtypeStruct((slots, width), bf16),
+            jax.ShapeDtypeStruct((members, per, width), bf16),
             jax.ShapeDtypeStruct((count, width), bf16),
         ),
         in_specs=[smem, vmem, vmem, vmem, vmem, hbm, hbm, hbm, hbm, hbm],
@@ -336,7 +387,7 @@
     share = share_ref[...]
     high = share.astype(jnp.bfloat16)
     low = (share - high.astype(jnp.float32)).astype(jnp.bfloat16)
-    rows = rows_ref[...]
+    rows = rows_of(rows_ref)
     total = jnp.dot(high, rows, preferred_element_type=jnp.float32) + jnp.dot(
         low, rows, preferred_element_type=jnp.float32
     )
@@ -350,6 +401,7 @@
         out_shape=jax.ShapeDtypeStruct(residual.shape, jnp.bfloat16),
         in_specs=[vmem] * 3,
         out_specs=vmem,
+        compiler_params=pltpu.CompilerParams(vmem_limit_bytes=32 * 2**20),
         name="combine",
     )(share, rows, residual)
 
@@ -386,9 +438,6 @@
     )
     near_normed = lax.all_gather(normed, NEAR, axis=0, tiled=True)
     queries = near_product(near_normed, query_blocks)
-    head_out = attention(
-        queries, new_keys, new_values, cache_keys, cache_values, lengths, lambdas, head_gain
-    )
     experts = lax.axis_size(EP)
     capacity = min(count, max(2, 2 * count * topk // experts))
     onehot = (routes.reshape(-1)[:, None] == jnp.arange(experts, dtype=jnp.int32)[None, :]).astype(
@@ -405,22 +454,17 @@
         jnp.where(slot_id[:, :, None] == slot_range[None, None, :], route_weights[:, :, None], 0.0),
         axis=1,
     )
-    outgoing = jnp.concatenate(
-        [
-            jnp.dot(dispatch, head_out, preferred_element_type=jnp.float32).astype(jnp.bfloat16),
-            jnp.pad(dispatch, ((0, 0), (0, 128 - count))),
-        ],
-        axis=1,
-    )
-    near_packed, outgoing, share = lax.optimization_barrier((near_packed, outgoing, share))
+    dispatch = jnp.pad(dispatch, ((0, 0), (0, 128 - count)))
+    head_out, outgoing = attention(
+        queries, new_keys, new_values, cache_keys, cache_values, lengths, lambdas, head_gain, dispatch, experts
+    )
+    received = lax.all_to_all(outgoing, EP, split_axis=0, concat_axis=0, tiled=True)
+    near_packed, head_out = lax.optimization_barrier((near_packed, head_out))
     other_packed = lax.ppermute(near_packed, "core", [(0, 1), (1, 0)])
-    received = lax.all_to_all(
-        outgoing.reshape(experts, capacity, -1), EP, split_axis=0, concat_axis=0, tiled=True
-    )
     core = lax.axis_index("core").astype(jnp.int32).reshape(1)
     results, residual = expert(
         core,
-        received.reshape(experts * capacity, -1),
+        received,
         head_out,
         tokens,
         moe_gain,
@@ -430,10 +474,8 @@
         up_weight,
         down_weight,
     )
-    returned = lax.all_to_all(
-        results.reshape(experts, capacity, -1), EP, split_axis=0, concat_axis=0, tiled=True
-    )
-    return combine(share, returned.reshape(experts * capacity, -1), residual)
+    returned = lax.all_to_all(results, EP, split_axis=0, concat_axis=0, tiled=True)
+    return combine(share, returned, residual)
 
 
 def solution(mesh):

time: 194 us -> 195 us (level)
  waiting for transfers between devices: 34.1 us -> 72.7 us
  blocking collectives: 65.8 us -> 29.4 us
  local copies, waits for them, and re-layouts: 11.6 us -> 5.83 us
  starting transfers between devices: 34.9 us -> 39.8 us
    all_to_all x1 -> x0, blocking collectives: 36.8 us -> none  [local(): lax.all_to_all(results.reshape(experts, capacity, -1), EP, split_axis=0,...]
    all_to_all x1 -> x2, waiting for transfers between devices: 20.2 us -> 53.6 us  [the longest x1 32 us: local(): lax.all_to_all(results, EP, split_axis=0, concat_axis=0, tiled=True)]
    all_to_all x1 -> x2, starting transfers between devices: 7.64 us -> 14.1 us  [the longest x1 8.38 us: local(): lax.all_to_all(outgoing, EP, split_axis=0, concat_axis=0, tiled=True)]
    all_gather x1, waiting for transfers between devices: 9.81 us -> 15.1 us  [local(): near_packed = lax.all_gather(packed, CHIPS, axis=0)]
    reshape x7 -> x0, local copies, waits for them, and re-layouts: 5.04 us -> none  [the longest x1 1.24 us: local(): results.reshape(experts, capacity, -1)]
  transfers between devices with their start and end apart: 7 -> 8, of which waited for: 3 -> 4; matrix products, arithmetic and copies ran while one was open for 9% -> 6% of each run, Pallas kernels for 4% -> 4%
where the time goes in v4:
time: 195 us; the launch traced here: 191 us
  waiting for transfers between devices  72.7 us (37%)
  starting transfers between devices  39.8 us (20%)
  blocking collectives  29.4 us (15%)
  Pallas kernels  20.1 us (10%)
  between operations  13.6 us (7%)
  other arithmetic  6.04 us (3%)
  local copies, waits for them, and re-layouts  5.83 us (3%)
  matrix products  4.06 us (2%)
    all_to_all x1, waiting for transfers between devices, local(): lax.all_to_all(results, EP, split_axis=0, concat_axis=0, tiled=True)  32 us
    all_gather x1, blocking collectives, local(): near_normed = lax.all_gather(normed, NEAR, axis=0, tiled=True)  29.4 us
    all_to_all x1, waiting for transfers between devices, local(): lax.all_to_all(outgoing, EP, split_axis=0, concat_axis=0, tiled=True)  21.6 us
    ppermute x3, starting transfers between devices, far_blocks(): lax.ppermute(block, 'far', [(i, (i + d) % size) for i in range(size)])  20.6 us
    all_gather x1, waiting for transfers between devices, local(): near_packed = lax.all_gather(packed, CHIPS, axis=0)  15.1 us
    pallas_call x1, Pallas kernels, expert(): pl.pallas_call(expert_kernel, out_shape=(jax.ShapeDtypeStruct((members, p...  10.5 us
    pallas_call x1, Pallas kernels, attention(): pl.pallas_call(functools.partial(attention_kernel, together, 128, shard),...  8.57 us
    all_to_all x1, starting transfers between devices, local(): lax.all_to_all(outgoing, EP, split_axis=0, concat_axis=0, tiled=True)  8.38 us
  transfers between devices with their start and end apart: 8, of which 4 were waited for; matrix products, arithmetic and copies ran while one was open for 6% of the time, Pallas kernels for 4%

profile of v4, /device:TPU:196, one launch (start us, length us, event | category | flops | bytes accessed | tf_op | source)
XLA Modules:
  0.0 191.5 jit_solution(10359708019073102131)
XLA Ops:
  6.6 0.9 fusion.9
  7.4 1.6 pad_maximum_fusion
  9.0 0.1 all-gather.3.cloned.1.call-update
  9.1 12.5 %collective-permute-start = (bf16[2048,32]{0,1:T(8,128)(2,1)}, bf16[2048,32]{0,1:T(8,128)(2,1)S(1)}, u32[]{:S(2)}, u32[]{:S(2)}) collective-permute-start(bf16[2048,32]{0,1:T(8,128)(2,1)} %param.19), channel_id=1, source_target_pairs={{0,24},{8,0},{16,8},{24,16},{1,25},{9,1},{17,9},{25,17},{2,26},{10... | collective-permute-start | bytes 393224 | tf_op jit(solution)/shard_map/ppermute | solution.py:37
  21.6 2.3 %collective-permute-start.1 = (bf16[2048,32]{0,1:T(8,128)(2,1)}, bf16[2048,32]{0,1:T(8,128)(2,1)S(1)}, u32[]{:S(2)}, u32[]{:S(2)}) collective-permute-start(bf16[2048,32]{0,1:T(8,128)(2,1)} %param.19), channel_id=1, source_target_pairs={{0,16},{8,24},{16,0},{24,8},{1,17},{9,25},{17,1},{25,9},{2,18},{10... | collective-permute-start | bytes 393224 | tf_op jit(solution)/shard_map/ppermute | solution.py:37
  23.9 5.8 %collective-permute-start.2 = (bf16[2048,32]{0,1:T(8,128)(2,1)}, bf16[2048,32]{0,1:T(8,128)(2,1)S(1)}, u32[]{:S(2)}, u32[]{:S(2)}) collective-permute-start(bf16[2048,32]{0,1:T(8,128)(2,1)} %param.19), channel_id=1, source_target_pairs={{0,8},{8,16},{16,24},{24,0},{1,9},{9,17},{17,25},{25,1},{2,10},{10... | collective-permute-start | bytes 393224 | tf_op jit(solution)/shard_map/ppermute | solution.py:37
  29.7 0.7 convert_element_type.35
  30.4 0.8 copy.33
  31.1 0.1 eq.20
  31.2 0.1 fusion.7
  31.3 0.1 reduce_window_sum.11
  31.4 0.2 select_reduce_fusion.1
  31.6 0.1 reshape.37
  31.6 0.1 copy.34
  31.7 1.0 fusion.4
  32.7 0.9 fusion.6
  33.7 29.4 %all_gather.9 = bf16[128,2048]{1,0:T(8,128)(2,1)S(1)} all-gather(bf16[16,2048]{1,0:T(8,128)(2,1)S(1)} %fusion.6), channel_id=1, replica_groups=mesh['grp'=4,'far'=4,'near'=4,'core'=2] {'near','core'}, dimensions={0}, use_global_device_ids=true | all-gather | bytes 589824 | tf_op jit(solution)/shard_map/all_gather | solution.py:439
  63.0 0.8 convolution_convert_fusion.nv_ref
  63.9 2.1 %convolution_convert_fusion.1.nk_ref = bf16[16,256]{1,0:T(8,128)(2,1)} fusion(bf16[16,2048]{1,0:T(8,128)(2,1)S(1)} %fusion.6, bf16[2048,256]{1,0:T(8,128)(2,1)} %param.20), kind=kOutput, calls=%fused_computation.1 | convolution fusion | flops 16781312 | bytes 1122304 | tf_op jit(solution)/shard_map/dot_general | solution.py:435
  65.9 0.7 multiply_add_fusion
  66.6 0.0 collective-permute-done
  66.6 0.3 constant_dynamic-update-slice_fusion.7
  66.9 0.0 collective-permute-done.1
  66.9 0.3 constant_dynamic-update-slice_fusion.6
  67.2 0.3 constant_dynamic-update-slice_fusion.5
  67.5 0.3 constant_dynamic-update-slice_fusion.4
  67.9 0.1 copy.35
  68.0 0.1 copy.36
  68.1 0.7 reshape.40
  68.9 5.2 %all-to-all-start = ((bf16[8,16,128]{2,1,0:T(8,128)(2,1)}), bf16[8,16,128]{2,1,0:T(8,128)(2,1)S(1)}, u32[]{:S(2)}, u32[]{:S(2)}) async-start(bf16[8,16,128]{2,1,0:T(8,128)(2,1)} %reshape.40), calls=%async_computation | async-start | bytes 65536 | tf_op jit(solution)/shard_map/all_to_all | solution.py:54
  74.1 0.1 fusion.8
  74.2 0.1 copy.37
  74.3 0.6 pad_convert_fusion.disp_ref
  74.9 4.0 %all-to-all-done.r_ref = bf16[8,16,128]{2,1,0:T(8,128)(2,1)S(1)} async-done(((bf16[8,16,128]{2,1,0:T(8,128)(2,1)}), bf16[8,16,128]{2,1,0:T(8,128)(2,1)S(1)}, u32[]{:S(2)}, u32[]{:S(2)}) %all-to-all-start) | async-done | bytes 32800 | tf_op jit(solution)/shard_map/all_to_all | solution.py:54
  78.9 0.6 copy-done.3
  79.5 8.6 %attention.1 = (bf16[16,1024]{1,0:T(8,128)(2,1)}, bf16[32,4,1152]{2,1,0:T(4,128)(2,1)}) custom-call(s32[16]{0:T(128)} %lens_ref.1, f32[8]{0:T(128)} %lam_ref.1, bf16[8,16,128]{2,1,0:T(8,128)(2,1)} %copy-done.3, bf16[16,256]{1,0:T(8,128)(2,1)} %convolution_convert_fusion.1.nk_ref, bf16[16,256]{1,0:T(8,128)(2,1)} %convolution_convert_fusion.nv_ref, ...), custom_call_target="tpu_custom_call" | custom-call | tf_op jit(solution)/shard_map/attention/pallas_call | solution.py:219
  88.1 15.1 %all-gather.3.cloned.1.call-done = bf16[1536,1024]{1,0:T(8,128)(2,1)} async-done(((bf16[96,1024]{1,0:T(8,128)(2,1)}), bf16[1536,1024]{1,0:T(8,128)(2,1)}) %all-gather.3.cloned.1.call-update) | async-done | bytes 3145744 | tf_op jit(solution)/shard_map/all_gather | solution.py:432
  103.2 8.4 %all-to-all-start.1 = ((bf16[32,4,1152]{2,1,0:T(4,128)(2,1)}), bf16[32,4,1152]{2,1,0:T(4,128)(2,1)S(1)}, u32[]{:S(2)}, u32[]{:S(2)}) async-start(bf16[32,4,1152]{2,1,0:T(4,128)(2,1)} %get-tuple-element.11), calls=%async_computation.1 | async-start | bytes 589824 | tf_op jit(solution)/shard_map/all_to_all | solution.py:461
  111.6 0.6 reshape.44.gain_ref
  112.2 21.6 %all-to-all-done.1.h_ref = bf16[32,4,1152]{2,1,0:T(4,128)(2,1)S(1)} async-done(((bf16[32,4,1152]{2,1,0:T(4,128)(2,1)}), bf16[32,4,1152]{2,1,0:T(4,128)(2,1)S(1)}, u32[]{:S(2)}, u32[]{:S(2)}) %all-to-all-start.1) | async-done | bytes 294944 | tf_op jit(solution)/shard_map/all_to_all | solution.py:461
  133.8 0.0 collective-permute-done.3.other_hbm
  133.8 0.7 copy-done.2
  134.5 10.5 %expert.1 = (bf16[32,4,2048]{2,1,0:T(4,128)(2,1)}, bf16[16,2048]{1,0:T(8,128)(2,1)}) custom-call(s32[1]{0:T(128)} %bitcast.core_ref, bf16[32,4,1152]{2,1,0:T(4,128)(2,1)} %copy-done.2, bf16[16,1024]{1,0:T(8,128)(2,1)} %get-tuple-element.13.own_ref, bf16[16,2048]{1,0:T(8,128)(2,1)} %tok_ref.1, bf16[1,2048]{1,0:T(2,128)(2,1)} %reshape.44.gain_ref, ...), custom_call_target="tpu_custom_call" | custom-call | tf_op jit(solution)/shard_map/expert/pallas_call | solution.py:361
  145.1 5.7 %all-to-all-start.2 = ((bf16[32,4,2048]{2,1,0:T(4,128)(2,1)}), bf16[32,4,2048]{2,1,0:T(4,128)(2,1)S(1)}, u32[]{:S(2)}, u32[]{:S(2)}) async-start(bf16[32,4,2048]{2,1,0:T(4,128)(2,1)} %get-tuple-element.15), calls=%async_computation.2 | async-start | bytes 1048576 | tf_op jit(solution)/shard_map/all_to_all | solution.py:477
  150.7 0.1 select_reduce_fusion.share_ref
  150.8 32.0 %all-to-all-done.2.rows_ref = bf16[32,4,2048]{2,1,0:T(4,128)(2,1)S(1)} async-done(((bf16[32,4,2048]{2,1,0:T(4,128)(2,1)}), bf16[32,4,2048]{2,1,0:T(4,128)(2,1)S(1)}, u32[]{:S(2)}, u32[]{:S(2)}) %all-to-all-start.2) | async-done | bytes 524320 | tf_op jit(solution)/shard_map/all_to_all | solution.py:477
  182.8 0.8 copy-done.1
  183.7 1.0 combine.1
  (20 shorter events, 0.1 us)
Async XLA Ops:
  6.5 56.5 %copy-start = (bf16[2048,256]{1,0:T(8,128)(2,1)S(1)}, bf16[2048,256]{1,0:T(8,128)(2,1)}, u32[]{:S(2)}) copy-start(bf16[2048,256]{1,0:T(8,128)(2,1)} %param.21) | copy-start | bytes 3145732
  6.6 61.0 %copy-start.4 = (bf16[2048,32]{0,1:T(8,128)(2,1)S(1)}, bf16[2048,32]{0,1:T(8,128)(2,1)}, u32[]{:S(2)}) copy-start(bf16[2048,32]{0,1:T(8,128)(2,1)} %param.19) | copy-start | bytes 393220
  6.6 96.6 %all-gather.3.cloned.1.call-start = ((), (), s32[]{:S(2)}) async-start(), calls=%async_computation.3 | async-start | bytes 3342336 | tf_op jit(solution)/shard_map/all_gather | solution.py:432
  9.1 57.5 %collective-permute-start = (bf16[2048,32]{0,1:T(8,128)(2,1)}, bf16[2048,32]{0,1:T(8,128)(2,1)S(1)}, u32[]{:S(2)}, u32[]{:S(2)}) collective-permute-start(bf16[2048,32]{0,1:T(8,128)(2,1)} %param.19), channel_id=1, source_target_pairs={{0,24},{8,0},{16,8},{24,16},{1,25},{9,1},{17,9},{25,17},{2,26},{10... | collective-permute-start | bytes 393224 | tf_op jit(solution)/shard_map/ppermute | solution.py:37
  21.6 45.4 %collective-permute-start.1 = (bf16[2048,32]{0,1:T(8,128)(2,1)}, bf16[2048,32]{0,1:T(8,128)(2,1)S(1)}, u32[]{:S(2)}, u32[]{:S(2)}) collective-permute-start(bf16[2048,32]{0,1:T(8,128)(2,1)} %param.19), channel_id=1, source_target_pairs={{0,16},{8,24},{16,0},{24,8},{1,17},{9,25},{17,1},{25,9},{2,18},{10... | collective-permute-start | bytes 393224 | tf_op jit(solution)/shard_map/ppermute | solution.py:37
  23.9 43.3 %collective-permute-start.2 = (bf16[2048,32]{0,1:T(8,128)(2,1)}, bf16[2048,32]{0,1:T(8,128)(2,1)S(1)}, u32[]{:S(2)}, u32[]{:S(2)}) collective-permute-start(bf16[2048,32]{0,1:T(8,128)(2,1)} %param.19), channel_id=1, source_target_pairs={{0,8},{8,16},{16,24},{24,0},{1,9},{9,17},{17,25},{25,1},{2,10},{10... | collective-permute-start | bytes 393224 | tf_op jit(solution)/shard_map/ppermute | solution.py:37
  68.9 10.0 %all-to-all-start = ((bf16[8,16,128]{2,1,0:T(8,128)(2,1)}), bf16[8,16,128]{2,1,0:T(8,128)(2,1)S(1)}, u32[]{:S(2)}, u32[]{:S(2)}) async-start(bf16[8,16,128]{2,1,0:T(8,128)(2,1)} %reshape.40), calls=%async_computation | async-start | bytes 65536 | tf_op jit(solution)/shard_map/all_to_all | solution.py:54
  78.9 0.6 copy-start.3
  79.5 32.1 %copy-start.5 = (bf16[2048]{0:T(1024)(128)(2,1)S(1)}, bf16[2048]{0:T(1024)(128)(2,1)}, u32[]{:S(2)}) copy-start(bf16[2048]{0:T(1024)(128)(2,1)} %param.28) | copy-start | bytes 12292
  103.2 30.6 %collective-permute-start.3 = (bf16[16,96,1024]{2,1,0:T(8,128)(2,1)}, bf16[16,96,1024]{2,1,0:T(8,128)(2,1)}, u32[]{:S(2)}, u32[]{:S(2)}) collective-permute-start(bf16[16,96,1024]{2,1,0:T(8,128)(2,1)} %bitcast.31), channel_id=1, source_target_pairs={{0,1},{1,0},{2,3},{3,2},{4,5},{5,4},{6,7},{7,6},{8,9},{9,8},{10,11... | collective-permute-start | bytes 9437192 | tf_op jit(solution)/shard_map/ppermute | solution.py:463
  103.2 30.6 %all-to-all-start.1 = ((bf16[32,4,1152]{2,1,0:T(4,128)(2,1)}), bf16[32,4,1152]{2,1,0:T(4,128)(2,1)S(1)}, u32[]{:S(2)}, u32[]{:S(2)}) async-start(bf16[32,4,1152]{2,1,0:T(4,128)(2,1)} %get-tuple-element.11), calls=%async_computation.1 | async-start | bytes 589824 | tf_op jit(solution)/shard_map/all_to_all | solution.py:461
  133.8 0.7 copy-start.2
  134.5 16.2 %copy-start.6 = (f32[16,4]{0,1:T(4,128)S(1)}, f32[16,4]{0,1:T(4,128)}, u32[]{:S(2)}) copy-start(f32[16,4]{0,1:T(4,128)} %param.33) | copy-start | bytes 772
  145.1 37.8 %all-to-all-start.2 = ((bf16[32,4,2048]{2,1,0:T(4,128)(2,1)}), bf16[32,4,2048]{2,1,0:T(4,128)(2,1)S(1)}, u32[]{:S(2)}, u32[]{:S(2)}) async-start(bf16[32,4,2048]{2,1,0:T(4,128)(2,1)} %get-tuple-element.15), calls=%async_computation.2 | async-start | bytes 1048576 | tf_op jit(solution)/shard_map/all_to_all | solution.py:477
  182.8 0.8 copy-start.1
Sparse Core Ops, SparseCore 0:
  9.2 93.9 all-gather.2

commit v5 on v4

--- a/solution.py
+++ b/solution.py
@@ -30,29 +30,18 @@
     )
 
 
-def far_blocks(block):
-    size = lax.axis_size("far")
-    out = [block]
-    for d in range(1, size):
-        out.append(lax.ppermute(block, "far", [(i, (i + d) % size) for i in range(size)]))
-    return out
-
-
-def near_product(rows, blocks):
+def query_exchange(normed, query_weight):
     members = lax.axis_size(NEAR)
-    size = len(blocks)
-    here = lax.axis_index("far")
-    cols = blocks[0].shape[1]
-    count = rows.shape[0] // members
-    parts = [
-        jnp.dot(rows, block, preferred_element_type=jnp.float32).astype(jnp.bfloat16)
-        for block in blocks
-    ]
-    stacked = jnp.stack(parts[::-1] + parts[::-1])
-    placed = lax.dynamic_slice_in_dim(stacked, size - 1 - here, size, axis=0)
-    outgoing = jnp.transpose(placed.reshape(size, members, count, cols), (1, 2, 0, 3))
+    blocks = [query_weight.T]
+    for d in range(1, members):
+        blocks.append(lax.ppermute(query_weight.T, NEAR, [(i, i ^ d) for i in range(members)]))
+    rows = lax.all_gather(normed, "far", axis=0, tiled=True)
+    held = jnp.concatenate(blocks, axis=0)
+    part = lax.dot_general(
+        rows, held, (((1,), (1,)), ((), ())), preferred_element_type=jnp.float32
+    ).astype(jnp.bfloat16)
     return lax.all_to_all(
-        outgoing.reshape(members, count, size * cols), NEAR, 0, 0, tiled=True
+        part.reshape(lax.axis_size("far"), normed.shape[0], held.shape[0]), "far", 0, 0, tiled=True
     )
 
 
@@ -67,7 +56,7 @@
 
 
 def attention_kernel(
-    group_size, chunk, shard, lens_ref, lam_ref, r_ref, nk_ref, nv_ref, gain_ref, disp_ref, k_hbm, v_hbm,
+    group_size, chunk, shard, member_ref, lens_ref, lam_ref, r_ref, nk_ref, nv_ref, gain_ref, disp_ref, k_hbm, v_hbm,
     o_ref, out_ref, k_buf, v_buf, s_buf, q_buf, k_sem, v_sem,
 ):
     count, heads, width = q_buf.shape
@@ -78,8 +67,6 @@
     chunk_rows = chunk * kv_count
     chunks = rows // chunk_rows
     inv_scale = half ** (-0.5)
-    channels = shard
-    far_heads = width // channels
 
     def piece(c):
         return pl.ds(pl.multiple_of(c * chunk_rows, chunk_rows), chunk_rows)
@@ -111,16 +98,20 @@
 
     lax.fori_loop(0, count, fetch, 0)
 
+    member = member_ref[0]
+    place = lax.broadcasted_iota(jnp.int32, (count, width), 1) // shard
     for h in range(heads):
-        parts = []
-        for m in range(far_heads):
-            piece_at = (h * far_heads + m) // r_ref.shape[0] * channels
-            parts.append(
-                r_ref[(h * far_heads + m) % r_ref.shape[0]].astype(jnp.float32)[
-                    :, piece_at : piece_at + channels
-                ]
+        head = r_ref[h].astype(jnp.float32)
+        bit = 1
+        while bit * shard < width:
+            turned = jnp.where(
+                (place // bit) % 2 == 0,
+                pltpu.roll(head, width - bit * shard, 1),
+                pltpu.roll(head, bit * shard, 1),
             )
-        q_buf[:, h, :] = jnp.concatenate(parts, axis=1)
+            head = jnp.where((member // bit) % 2 == 1, turned, head)
+            bit *= 2
+        q_buf[:, h, :] = head
 
     lane = lax.broadcasted_iota(jnp.int32, (heads, width), 1)
     head_row = lax.broadcasted_iota(jnp.int32, (heads, width), 0)
@@ -222,7 +213,7 @@
             jax.ShapeDtypeStruct((count, heads * width), jnp.bfloat16),
             jax.ShapeDtypeStruct((experts, slots // experts, heads * width + lanes), jnp.bfloat16),
         ),
-        in_specs=[smem, smem, vmem, vmem, vmem, vmem, vmem, hbm, hbm],
+        in_specs=[smem, smem, smem, vmem, vmem, vmem, vmem, vmem, hbm, hbm],
         out_specs=(vmem, vmem),
         scratch_shapes=[
             pltpu.VMEM((count, rows, width), jnp.bfloat16),
@@ -232,9 +223,10 @@
             pltpu.SemaphoreType.DMA((count,)),
             pltpu.SemaphoreType.DMA((count,)),
         ],
-        compiler_params=pltpu.CompilerParams(vmem_limit_bytes=56 * 2**20),
+        compiler_params=pltpu.CompilerParams(vmem_limit_bytes=53 * 2**20),
         name="attention",
     )(
+        lax.axis_index(NEAR).astype(jnp.int32).reshape(1),
         lengths,
         lambdas,
         queries,
@@ -378,7 +370,7 @@
             pltpu.SemaphoreType.DMA,
             pltpu.SemaphoreType.DMA((pieces,)),
         ],
-        compiler_params=pltpu.CompilerParams(vmem_limit_bytes=60 * 2**20),
+        compiler_params=pltpu.CompilerParams(vmem_limit_bytes=50 * 2**20),
         name="expert",
     )(core, received, head_out, tokens, moe_gain.reshape(1, width), near, other, gate_w, up_w, down_w)
 
@@ -430,14 +422,12 @@
     depth = out_weight.shape[0]
     packed = jnp.concatenate([out_weight.T, tokens[:, :depth], tokens[:, depth:]], axis=0)
     near_packed = lax.all_gather(packed, CHIPS, axis=0)
-    query_blocks = far_blocks(query_weight)
     normed = rms_scaled(tokens, norm_gain).astype(jnp.bfloat16)
+    queries = query_exchange(normed, query_weight)
     new_keys = jnp.dot(normed, key_weight, preferred_element_type=jnp.float32).astype(jnp.bfloat16)
     new_values = jnp.dot(normed, value_weight, preferred_element_type=jnp.float32).astype(
         jnp.bfloat16
     )
-    near_normed = lax.all_gather(normed, NEAR, axis=0, tiled=True)
-    queries = near_product(near_normed, query_blocks)
     experts = lax.axis_size(EP)
     capacity = min(count, max(2, 2 * count * topk // experts))
     onehot = (routes.reshape(-1)[:, None] == jnp.arange(experts, dtype=jnp.int32)[None, :]).astype(
@@ -479,7 +469,7 @@
 
 
 def solution(mesh):
-    devices = mesh.devices.reshape(mesh.shape["grp"], -1, 4, 2)
+    devices = mesh.devices.reshape(mesh.shape["grp"], -1, 2, 2)
     torus = Mesh(devices, ("grp", "far", "near", "core"))
     return jax.shard_map(
         local,

time: 195 us -> 181 us (0.928)
  starting transfers between devices: 39.8 us -> 29.4 us
  blocking collectives: 29.4 us -> 33.3 us
  local copies, waits for them, and re-layouts: 5.83 us -> 2.04 us
  waiting for transfers between devices: 72.7 us -> 69 us
    all_gather x1, waiting for transfers between devices: 15.1 us -> 1.84 us  [local(): near_packed = lax.all_gather(packed, CHIPS, axis=0)]
    ppermute x3, starting transfers between devices: 20.6 us -> 8.64 us  [query_exchange(): lax.ppermute(query_weight.T, NEAR, [(i, i ^ d) for i in range(members)])]
    all_to_all x1, waiting for transfers between devices: 3.96 us -> 12.9 us  [query_exchange(): lax.all_to_all(part.reshape(lax.axis_size('far'), normed.shape[0], held.s...]
    all_gather x1, blocking collectives: 29.4 us -> 33.3 us  [query_exchange(): rows = lax.all_gather(normed, 'far', axis=0, tiled=True)]
    unnamed x18 -> x15, local copies, waits for them, and re-layouts: 2.98 us -> 0.79 us
  transfers between devices with their start and end apart: 8 -> 8, of which waited for: 4 -> 4; matrix products, arithmetic and copies ran while one was open for 6% -> 5% of each run, Pallas kernels for 4% -> 5%
where the time goes in v5:
time: 181 us; the launch traced here: 178 us
  waiting for transfers between devices  69 us (38%)
  blocking collectives  33.3 us (18%)
  starting transfers between devices  29.4 us (16%)
  Pallas kernels  21.3 us (12%)
  between operations  13.6 us (8%)
  other arithmetic  5.42 us (3%)
  matrix products  3.56 us (2%)
  local copies, waits for them, and re-layouts  2.04 us (1%)
    all_gather x1, blocking collectives, query_exchange(): rows = lax.all_gather(normed, 'far', axis=0, tiled=True)  33.3 us
    all_to_all x1, waiting for transfers between devices, local(): lax.all_to_all(results, EP, split_axis=0, concat_axis=0, tiled=True)  32 us
    all_to_all x1, waiting for transfers between devices, local(): lax.all_to_all(outgoing, EP, split_axis=0, concat_axis=0, tiled=True)  22.2 us
    all_to_all x1, waiting for transfers between devices, query_exchange(): lax.all_to_all(part.reshape(lax.axis_size('far'), normed.shape[0], held.s...  12.9 us
    pallas_call x1, Pallas kernels, expert(): pl.pallas_call(expert_kernel, out_shape=(jax.ShapeDtypeStruct((members, p...  12 us
    ppermute x3, starting transfers between devices, query_exchange(): lax.ppermute(query_weight.T, NEAR, [(i, i ^ d) for i in range(members)])  8.64 us
    pallas_call x1, Pallas kernels, attention(): pl.pallas_call(functools.partial(attention_kernel, together, 128, shard),...  8.33 us
    all_to_all x1, starting transfers between devices, local(): lax.all_to_all(outgoing, EP, split_axis=0, concat_axis=0, tiled=True)  8.19 us
  transfers between devices with their start and end apart: 8, of which 4 were waited for; matrix products, arithmetic and copies ran while one was open for 5% of the time, Pallas kernels for 5%

profile of v5, /device:TPU:196, one launch (start us, length us, event | category | flops | bytes accessed | tf_op | source)
XLA Modules:
  0.0 177.6 jit_solution(4534139093768913510)
XLA Ops:
  6.5 0.0 copy-start
  6.6 0.1 all-gather.3.cloned.1.call-start
  6.6 0.9 fusion.13
  7.5 1.6 pad_maximum_fusion
  9.1 0.1 all-gather.3.cloned.1.call-update
  9.1 0.1 collective-permute-start
  9.3 8.5 %collective-permute-start.1 = (bf16[32,2048]{1,0:T(8,128)(2,1)}, bf16[32,2048]{1,0:T(8,128)(2,1)S(1)}, u32[]{:S(2)}, u32[]{:S(2)}) collective-permute-start(bf16[32,2048]{1,0:T(8,128)(2,1)} %bitcast.21), channel_id=1, source_target_pairs={{0,2},{1,3},{2,0},{3,1},{4,6},{5,7},{6,4},{7,5},{8,10},{9,11},{10,... | collective-permute-start | bytes 393224 | tf_op jit(solution)/shard_map/ppermute | solution.py:37
  17.8 0.0 collective-permute-start.2
  17.8 0.7 convert_element_type.26
  18.5 0.8 copy.29
  19.2 0.1 eq.20
  19.3 0.1 fusion.10
  19.4 0.1 reduce_window_sum.11
  19.5 0.2 select_reduce_fusion.1
  19.7 0.1 reshape.37
  19.8 0.1 copy.30
  19.9 1.0 fusion.7
  20.8 0.9 fusion.9
  21.8 33.3 %all_gather.9 = bf16[128,2048]{1,0:T(8,128)(2,1)S(1)} all-gather(bf16[16,2048]{1,0:T(8,128)(2,1)S(1)} %fusion.9), channel_id=1, replica_groups=mesh['grp'=4,'far'=8,'near'=2,'core'=2] {'far'}, dimensions={0}, use_global_device_ids=true | all-gather | bytes 589824 | tf_op jit(solution)/shard_map/all_gather | solution.py:38
  55.1 0.0 copy-done
  55.1 0.2 convolution_convert_fusion.1.nv_ref
  55.4 1.5 convolution_convert_fusion.2.nk_ref
  56.8 0.7 multiply_add_fusion
  57.5 0.0 collective-permute-done
  57.5 0.0 collective-permute-done.1
  57.5 0.0 collective-permute-done.2
  57.5 1.8 %convolution_convert_fusion = bf16[128,128]{1,0:T(8,128)(2,1)} fusion(bf16[128,2048]{1,0:T(8,128)(2,1)S(1)} %all_gather.9, bf16[32,2048]{1,0:T(8,128)(2,1)S(1)} %collective-permute-done.2, bf16[32,2048]{1,0:T(8,128)(2,1)S(1)} %collective-permute-done.1, bf16[32,2048]{1,0:T(8,128)(2,1)S(1)} %collective-permute-done, bf16[32,2048]{1,0:T(8,128)(2,1)} %bitcast.23), kind=kOutput, calls=%fused_computation | convolution fusion | flops 69222400 | bytes 1081344 | tf_op jit(solution)/shard_map/dot_general | solution.py:40
  59.4 6.9 %all-to-all-start = ((bf16[8,16,128]{2,1,0:T(8,128)(2,1)}), bf16[8,16,128]{2,1,0:T(8,128)(2,1)S(1)}, u32[]{:S(2)}, u32[]{:S(2)}) async-start(bf16[8,16,128]{2,1,0:T(8,128)(2,1)} %bitcast.3), calls=%async_computation | async-start | bytes 65536 | tf_op jit(solution)/shard_map/all_to_all | solution.py:43
  66.2 0.1 fusion.11
  66.3 0.1 copy.31
  66.5 12.9 %all-to-all-done.r_ref = bf16[8,16,128]{2,1,0:T(8,128)(2,1)S(1)} async-done(((bf16[8,16,128]{2,1,0:T(8,128)(2,1)}), bf16[8,16,128]{2,1,0:T(8,128)(2,1)S(1)}, u32[]{:S(2)}, u32[]{:S(2)}) %all-to-all-start) | async-done | bytes 32800 | tf_op jit(solution)/shard_map/all_to_all | solution.py:43
  79.4 0.0 copy-done.4
  79.4 0.0 copy-done.3
  79.4 0.0 copy-done.2
  79.4 0.0 copy-start.5
  79.4 0.0 copy-start.1
  79.5 8.3 %attention.1 = (bf16[16,1024]{1,0:T(8,128)(2,1)S(1)}, bf16[32,4,1152]{2,1,0:T(4,128)(2,1)}) custom-call(s32[1]{0:T(128)} %bitcast.1.member_ref, s32[16]{0:T(128)S(1)} %copy-done.2, f32[8]{0:T(128)S(1)} %copy-done.3, bf16[8,16,128]{2,1,0:T(8,128)(2,1)S(1)} %all-to-all-done.r_ref, bf16[16,256]{1,0:T(8,128)(2,1)S(1)} %convolution_convert_fusion.2.nk_ref, ...), custom_call_target="tpu_custom_call" | custom-call | tf_op jit(solution)/shard_map/attention/pallas_call | solution.py:210
  87.8 1.8 %all-gather.3.cloned.1.call-done = bf16[1536,1024]{1,0:T(8,128)(2,1)} async-done(((bf16[96,1024]{1,0:T(8,128)(2,1)}), bf16[1536,1024]{1,0:T(8,128)(2,1)}) %all-gather.3.cloned.1.call-update) | async-done | bytes 3145744 | tf_op jit(solution)/shard_map/all_gather | solution.py:424
  89.6 0.0 collective-permute-start.3
  89.6 8.2 %all-to-all-start.1 = ((bf16[32,4,1152]{2,1,0:T(4,128)(2,1)}), bf16[32,4,1152]{2,1,0:T(4,128)(2,1)S(1)}, u32[]{:S(2)}, u32[]{:S(2)}) async-start(bf16[32,4,1152]{2,1,0:T(4,128)(2,1)} %get-tuple-element.11), calls=%async_computation.1 | async-start | bytes 589824 | tf_op jit(solution)/shard_map/all_to_all | solution.py:451
  97.9 22.2 %all-to-all-done.1.h_ref = bf16[32,4,1152]{2,1,0:T(4,128)(2,1)S(1)} async-done(((bf16[32,4,1152]{2,1,0:T(4,128)(2,1)}), bf16[32,4,1152]{2,1,0:T(4,128)(2,1)S(1)}, u32[]{:S(2)}, u32[]{:S(2)}) %all-to-all-start.1) | async-done | bytes 294944 | tf_op jit(solution)/shard_map/all_to_all | solution.py:451
  120.1 0.0 collective-permute-done.3.other_hbm
  120.1 12.0 %expert.1 = (bf16[32,4,2048]{2,1,0:T(4,128)(2,1)}, bf16[16,2048]{1,0:T(8,128)(2,1)S(1)}) custom-call(s32[1]{0:T(128)} %bitcast.core_ref, bf16[32,4,1152]{2,1,0:T(4,128)(2,1)S(1)} %all-to-all-done.1.h_ref, bf16[16,1024]{1,0:T(8,128)(2,1)S(1)} %get-tuple-element.13.own_ref, bf16[16,2048]{1,0:T(8,128)(2,1)S(1)} %copy-done.1, ...), custom_call_target="tpu_custom_call" | custom-call | tf_op jit(solution)/shard_map/expert/pallas_call | solution.py:353
  132.0 5.7 %all-to-all-start.2 = ((bf16[32,4,2048]{2,1,0:T(4,128)(2,1)}), bf16[32,4,2048]{2,1,0:T(4,128)(2,1)S(1)}, u32[]{:S(2)}, u32[]{:S(2)}) async-start(bf16[32,4,2048]{2,1,0:T(4,128)(2,1)} %get-tuple-element.15), calls=%async_computation.2 | async-start | bytes 1048576 | tf_op jit(solution)/shard_map/all_to_all | solution.py:467
  137.7 0.0 copy-done.6
  137.7 0.1 select_reduce_fusion.share_ref
  137.8 32.0 %all-to-all-done.2.rows_ref = bf16[32,4,2048]{2,1,0:T(4,128)(2,1)S(1)} async-done(((bf16[32,4,2048]{2,1,0:T(4,128)(2,1)}), bf16[32,4,2048]{2,1,0:T(4,128)(2,1)S(1)}, u32[]{:S(2)}, u32[]{:S(2)}) %all-to-all-start.2) | async-done | bytes 524320 | tf_op jit(solution)/shard_map/all_to_all | solution.py:467
  169.8 1.0 combine.1
  (9 shorter events, 0.0 us)
Async XLA Ops:
  6.5 48.6 %copy-start = (bf16[2048,256]{1,0:T(8,128)(2,1)S(1)}, bf16[2048,256]{1,0:T(8,128)(2,1)}, u32[]{:S(2)}) copy-start(bf16[2048,256]{1,0:T(8,128)(2,1)} %param.21) | copy-start | bytes 3145732
  6.6 72.9 %copy-start.4 = (bf16[128]{0:T(256)(128)(2,1)S(1)}, bf16[128]{0:T(256)(128)(2,1)}, u32[]{:S(2)}) copy-start(bf16[128]{0:T(256)(128)(2,1)} %param.23) | copy-start | bytes 772
  6.6 72.9 %copy-start.3 = (f32[8]{0:T(128)S(1)}, f32[8]{0:T(128)}, u32[]{:S(2)}) copy-start(f32[8]{0:T(128)} %lam_ref.1) | copy-start | bytes 100
  6.6 72.9 %copy-start.2 = (s32[16]{0:T(128)S(1)}, s32[16]{0:T(128)}, u32[]{:S(2)}) copy-start(s32[16]{0:T(128)} %lens_ref.1) | copy-start | bytes 196
  6.6 83.1 %all-gather.3.cloned.1.call-start = ((), (), s32[]{:S(2)}) async-start(), calls=%async_computation.3 | async-start | bytes 3342336 | tf_op jit(solution)/shard_map/all_gather | solution.py:424
  9.1 48.4 %collective-permute-start = (bf16[32,2048]{1,0:T(8,128)(2,1)}, bf16[32,2048]{1,0:T(8,128)(2,1)S(1)}, u32[]{:S(2)}, u32[]{:S(2)}) collective-permute-start(bf16[32,2048]{1,0:T(8,128)(2,1)} %bitcast.20), channel_id=1, source_target_pairs={{0,1},{1,0},{2,3},{3,2},{4,5},{5,4},{6,7},{7,6},{8,9},{9,8},{10,11... | collective-permute-start | bytes 393224 | tf_op jit(solution)/shard_map/ppermute | solution.py:37
  9.3 48.2 %collective-permute-start.1 = (bf16[32,2048]{1,0:T(8,128)(2,1)}, bf16[32,2048]{1,0:T(8,128)(2,1)S(1)}, u32[]{:S(2)}, u32[]{:S(2)}) collective-permute-start(bf16[32,2048]{1,0:T(8,128)(2,1)} %bitcast.21), channel_id=1, source_target_pairs={{0,2},{1,3},{2,0},{3,1},{4,6},{5,7},{6,4},{7,5},{8,10},{9,11},{10,... | collective-permute-start | bytes 393224 | tf_op jit(solution)/shard_map/ppermute | solution.py:37
  17.8 39.8 %collective-permute-start.2 = (bf16[32,2048]{1,0:T(8,128)(2,1)}, bf16[32,2048]{1,0:T(8,128)(2,1)S(1)}, u32[]{:S(2)}, u32[]{:S(2)}) collective-permute-start(bf16[32,2048]{1,0:T(8,128)(2,1)} %bitcast.22), channel_id=1, source_target_pairs={{0,3},{1,2},{2,1},{3,0},{4,7},{5,6},{6,5},{7,4},{8,11},{9,10},{10,... | collective-permute-start | bytes 393224 | tf_op jit(solution)/shard_map/ppermute | solution.py:37
  59.4 20.0 %all-to-all-start = ((bf16[8,16,128]{2,1,0:T(8,128)(2,1)}), bf16[8,16,128]{2,1,0:T(8,128)(2,1)S(1)}, u32[]{:S(2)}, u32[]{:S(2)}) async-start(bf16[8,16,128]{2,1,0:T(8,128)(2,1)} %bitcast.3), calls=%async_computation | async-start | bytes 65536 | tf_op jit(solution)/shard_map/all_to_all | solution.py:43
  79.4 18.4 %copy-start.5 = (bf16[2048]{0:T(1024)(128)(2,1)S(1)}, bf16[2048]{0:T(1024)(128)(2,1)}, u32[]{:S(2)}) copy-start(bf16[2048]{0:T(1024)(128)(2,1)} %param.28) | copy-start | bytes 12292
  79.4 40.6 %copy-start.1 = (bf16[16,2048]{1,0:T(8,128)(2,1)S(1)}, bf16[16,2048]{1,0:T(8,128)(2,1)}, u32[]{:S(2)}) copy-start(bf16[16,2048]{1,0:T(8,128)(2,1)} %tok_ref.1) | copy-start | bytes 196612
  89.6 30.4 %collective-permute-start.3 = (bf16[16,96,1024]{2,1,0:T(8,128)(2,1)}, bf16[16,96,1024]{2,1,0:T(8,128)(2,1)}, u32[]{:S(2)}, u32[]{:S(2)}) collective-permute-start(bf16[16,96,1024]{2,1,0:T(8,128)(2,1)} %bitcast.17), channel_id=1, source_target_pairs={{0,1},{1,0},{2,3},{3,2},{4,5},{5,4},{6,7},{7,6},{8,9},{9,8},{10,11... | collective-permute-start | bytes 9437192 | tf_op jit(solution)/shard_map/ppermute | solution.py:453
  89.6 30.4 %all-to-all-start.1 = ((bf16[32,4,1152]{2,1,0:T(4,128)(2,1)}), bf16[32,4,1152]{2,1,0:T(4,128)(2,1)S(1)}, u32[]{:S(2)}, u32[]{:S(2)}) async-start(bf16[32,4,1152]{2,1,0:T(4,128)(2,1)} %get-tuple-element.11), calls=%async_computation.1 | async-start | bytes 589824 | tf_op jit(solution)/shard_map/all_to_all | solution.py:451
  120.1 17.7 %copy-start.6 = (f32[16,4]{0,1:T(4,128)S(1)}, f32[16,4]{0,1:T(4,128)}, u32[]{:S(2)}) copy-start(f32[16,4]{0,1:T(4,128)} %param.33) | copy-start | bytes 772
  132.0 37.8 %all-to-all-start.2 = ((bf16[32,4,2048]{2,1,0:T(4,128)(2,1)}), bf16[32,4,2048]{2,1,0:T(4,128)(2,1)S(1)}, u32[]{:S(2)}, u32[]{:S(2)}) async-start(bf16[32,4,2048]{2,1,0:T(4,128)(2,1)} %get-tuple-element.15), calls=%async_computation.2 | async-start | bytes 1048576 | tf_op jit(solution)/shard_map/all_to_all | solution.py:467
Sparse Core Ops, SparseCore 0:
  9.3 80.3 all-gather.2

commit v6 on v5

--- a/solution.py
+++ b/solution.py
@@ -30,18 +30,46 @@
     )
 
 
-def query_exchange(normed, query_weight):
+def query_kernel(place_ref, rows_ref, gain_ref, *refs):
+    *block_refs, part_ref, own_ref = refs
+    count = own_ref.shape[0]
+    normed = rms_scaled(rows_ref[...], gain_ref[...]).astype(jnp.bfloat16)
+    held = jnp.concatenate([ref[...] for ref in block_refs], axis=0)
+    part = lax.dot_general(
+        normed, held, (((1,), (1,)), ((), ())), preferred_element_type=jnp.float32
+    ).astype(part_ref.dtype)
+    own = rows_ref[pl.ds(pl.multiple_of(place_ref[0] * count, count), count)]
+    own_ref[...] = rms_scaled(own, gain_ref[...]).astype(own_ref.dtype)
+    for i in range(part_ref.shape[0]):
+        part_ref[i] = part[i * count : (i + 1) * count]
+
+
+def query_product(tokens, norm_gain, query_weight):
+    count, width = tokens.shape
     members = lax.axis_size(NEAR)
-    blocks = [query_weight.T]
+    shard = query_weight.T
+    blocks = [shard]
     for d in range(1, members):
-        blocks.append(lax.ppermute(query_weight.T, NEAR, [(i, i ^ d) for i in range(members)]))
-    rows = lax.all_gather(normed, "far", axis=0, tiled=True)
-    held = jnp.concatenate(blocks, axis=0)
-    part = lax.dot_general(
-        rows, held, (((1,), (1,)), ((), ())), preferred_element_type=jnp.float32
-    ).astype(jnp.bfloat16)
-    return lax.all_to_all(
-        part.reshape(lax.axis_size("far"), normed.shape[0], held.shape[0]), "far", 0, 0, tiled=True
+        blocks.append(lax.ppermute(shard, NEAR, [(i, i ^ d) for i in range(members)]))
+    rows = lax.all_gather(tokens, "far", axis=0, tiled=True)
+    far = lax.axis_size("far")
+    vmem = pl.BlockSpec(memory_space=pltpu.VMEM)
+    smem = pl.BlockSpec(memory_space=pltpu.SMEM)
+    return pl.pallas_call(
+        query_kernel,
+        out_shape=(
+            jax.ShapeDtypeStruct((far, count, members * shard.shape[0]), jnp.bfloat16),
+            jax.ShapeDtypeStruct((count, width), jnp.bfloat16),
+        ),
+        in_specs=[smem] + [vmem] * (2 + members),
+        out_specs=(vmem, vmem),
+        compiler_params=pltpu.CompilerParams(vmem_limit_bytes=50 * 2**20),
+        name="query",
+    )(
+        lax.axis_index("far").astype(jnp.int32).reshape(1),
+        rows,
+        norm_gain.reshape(1, width),
+        *blocks,
     )
 
 
@@ -422,29 +450,30 @@
     depth = out_weight.shape[0]
     packed = jnp.concatenate([out_weight.T, tokens[:, :depth], tokens[:, depth:]], axis=0)
     near_packed = lax.all_gather(packed, CHIPS, axis=0)
-    normed = rms_scaled(tokens, norm_gain).astype(jnp.bfloat16)
-    queries = query_exchange(normed, query_weight)
+    part, normed = query_product(tokens, norm_gain, query_weight)
+    queries = lax.all_to_all(part, "far", 0, 0, tiled=True)
     new_keys = jnp.dot(normed, key_weight, preferred_element_type=jnp.float32).astype(jnp.bfloat16)
     new_values = jnp.dot(normed, value_weight, preferred_element_type=jnp.float32).astype(
         jnp.bfloat16
     )
     experts = lax.axis_size(EP)
     capacity = min(count, max(2, 2 * count * topk // experts))
-    onehot = (routes.reshape(-1)[:, None] == jnp.arange(experts, dtype=jnp.int32)[None, :]).astype(
-        jnp.int32
-    )
+    routes, new_keys = lax.optimization_barrier((routes, new_keys))
+    slot_range = jnp.arange(experts * capacity, dtype=jnp.int32)
+    onehot = (
+        routes.reshape(-1)[:, None] == jnp.arange(experts, dtype=jnp.int32)[None, :]
+    ).astype(jnp.int32)
     earlier_all = jnp.cumsum(onehot, axis=0) - onehot
     ranks = jnp.sum(earlier_all * onehot, axis=1).reshape(count, topk)
     slot_id = routes * capacity + ranks
-    slot_range = jnp.arange(experts * capacity, dtype=jnp.int32)
     dispatch = jnp.any(slot_id[None, :, :] == slot_range[:, None, None], axis=2).astype(
         jnp.bfloat16
     )
+    dispatch = jnp.pad(dispatch, ((0, 0), (0, 128 - count)))
     share = jnp.sum(
         jnp.where(slot_id[:, :, None] == slot_range[None, None, :], route_weights[:, :, None], 0.0),
         axis=1,
     )
-    dispatch = jnp.pad(dispatch, ((0, 0), (0, 128 - count)))
     head_out, outgoing = attention(
         queries, new_keys, new_values, cache_keys, cache_values, lengths, lambdas, head_gain, dispatch, experts
     )

time: 181 us -> 181 us (level)
  other arithmetic: 5.42 us -> 2.82 us
  matrix products: 3.56 us -> 1.73 us
    all_to_all x1, waiting for transfers between devices: 12.9 us -> 10.8 us  [local(): queries = lax.all_to_all(part, 'far', 0, 0, tiled=True)]
    all_gather x1, waiting for transfers between devices: 1.84 us -> 3.9 us  [local(): near_packed = lax.all_gather(packed, CHIPS, axis=0)]
    dot_general x1 -> x0, matrix products: 1.83 us -> none  [query_exchange(): lax.dot_general(rows, held, (((1,), (1,)), ((), ())), preferred_element_t...]
  transfers between devices with their start and end apart: 8 -> 8, of which waited for: 4 -> 4; matrix products, arithmetic and copies ran while one was open for 5% -> 3% of each run, Pallas kernels for 5% -> 5%
where the time goes in v6:
time: 181 us; the launch traced here: 177 us
  waiting for transfers between devices  68.9 us (38%)
  blocking collectives  34.3 us (19%)
  starting transfers between devices  30.1 us (17%)
  Pallas kernels  22.3 us (12%)
  between operations  13.6 us (8%)
  local copies, waits for them, and re-layouts  3.64 us (2%)
  other arithmetic  2.82 us (2%)
    all_gather x1, blocking collectives, query_product(): rows = lax.all_gather(tokens, 'far', axis=0, tiled=True)  34.3 us
    all_to_all x1, waiting for transfers between devices, local(): lax.all_to_all(results, EP, split_axis=0, concat_axis=0, tiled=True)  32 us
    all_to_all x1, waiting for transfers between devices, local(): lax.all_to_all(outgoing, EP, split_axis=0, concat_axis=0, tiled=True)  22.2 us
    pallas_call x1, Pallas kernels, expert(): pl.pallas_call(expert_kernel, out_shape=(jax.ShapeDtypeStruct((members, p...  11.9 us
    all_to_all x1, waiting for transfers between devices, local(): queries = lax.all_to_all(part, 'far', 0, 0, tiled=True)  10.8 us
    ppermute x3, starting transfers between devices, query_product(): lax.ppermute(shard, NEAR, [(i, i ^ d) for i in range(members)])  8.64 us
    all_to_all x1, starting transfers between devices, local(): lax.all_to_all(outgoing, EP, split_axis=0, concat_axis=0, tiled=True)  8.4 us
    pallas_call x1, Pallas kernels, attention(): pl.pallas_call(functools.partial(attention_kernel, together, 128, shard),...  8.34 us
  transfers between devices with their start and end apart: 8, of which 4 were waited for; matrix products, arithmetic and copies ran while one was open for 3% of the time, Pallas kernels for 5%

profile of v6, /device:TPU:196, one launch (start us, length us, event | category | flops | bytes accessed | tf_op | source)
XLA Modules:
  0.0 177.3 jit_solution(9313309853775760231)
XLA Ops:
  6.5 0.0 copy-start
  6.6 0.1 all-gather.3.cloned.1.call-start
  6.6 0.9 fusion.2
  7.5 1.6 pad_maximum_fusion
  9.1 0.1 all-gather.3.cloned.1.call-update
  9.1 0.1 collective-permute-start
  9.3 8.5 %collective-permute-start.1 = (bf16[32,2048]{1,0:T(8,128)(2,1)}, bf16[32,2048]{1,0:T(8,128)(2,1)S(1)}, u32[]{:S(2)}, u32[]{:S(2)}) collective-permute-start(bf16[32,2048]{1,0:T(8,128)(2,1)} %bitcast.14), channel_id=1, source_target_pairs={{0,2},{1,3},{2,0},{3,1},{4,6},{5,7},{6,4},{7,5},{8,10},{9,11},{10,... | collective-permute-start | bytes 393224 | tf_op jit(solution)/shard_map/ppermute | solution.py:53
  17.8 0.0 collective-permute-start.2
  17.8 0.7 reshape.32.gain_ref
  18.5 34.3 %all_gather.9.rows_ref = bf16[128,2048]{1,0:T(8,128)(2,1)S(1)} all-gather(bf16[16,2048]{1,0:T(8,128)(2,1)} %tok_ref.1), channel_id=1, replica_groups=mesh['grp'=4,'far'=8,'near'=2,'core'=2] {'far'}, dimensions={0}, use_global_device_ids=true | all-gather | bytes 589824 | tf_op jit(solution)/shard_map/all_gather | solution.py:54
  52.7 0.0 collective-permute-done.refs_1_
  52.7 0.0 collective-permute-done.1.refs_2_
  52.7 0.0 collective-permute-done.2.refs_3_
  52.8 0.0 copy-start.2
  52.8 0.9 copy-done.2
  53.7 1.1 query.1
  54.7 0.0 copy-done
  54.7 0.2 convolution_convert_fusion.1.nk_ref
  55.0 0.8 copy.29
  55.7 0.1 eq.20
  55.8 0.1 fusion
  55.9 0.1 reduce_window_sum.11
  56.0 0.2 select_reduce_fusion.1
  56.2 0.1 reshape.33
  56.3 0.1 copy.30
  56.4 7.3 %all-to-all-start = ((bf16[8,16,128]{2,1,0:T(8,128)(2,1)}), bf16[8,16,128]{2,1,0:T(8,128)(2,1)S(1)}, u32[]{:S(2)}, u32[]{:S(2)}) async-start(bf16[8,16,128]{2,1,0:T(8,128)(2,1)} %get-tuple-element.17), calls=%async_computation | async-start | bytes 65536 | tf_op jit(solution)/shard_map/all_to_all | solution.py:454
  63.7 0.7 multiply_add_fusion
  64.4 1.5 convolution_convert_fusion.nv_ref
  65.9 0.1 fusion.1
  65.9 0.1 copy.31
  66.1 10.8 %all-to-all-done.r_ref = bf16[8,16,128]{2,1,0:T(8,128)(2,1)S(1)} async-done(((bf16[8,16,128]{2,1,0:T(8,128)(2,1)}), bf16[8,16,128]{2,1,0:T(8,128)(2,1)S(1)}, u32[]{:S(2)}, u32[]{:S(2)}) %all-to-all-start) | async-done | bytes 32800 | tf_op jit(solution)/shard_map/all_to_all | solution.py:454
  76.8 0.0 copy-done.5
  76.9 0.0 copy-done.4
  76.9 0.0 copy-done.3
  76.9 0.0 copy-start.6
  76.9 0.0 copy-start.1
  76.9 8.3 %attention.1 = (bf16[16,1024]{1,0:T(8,128)(2,1)S(1)}, bf16[32,4,1152]{2,1,0:T(4,128)(2,1)}) custom-call(s32[1]{0:T(128)} %bitcast.3.member_ref, s32[16]{0:T(128)S(1)} %copy-done.3, f32[8]{0:T(128)S(1)} %copy-done.4, bf16[8,16,128]{2,1,0:T(8,128)(2,1)S(1)} %all-to-all-done.r_ref, bf16[16,256]{1,0:T(8,128)(2,1)S(1)} %convolution_convert_fusion.1.nk_ref, ...), custom_call_target="tpu_custom_call" | custom-call | tf_op jit(solution)/shard_map/attention/pallas_call | solution.py:238
  85.2 3.9 %all-gather.3.cloned.1.call-done = bf16[1536,1024]{1,0:T(8,128)(2,1)} async-done(((bf16[96,1024]{1,0:T(8,128)(2,1)}), bf16[1536,1024]{1,0:T(8,128)(2,1)}) %all-gather.3.cloned.1.call-update) | async-done | bytes 3145744 | tf_op jit(solution)/shard_map/all_gather | solution.py:452
  89.1 0.0 collective-permute-start.3
  89.1 8.4 %all-to-all-start.1 = ((bf16[32,4,1152]{2,1,0:T(4,128)(2,1)}), bf16[32,4,1152]{2,1,0:T(4,128)(2,1)S(1)}, u32[]{:S(2)}, u32[]{:S(2)}) async-start(bf16[32,4,1152]{2,1,0:T(4,128)(2,1)} %get-tuple-element.19), calls=%async_computation.1 | async-start | bytes 589824 | tf_op jit(solution)/shard_map/all_to_all | solution.py:480
  97.6 22.2 %all-to-all-done.1.h_ref = bf16[32,4,1152]{2,1,0:T(4,128)(2,1)S(1)} async-done(((bf16[32,4,1152]{2,1,0:T(4,128)(2,1)}), bf16[32,4,1152]{2,1,0:T(4,128)(2,1)S(1)}, u32[]{:S(2)}, u32[]{:S(2)}) %all-to-all-start.1) | async-done | bytes 294944 | tf_op jit(solution)/shard_map/all_to_all | solution.py:480
  119.8 0.0 collective-permute-done.3.other_hbm
  119.8 11.9 %expert.1 = (bf16[32,4,2048]{2,1,0:T(4,128)(2,1)}, bf16[16,2048]{1,0:T(8,128)(2,1)S(1)}) custom-call(s32[1]{0:T(128)} %bitcast.2.core_ref, bf16[32,4,1152]{2,1,0:T(4,128)(2,1)S(1)} %all-to-all-done.1.h_ref, bf16[16,1024]{1,0:T(8,128)(2,1)S(1)} %get-tuple-element.21.own_ref, bf16[16,2048]{1,0:T(8,128)(2,1)S(1)} %copy-done.1, ...), custom_call_target="tpu_custom_call" | custom-call | tf_op jit(solution)/shard_map/expert/pallas_call | solution.py:381
  131.7 5.7 %all-to-all-start.2 = ((bf16[32,4,2048]{2,1,0:T(4,128)(2,1)}), bf16[32,4,2048]{2,1,0:T(4,128)(2,1)S(1)}, u32[]{:S(2)}, u32[]{:S(2)}) async-start(bf16[32,4,2048]{2,1,0:T(4,128)(2,1)} %get-tuple-element.23), calls=%async_computation.2 | async-start | bytes 1048576 | tf_op jit(solution)/shard_map/all_to_all | solution.py:496
  137.4 0.0 copy-done.7
  137.4 0.1 select_reduce_fusion.share_ref
  137.5 32.0 %all-to-all-done.2.rows_ref = bf16[32,4,2048]{2,1,0:T(4,128)(2,1)S(1)} async-done(((bf16[32,4,2048]{2,1,0:T(4,128)(2,1)}), bf16[32,4,2048]{2,1,0:T(4,128)(2,1)S(1)}, u32[]{:S(2)}, u32[]{:S(2)}) %all-to-all-start.2) | async-done | bytes 524320 | tf_op jit(solution)/shard_map/all_to_all | solution.py:496
  169.5 1.0 combine.1
  (8 shorter events, 0.0 us)
Async XLA Ops:
  6.5 48.2 %copy-start = (bf16[2048,256]{1,0:T(8,128)(2,1)S(1)}, bf16[2048,256]{1,0:T(8,128)(2,1)}, u32[]{:S(2)}) copy-start(bf16[2048,256]{1,0:T(8,128)(2,1)} %param.20) | copy-start | bytes 3145732
  6.6 70.3 %copy-start.5 = (bf16[128]{0:T(256)(128)(2,1)S(1)}, bf16[128]{0:T(256)(128)(2,1)}, u32[]{:S(2)}) copy-start(bf16[128]{0:T(256)(128)(2,1)} %param.23) | copy-start | bytes 772
  6.6 70.3 %copy-start.4 = (f32[8]{0:T(128)S(1)}, f32[8]{0:T(128)}, u32[]{:S(2)}) copy-start(f32[8]{0:T(128)} %lam_ref.1) | copy-start | bytes 100
  6.6 70.3 %copy-start.3 = (s32[16]{0:T(128)S(1)}, s32[16]{0:T(128)}, u32[]{:S(2)}) copy-start(s32[16]{0:T(128)} %lens_ref.1) | copy-start | bytes 196
  6.6 82.6 %all-gather.3.cloned.1.call-start = ((), (), s32[]{:S(2)}) async-start(), calls=%async_computation.3 | async-start | bytes 3342336 | tf_op jit(solution)/shard_map/all_gather | solution.py:452
  9.1 43.6 %collective-permute-start = (bf16[32,2048]{1,0:T(8,128)(2,1)}, bf16[32,2048]{1,0:T(8,128)(2,1)S(1)}, u32[]{:S(2)}, u32[]{:S(2)}) collective-permute-start(bf16[32,2048]{1,0:T(8,128)(2,1)} %bitcast.13), channel_id=1, source_target_pairs={{0,1},{1,0},{2,3},{3,2},{4,5},{5,4},{6,7},{7,6},{8,9},{9,8},{10,11... | collective-permute-start | bytes 393224 | tf_op jit(solution)/shard_map/ppermute | solution.py:53
  9.3 43.5 %collective-permute-start.1 = (bf16[32,2048]{1,0:T(8,128)(2,1)}, bf16[32,2048]{1,0:T(8,128)(2,1)S(1)}, u32[]{:S(2)}, u32[]{:S(2)}) collective-permute-start(bf16[32,2048]{1,0:T(8,128)(2,1)} %bitcast.14), channel_id=1, source_target_pairs={{0,2},{1,3},{2,0},{3,1},{4,6},{5,7},{6,4},{7,5},{8,10},{9,11},{10,... | collective-permute-start | bytes 393224 | tf_op jit(solution)/shard_map/ppermute | solution.py:53
  17.8 35.0 %collective-permute-start.2 = (bf16[32,2048]{1,0:T(8,128)(2,1)}, bf16[32,2048]{1,0:T(8,128)(2,1)S(1)}, u32[]{:S(2)}, u32[]{:S(2)}) collective-permute-start(bf16[32,2048]{1,0:T(8,128)(2,1)} %bitcast.15), channel_id=1, source_target_pairs={{0,3},{1,2},{2,1},{3,0},{4,7},{5,6},{6,5},{7,4},{8,11},{9,10},{10,... | collective-permute-start | bytes 393224 | tf_op jit(solution)/shard_map/ppermute | solution.py:53
  52.8 0.9 copy-start.2
  56.4 20.5 %all-to-all-start = ((bf16[8,16,128]{2,1,0:T(8,128)(2,1)}), bf16[8,16,128]{2,1,0:T(8,128)(2,1)S(1)}, u32[]{:S(2)}, u32[]{:S(2)}) async-start(bf16[8,16,128]{2,1,0:T(8,128)(2,1)} %get-tuple-element.17), calls=%async_computation | async-start | bytes 65536 | tf_op jit(solution)/shard_map/all_to_all | solution.py:454
  76.9 20.7 %copy-start.6 = (bf16[2048]{0:T(1024)(128)(2,1)S(1)}, bf16[2048]{0:T(1024)(128)(2,1)}, u32[]{:S(2)}) copy-start(bf16[2048]{0:T(1024)(128)(2,1)} %param.28) | copy-start | bytes 12292
  76.9 42.9 %copy-start.1 = (bf16[16,2048]{1,0:T(8,128)(2,1)S(1)}, bf16[16,2048]{1,0:T(8,128)(2,1)}, u32[]{:S(2)}) copy-start(bf16[16,2048]{1,0:T(8,128)(2,1)} %tok_ref.1) | copy-start | bytes 196612
  89.1 30.6 %collective-permute-start.3 = (bf16[16,96,1024]{2,1,0:T(8,128)(2,1)}, bf16[16,96,1024]{2,1,0:T(8,128)(2,1)}, u32[]{:S(2)}, u32[]{:S(2)}) collective-permute-start(bf16[16,96,1024]{2,1,0:T(8,128)(2,1)} %bitcast.20), channel_id=1, source_target_pairs={{0,1},{1,0},{2,3},{3,2},{4,5},{5,4},{6,7},{7,6},{8,9},{9,8},{10,11... | collective-permute-start | bytes 9437192 | tf_op jit(solution)/shard_map/ppermute | solution.py:482
  89.1 30.6 %all-to-all-start.1 = ((bf16[32,4,1152]{2,1,0:T(4,128)(2,1)}), bf16[32,4,1152]{2,1,0:T(4,128)(2,1)S(1)}, u32[]{:S(2)}, u32[]{:S(2)}) async-start(bf16[32,4,1152]{2,1,0:T(4,128)(2,1)} %get-tuple-element.19), calls=%async_computation.1 | async-start | bytes 589824 | tf_op jit(solution)/shard_map/all_to_all | solution.py:480
  119.8 17.6 %copy-start.7 = (f32[16,4]{0,1:T(4,128)S(1)}, f32[16,4]{0,1:T(4,128)}, u32[]{:S(2)}) copy-start(f32[16,4]{0,1:T(4,128)} %param.33) | copy-start | bytes 772
  131.7 37.8 %all-to-all-start.2 = ((bf16[32,4,2048]{2,1,0:T(4,128)(2,1)}), bf16[32,4,2048]{2,1,0:T(4,128)(2,1)S(1)}, u32[]{:S(2)}, u32[]{:S(2)}) async-start(bf16[32,4,2048]{2,1,0:T(4,128)(2,1)} %get-tuple-element.23), calls=%async_computation.2 | async-start | bytes 1048576 | tf_op jit(solution)/shard_map/all_to_all | solution.py:496
Sparse Core Ops, SparseCore 0:
  9.3 79.8 all-gather.2

commit v7 on v6

--- a/solution.py
+++ b/solution.py
@@ -63,7 +63,7 @@
         ),
         in_specs=[smem] + [vmem] * (2 + members),
         out_specs=(vmem, vmem),
-        compiler_params=pltpu.CompilerParams(vmem_limit_bytes=50 * 2**20),
+        compiler_params=pltpu.CompilerParams(vmem_limit_bytes=24 * 2**20),
         name="query",
     )(
         lax.axis_index("far").astype(jnp.int32).reshape(1),
@@ -220,7 +220,6 @@
         pl.ds(0, heads * width),
         jnp.dot(chosen, full, preferred_element_type=jnp.float32).astype(out_ref.dtype),
     )
-    put_rows(out_ref, pl.ds(heads * width, chosen.shape[1]), chosen)
 
 
 def attention(
@@ -228,7 +227,7 @@
 ):
     count, ctx_len, kv_count, width = cache_keys.shape
     heads = lambdas.shape[0]
-    slots, lanes = dispatch.shape
+    slots = dispatch.shape[0]
     shard = heads * width // experts
     vmem = pl.BlockSpec(memory_space=pltpu.VMEM)
     smem = pl.BlockSpec(memory_space=pltpu.SMEM)
@@ -239,7 +238,7 @@
         functools.partial(attention_kernel, together, 128, shard),
         out_shape=(
             jax.ShapeDtypeStruct((count, heads * width), jnp.bfloat16),
-            jax.ShapeDtypeStruct((experts, slots // experts, heads * width + lanes), jnp.bfloat16),
+            jax.ShapeDtypeStruct((experts, slots // experts, heads * width), jnp.bfloat16),
         ),
         in_specs=[smem, smem, smem, vmem, vmem, vmem, vmem, vmem, hbm, hbm],
         out_specs=(vmem, vmem),
@@ -268,36 +267,24 @@
 
 
 def expert_kernel(
-    core_ref, h_ref, own_ref, tok_ref, gain_ref, near_hbm, other_hbm, gate_hbm, up_hbm, down_hbm,
-    o_ref, res_ref, wo_buf, x_buf, gate_buf, up_buf, down_buf, wo_sem, x_sem, gate_sem, up_sem, down_sem,
+    core_ref, h_ref, rows_ref, own_ref, tok_ref, gain_ref, near_hbm, other_hbm, gate_hbm, up_hbm, down_hbm,
+    o_ref, res_ref, wo_buf, gate_buf, up_buf, down_buf, wo_sem, gate_sem, up_sem, down_sem,
 ):
     core = core_ref[0]
     cols = wo_buf.shape[1] // 2
     depth = wo_buf.shape[2]
-    count = own_ref.shape[0]
     slots = h_ref.shape[0] * h_ref.shape[1]
-    members = x_buf.shape[1] * 2
-    halves = x_buf.shape[0]
     pieces = down_sem.shape[0]
     width = o_ref.shape[2]
     step = width // pieces
 
     wo_copies = []
-    x_copies = []
     for i, source in enumerate((near_hbm, other_hbm)):
         side = core if i == 0 else 1 - core
         at = pl.ds(pl.multiple_of(side * cols, cols), cols)
         wo_copies.append(
             pltpu.make_async_copy(source.at[:, pl.ds(0, cols)], wo_buf.at[:, at], wo_sem.at[i])
         )
-        at = pl.ds(pl.multiple_of(side * count, count), count)
-        for half in range(halves):
-            rows = pl.ds(cols + half * count, count)
-            x_copies.append(
-                pltpu.make_async_copy(
-                    source.at[:, rows], x_buf.at[half, :, at], x_sem.at[i * halves + half]
-                )
-            )
     gate_copy = pltpu.make_async_copy(gate_hbm.at[0], gate_buf, gate_sem)
     up_copy = pltpu.make_async_copy(up_hbm.at[0], up_buf, up_sem)
     down_copies = [
@@ -306,22 +293,10 @@
         )
         for i in range(pieces)
     ]
-    for copy in (*wo_copies, *x_copies, gate_copy, up_copy, *down_copies):
+    for copy in (*wo_copies, gate_copy, up_copy, *down_copies):
         copy.start()
 
-    arrived = rows_of(h_ref)
-    heads = jnp.concatenate([arrived[:, :depth], own_ref[...]], axis=0)
-    chosen = arrived[:, depth:]
-    lanes = chosen.shape[1]
-    per = slots // members
-    token = lax.broadcasted_iota(jnp.int32, (lanes, members * count), 0)
-    column = lax.broadcasted_iota(jnp.int32, (lanes, members * count), 1)
-    repeat = jnp.where(column % count == token, 1.0, 0.0).astype(jnp.bfloat16)
-    spread = jnp.dot(chosen, repeat, preferred_element_type=jnp.float32)
-    slot = lax.broadcasted_iota(jnp.int32, (slots, members * count), 0)
-    column = lax.broadcasted_iota(jnp.int32, (slots, members * count), 1)
-    select = jnp.where(slot // per == column // count, spread, 0.0).astype(jnp.bfloat16)
-
+    heads = jnp.concatenate([rows_of(h_ref), own_ref[...]], axis=0)
     for copy in wo_copies:
         copy.wait()
     attn = lax.dot_general(
@@ -333,20 +308,9 @@
     res_ref[...] = (
         tok_ref[...].astype(jnp.float32) + attn[slots:].astype(jnp.float32)
     ).astype(res_ref.dtype)
-    for copy in x_copies:
-        copy.wait()
-    rows = jnp.concatenate(
-        [
-            jnp.dot(
-                select,
-                x_buf[half].reshape(members * count, depth),
-                preferred_element_type=jnp.float32,
-            )
-            for half in range(halves)
-        ],
-        axis=1,
-    )
-    residual = (rows + attn[:slots].astype(jnp.float32)).astype(jnp.bfloat16)
+    residual = (
+        rows_ref[...].astype(jnp.float32) + attn[:slots].astype(jnp.float32)
+    ).astype(jnp.bfloat16)
     inputs = rms_scaled(residual, gain_ref[...]).astype(jnp.bfloat16)
     gate_copy.wait()
     gate = jnp.dot(inputs, gate_buf[...], preferred_element_type=jnp.float32)
@@ -366,12 +330,10 @@
         )
 
 
-def expert(core, received, head_out, tokens, moe_gain, near, other, gate_w, up_w, down_w):
+def expert(core, received, rows, head_out, tokens, moe_gain, near, other, cols, gate_w, up_w, down_w):
     members, per, _ = received.shape
     count, width = tokens.shape
-    chips, packed, depth = near.shape
-    halves = width // depth
-    cols = packed - halves * count
+    chips, _, depth = near.shape
     hidden = gate_w.shape[2]
     pieces = 4
     vmem = pl.BlockSpec(memory_space=pltpu.VMEM)
@@ -384,23 +346,107 @@
             jax.ShapeDtypeStruct((members, per, width), bf16),
             jax.ShapeDtypeStruct((count, width), bf16),
         ),
-        in_specs=[smem, vmem, vmem, vmem, vmem, hbm, hbm, hbm, hbm, hbm],
+        in_specs=[smem, vmem, vmem, vmem, vmem, vmem, hbm, hbm, hbm, hbm, hbm],
         out_specs=(vmem, vmem),
         scratch_shapes=[
             pltpu.VMEM((chips, 2 * cols, depth), bf16),
-            pltpu.VMEM((halves, chips, 2 * count, depth), bf16),
             pltpu.VMEM((width, hidden), bf16),
             pltpu.VMEM((width, hidden), bf16),
             pltpu.VMEM((hidden, width), bf16),
             pltpu.SemaphoreType.DMA((2,)),
-            pltpu.SemaphoreType.DMA((2 * halves,)),
             pltpu.SemaphoreType.DMA,
             pltpu.SemaphoreType.DMA,
             pltpu.SemaphoreType.DMA((pieces,)),
         ],
         compiler_params=pltpu.CompilerParams(vmem_limit_bytes=50 * 2**20),
         name="expert",
-    )(core, received, head_out, tokens, moe_gain.reshape(1, width), near, other, gate_w, up_w, down_w)
+    )(core, received, rows, head_out, tokens, moe_gain.reshape(1, width), near, other, gate_w, up_w, down_w)
+
+
+def pick_kernel(cols, count, where_ref, near_hbm, other_hbm, o_ref, x_buf, name_buf, x_sem, name_sem):
+    core = where_ref[0]
+    expert = where_ref[1].astype(jnp.float32)
+    halves, chips, _, depth = x_buf.shape
+    names = name_buf.shape[1] // 2
+    lanes = name_buf.shape[2]
+    members = 2 * chips
+    slots = o_ref.shape[0]
+    per = slots // members
+    copies = []
+    for i, source in enumerate((near_hbm, other_hbm)):
+        side = core if i == 0 else 1 - core
+        at = pl.ds(pl.multiple_of(side * names, names), names)
+        first = cols + halves * count
+        copies.append(
+            pltpu.make_async_copy(
+                source.at[:, pl.ds(first, names), pl.ds(0, lanes)], name_buf.at[:, at], name_sem.at[i]
+            )
+        )
+    for i, source in enumerate((near_hbm, other_hbm)):
+        side = core if i == 0 else 1 - core
+        at = pl.ds(pl.multiple_of(side * count, count), count)
+        for half in range(halves):
+            rows = pl.ds(cols + half * count, count)
+            copies.append(
+                pltpu.make_async_copy(
+                    source.at[:, rows], x_buf.at[half, :, at], x_sem.at[i * halves + half]
+                )
+            )
+    for copy in copies:
+        copy.start()
+
+    def table(shape, rule):
+        rows = lax.broadcasted_iota(jnp.int32, shape, 0)
+        columns = lax.broadcasted_iota(jnp.int32, shape, 1)
+        return jnp.where(rule(rows, columns), 1.0, 0.0).astype(jnp.bfloat16)
+
+    def product(a, b):
+        return jnp.dot(a, b, preferred_element_type=jnp.float32)
+
+    for copy in copies[:2]:
+        copy.wait()
+    named = name_buf[...].reshape(members * names, lanes).astype(jnp.float32)
+    found = jnp.where(named == expert, 1.0, 0.0).astype(jnp.bfloat16)
+    found = product(table((members, members * names), lambda r, c: c // names == r), found)
+    found = found.astype(jnp.bfloat16)
+    earlier = product(found, table((lanes, lanes), lambda r, c: r < c)).astype(jnp.bfloat16)
+    repeat = table((slots, members), lambda r, c: r // per == c)
+    rank = lax.broadcasted_iota(jnp.int32, (slots, lanes), 0) % per
+    chosen = jnp.where(
+        product(repeat, earlier) == rank.astype(jnp.float32), product(repeat, found), 0.0
+    ).astype(jnp.bfloat16)
+    spread = product(chosen, table((lanes, members * count), lambda r, c: c % count == r))
+    slot = lax.broadcasted_iota(jnp.int32, (slots, members * count), 0)
+    column = lax.broadcasted_iota(jnp.int32, (slots, members * count), 1)
+    select = jnp.where(slot // per == column // count, spread, 0.0).astype(jnp.bfloat16)
+    for copy in copies[2:]:
+        copy.wait()
+    for half in range(halves):
+        o_ref[:, pl.ds(half * depth, depth)] = product(
+            select, x_buf[half].reshape(members * count, depth)
+        ).astype(o_ref.dtype)
+
+
+def pick(where, near, other, cols, slots, tokens):
+    count, width = tokens.shape
+    chips, packed, depth = near.shape
+    halves = width // depth
+    names = packed - cols - halves * count
+    hbm = pl.BlockSpec(memory_space=pltpu.HBM)
+    return pl.pallas_call(
+        functools.partial(pick_kernel, cols, count),
+        out_shape=jax.ShapeDtypeStruct((slots, width), jnp.bfloat16),
+        in_specs=[pl.BlockSpec(memory_space=pltpu.SMEM), hbm, hbm],
+        out_specs=pl.BlockSpec(memory_space=pltpu.VMEM),
+        scratch_shapes=[
+            pltpu.VMEM((halves, chips, 2 * count, depth), jnp.bfloat16),
+            pltpu.VMEM((chips, 2 * names, 128), jnp.bfloat16),
+            pltpu.SemaphoreType.DMA((2 * halves,)),
+            pltpu.SemaphoreType.DMA((2,)),
+        ],
+        compiler_params=pltpu.CompilerParams(vmem_limit_bytes=50 * 2**20),
+        name="pick",
+    )(where, near, other)
 
 
 def combine_kernel(share_ref, rows_ref, res_ref, o_ref):
@@ -448,7 +494,10 @@
     count = tokens.shape[0]
     topk = routes.shape[1]
     depth = out_weight.shape[0]
-    packed = jnp.concatenate([out_weight.T, tokens[:, :depth], tokens[:, depth:]], axis=0)
+    named = jnp.pad(
+        routes.T.astype(jnp.bfloat16), ((0, 8 - topk), (0, depth - count)), constant_values=-1
+    )
+    packed = jnp.concatenate([out_weight.T, tokens[:, :depth], tokens[:, depth:], named], axis=0)
     near_packed = lax.all_gather(packed, CHIPS, axis=0)
     part, normed = query_product(tokens, norm_gain, query_weight)
     queries = lax.all_to_all(part, "far", 0, 0, tiled=True)
@@ -480,15 +529,20 @@
     received = lax.all_to_all(outgoing, EP, split_axis=0, concat_axis=0, tiled=True)
     near_packed, head_out = lax.optimization_barrier((near_packed, head_out))
     other_packed = lax.ppermute(near_packed, "core", [(0, 1), (1, 0)])
-    core = lax.axis_index("core").astype(jnp.int32).reshape(1)
+    core = lax.axis_index("core").astype(jnp.int32)
+    where = jnp.stack([core, lax.axis_index(EP).astype(jnp.int32)])
+    cols = out_weight.shape[1]
+    rows = pick(where, near_packed, other_packed, cols, experts * capacity, tokens)
     results, residual = expert(
-        core,
+        where,
         received,
+        rows,
         head_out,
         tokens,
         moe_gain,
         near_packed,
         other_packed,
+        cols,
         gate_weight,
         up_weight,
         down_weight,

time: 181 us -> 179 us (0.989)
  waiting for transfers between devices: 68.9 us -> 63.2 us
  local copies, waits for them, and re-layouts: 3.64 us -> 5.61 us
    all_to_all x1, waiting for transfers between devices: 22.2 us -> 16.4 us  [local(): lax.all_to_all(outgoing, EP, split_axis=0, concat_axis=0, tiled=True)]
    pallas_call x1, Pallas kernels: 11.9 us -> 9.14 us  [expert(): pl.pallas_call(expert_kernel, out_shape=(jax.ShapeDtypeStruct((members, p...]
    pallas_call x0 -> x1, Pallas kernels: none -> 2.35 us  [pick(): pl.pallas_call(functools.partial(pick_kernel, cols, count), out_shape=jax...]
    unnamed x16 -> x18, local copies, waits for them, and re-layouts: 0.93 us -> 2.9 us
  transfers between devices with their start and end apart: 8 -> 8, of which waited for: 4 -> 4; matrix products, arithmetic and copies ran while one was open for 3% -> 3% of each run, Pallas kernels for 5% -> 7%
where the time goes in v7:
time: 179 us; the launch traced here: 175 us
  waiting for transfers between devices  63.2 us (35%)
  blocking collectives  34.4 us (19%)
  starting transfers between devices  31.2 us (17%)
  Pallas kernels  21.8 us (12%)
  between operations  13.6 us (8%)
  local copies, waits for them, and re-layouts  5.61 us (3%)
  other arithmetic  3.59 us (2%)
    all_gather x1, blocking collectives, query_product(): rows = lax.all_gather(tokens, 'far', axis=0, tiled=True)  34.4 us
    all_to_all x1, waiting for transfers between devices, local(): lax.all_to_all(results, EP, split_axis=0, concat_axis=0, tiled=True)  32 us
    all_to_all x1, waiting for transfers between devices, local(): lax.all_to_all(outgoing, EP, split_axis=0, concat_axis=0, tiled=True)  16.4 us
    all_to_all x1, waiting for transfers between devices, local(): queries = lax.all_to_all(part, 'far', 0, 0, tiled=True)  10.8 us
    pallas_call x1, Pallas kernels, expert(): pl.pallas_call(expert_kernel, out_shape=(jax.ShapeDtypeStruct((members, p...  9.14 us
    all_to_all x1, starting transfers between devices, local(): lax.all_to_all(outgoing, EP, split_axis=0, concat_axis=0, tiled=True)  8.68 us
    ppermute x3, starting transfers between devices, query_product(): lax.ppermute(shard, NEAR, [(i, i ^ d) for i in range(members)])  8.64 us
    pallas_call x1, Pallas kernels, attention(): pl.pallas_call(functools.partial(attention_kernel, together, 128, shard),...  8.3 us
  transfers between devices with their start and end apart: 8, of which 4 were waited for; matrix products, arithmetic and copies ran while one was open for 3% of the time, Pallas kernels for 7%

profile of v7, /device:TPU:196, one launch (start us, length us, event | category | flops | bytes accessed | tf_op | source)
XLA Modules:
  0.0 175.2 jit_solution(1685240687355370787)
XLA Ops:
  6.6 0.1 all-gather.3.cloned.1.call-start
  6.6 0.9 fusion.4
  7.5 0.7 convert_bitcast_fusion
  8.2 1.6 fusion.1
  9.8 0.1 all-gather.3.cloned.1.call-update
  9.8 0.1 collective-permute-start
  10.0 8.5 %collective-permute-start.1 = (bf16[32,2048]{1,0:T(8,128)(2,1)}, bf16[32,2048]{1,0:T(8,128)(2,1)S(1)}, u32[]{:S(2)}, u32[]{:S(2)}) collective-permute-start(bf16[32,2048]{1,0:T(8,128)(2,1)} %bitcast.20), channel_id=1, source_target_pairs={{0,2},{1,3},{2,0},{3,1},{4,6},{5,7},{6,4},{7,5},{8,10},{9,11},{10,... | collective-permute-start | bytes 393224 | tf_op jit(solution)/shard_map/ppermute | solution.py:53
  18.5 0.0 collective-permute-start.2
  18.5 0.7 reshape.29.gain_ref
  19.2 34.4 %all_gather.9.rows_ref = bf16[128,2048]{1,0:T(8,128)(2,1)S(1)} all-gather(bf16[16,2048]{1,0:T(8,128)(2,1)} %tok_ref.1), channel_id=1, replica_groups=mesh['grp'=4,'far'=8,'near'=2,'core'=2] {'far'}, dimensions={0}, use_global_device_ids=true | all-gather | bytes 589824 | tf_op jit(solution)/shard_map/all_gather | solution.py:54
  53.6 0.0 collective-permute-done.refs_1_
  53.6 0.0 collective-permute-done.1.refs_2_
  53.6 0.0 collective-permute-done.2.refs_3_
  53.6 0.0 copy-start.3
  53.6 0.9 copy-done.3
  54.5 1.1 query.1
  55.6 0.2 convolution_convert_fusion.1.nk_ref
  55.8 0.8 copy.29
  56.6 0.1 eq.20
  56.7 0.1 fusion.2
  56.8 0.1 reduce_window_sum.11
  56.9 0.2 select_reduce_fusion.1
  57.1 0.1 reshape.30
  57.1 0.1 copy.30
  57.2 8.2 %all-to-all-start = ((bf16[8,16,128]{2,1,0:T(8,128)(2,1)}), bf16[8,16,128]{2,1,0:T(8,128)(2,1)S(1)}, u32[]{:S(2)}, u32[]{:S(2)}) async-start(bf16[8,16,128]{2,1,0:T(8,128)(2,1)} %get-tuple-element.17), calls=%async_computation | async-start | bytes 65536 | tf_op jit(solution)/shard_map/all_to_all | solution.py:503
  65.4 0.7 multiply_add_fusion
  66.1 1.5 convolution_convert_fusion.nv_ref
  67.6 0.1 fusion.3
  67.7 0.1 copy.31
  67.8 10.8 %all-to-all-done.r_ref = bf16[8,16,128]{2,1,0:T(8,128)(2,1)S(1)} async-done(((bf16[8,16,128]{2,1,0:T(8,128)(2,1)}), bf16[8,16,128]{2,1,0:T(8,128)(2,1)S(1)}, u32[]{:S(2)}, u32[]{:S(2)}) %all-to-all-start) | async-done | bytes 32800 | tf_op jit(solution)/shard_map/all_to_all | solution.py:503
  78.7 0.0 copy-start.7
  78.7 8.3 %attention.1 = (bf16[16,1024]{1,0:T(8,128)(2,1)S(1)}, bf16[32,4,1024]{2,1,0:T(4,128)(2,1)}) custom-call(s32[1]{0:T(128)} %bitcast.4.member_ref, s32[16]{0:T(128)S(1)} %copy-done.4, f32[8]{0:T(128)S(1)} %copy-done.5, bf16[8,16,128]{2,1,0:T(8,128)(2,1)S(1)} %all-to-all-done.r_ref, bf16[16,256]{1,0:T(8,128)(2,1)S(1)} %convolution_convert_fusion.1.nk_ref, ...), custom_call_target="tpu_custom_call" | custom-call | tf_op jit(solution)/shard_map/attention/pallas_call | solution.py:237
  87.0 0.0 copy-start.2
  87.0 3.9 %all-gather.3.cloned.1.call-done = bf16[1664,1024]{1,0:T(8,128)(2,1)} async-done(((bf16[104,1024]{1,0:T(8,128)(2,1)}), bf16[1664,1024]{1,0:T(8,128)(2,1)}) %all-gather.3.cloned.1.call-update) | async-done | bytes 3407888 | tf_op jit(solution)/shard_map/all_gather | solution.py:501
  90.9 0.0 collective-permute-start.3
  90.9 8.7 %all-to-all-start.1 = ((bf16[32,4,1024]{2,1,0:T(4,128)(2,1)}), bf16[32,4,1024]{2,1,0:T(4,128)(2,1)S(1)}, u32[]{:S(2)}, u32[]{:S(2)}) async-start(bf16[32,4,1024]{2,1,0:T(4,128)(2,1)} %get-tuple-element.19), calls=%async_computation.1 | async-start | bytes 524288 | tf_op jit(solution)/shard_map/all_to_all | solution.py:529
  99.6 0.0 copy-done.7
  99.6 0.1 pad_add_fusion.where_ref.core_ref
  99.7 0.0 collective-permute-done.3.other_hbm
  99.7 2.0 %copy-done.1 = bf16[1664,1024]{1,0:T(8,128)(2,1)S(1)} copy-done((bf16[1664,1024]{1,0:T(8,128)(2,1)S(1)}, bf16[1664,1024]{1,0:T(8,128)(2,1)}, u32[]{:S(2)}) %copy-start.1) | copy-done | bytes 3407896
  101.7 2.3 %pick.1.rows_ref = bf16[128,2048]{1,0:T(8,128)(2,1)S(1)} custom-call(s32[2]{0:T(128)S(1)} %pad_add_fusion.where_ref.core_ref, bf16[16,104,1024]{2,1,0:T(8,128)(2,1)S(1)} %bitcast.18, bf16[16,104,1024]{2,1,0:T(8,128)(2,1)} %collective-permute-done.3.other_hbm), custom_call_target="tpu_custom_call" | custom-call | tf_op jit(solution)/shard_map/pick/pallas_call | solution.py:436
  104.1 0.0 copy-start.8
  104.1 16.4 %all-to-all-done.1.h_ref = bf16[32,4,1024]{2,1,0:T(4,128)(2,1)S(1)} async-done(((bf16[32,4,1024]{2,1,0:T(4,128)(2,1)}), bf16[32,4,1024]{2,1,0:T(4,128)(2,1)S(1)}, u32[]{:S(2)}, u32[]{:S(2)}) %all-to-all-start.1) | async-done | bytes 262176 | tf_op jit(solution)/shard_map/all_to_all | solution.py:529
  120.5 9.1 %expert.1 = (bf16[32,4,2048]{2,1,0:T(4,128)(2,1)}, bf16[16,2048]{1,0:T(8,128)(2,1)S(1)}) custom-call(s32[2]{0:T(128)S(1)} %pad_add_fusion.where_ref.core_ref, bf16[32,4,1024]{2,1,0:T(4,128)(2,1)S(1)} %all-to-all-done.1.h_ref, bf16[128,2048]{1,0:T(8,128)(2,1)S(1)} %pick.1.rows_ref, bf16[16,1024]{1,0:T(8,128)(2,1)S(1)} %get-tuple-element.22.own_ref, ...), custom_call_target="tpu_custom_call" | custom-call | tf_op jit(solution)/shard_map/expert/pallas_call | solution.py:343
  129.6 5.6 %all-to-all-start.2 = ((bf16[32,4,2048]{2,1,0:T(4,128)(2,1)}), bf16[32,4,2048]{2,1,0:T(4,128)(2,1)S(1)}, u32[]{:S(2)}, u32[]{:S(2)}) async-start(bf16[32,4,2048]{2,1,0:T(4,128)(2,1)} %get-tuple-element.23), calls=%async_computation.2 | async-start | bytes 1048576 | tf_op jit(solution)/shard_map/all_to_all | solution.py:550
  135.3 0.1 select_reduce_fusion.share_ref
  135.4 32.0 %all-to-all-done.2.rows_ref = bf16[32,4,2048]{2,1,0:T(4,128)(2,1)S(1)} async-done(((bf16[32,4,2048]{2,1,0:T(4,128)(2,1)}), bf16[32,4,2048]{2,1,0:T(4,128)(2,1)S(1)}, u32[]{:S(2)}, u32[]{:S(2)}) %all-to-all-start.2) | async-done | bytes 524320 | tf_op jit(solution)/shard_map/all_to_all | solution.py:550
  167.3 1.0 combine.1
  (13 shorter events, 0.0 us)
Async XLA Ops:
  6.5 49.1 %copy-start = (bf16[2048,256]{1,0:T(8,128)(2,1)S(1)}, bf16[2048,256]{1,0:T(8,128)(2,1)}, u32[]{:S(2)}) copy-start(bf16[2048,256]{1,0:T(8,128)(2,1)} %param.20) | copy-start | bytes 3145732
  6.6 72.1 %copy-start.6 = (bf16[128]{0:T(256)(128)(2,1)S(1)}, bf16[128]{0:T(256)(128)(2,1)}, u32[]{:S(2)}) copy-start(bf16[128]{0:T(256)(128)(2,1)} %param.23) | copy-start | bytes 772
  6.6 72.1 %copy-start.5 = (f32[8]{0:T(128)S(1)}, f32[8]{0:T(128)}, u32[]{:S(2)}) copy-start(f32[8]{0:T(128)} %lam_ref.1) | copy-start | bytes 100
  6.6 72.1 %copy-start.4 = (s32[16]{0:T(128)S(1)}, s32[16]{0:T(128)}, u32[]{:S(2)}) copy-start(s32[16]{0:T(128)} %lens_ref.1) | copy-start | bytes 196
  6.6 84.4 %all-gather.3.cloned.1.call-start = ((), (), s32[]{:S(2)}) async-start(), calls=%async_computation.3 | async-start | bytes 3620864 | tf_op jit(solution)/shard_map/all_gather | solution.py:501
  9.8 43.8 %collective-permute-start = (bf16[32,2048]{1,0:T(8,128)(2,1)}, bf16[32,2048]{1,0:T(8,128)(2,1)S(1)}, u32[]{:S(2)}, u32[]{:S(2)}) collective-permute-start(bf16[32,2048]{1,0:T(8,128)(2,1)} %bitcast.19), channel_id=1, source_target_pairs={{0,1},{1,0},{2,3},{3,2},{4,5},{5,4},{6,7},{7,6},{8,9},{9,8},{10,11... | collective-permute-start | bytes 393224 | tf_op jit(solution)/shard_map/ppermute | solution.py:53
  10.0 43.6 %collective-permute-start.1 = (bf16[32,2048]{1,0:T(8,128)(2,1)}, bf16[32,2048]{1,0:T(8,128)(2,1)S(1)}, u32[]{:S(2)}, u32[]{:S(2)}) collective-permute-start(bf16[32,2048]{1,0:T(8,128)(2,1)} %bitcast.20), channel_id=1, source_target_pairs={{0,2},{1,3},{2,0},{3,1},{4,6},{5,7},{6,4},{7,5},{8,10},{9,11},{10,... | collective-permute-start | bytes 393224 | tf_op jit(solution)/shard_map/ppermute | solution.py:53
  18.5 35.1 %collective-permute-start.2 = (bf16[32,2048]{1,0:T(8,128)(2,1)}, bf16[32,2048]{1,0:T(8,128)(2,1)S(1)}, u32[]{:S(2)}, u32[]{:S(2)}) collective-permute-start(bf16[32,2048]{1,0:T(8,128)(2,1)} %bitcast.21), channel_id=1, source_target_pairs={{0,3},{1,2},{2,1},{3,0},{4,7},{5,6},{6,5},{7,4},{8,11},{9,10},{10,... | collective-permute-start | bytes 393224 | tf_op jit(solution)/shard_map/ppermute | solution.py:53
  53.6 0.9 copy-start.3
  57.2 21.4 %all-to-all-start = ((bf16[8,16,128]{2,1,0:T(8,128)(2,1)}), bf16[8,16,128]{2,1,0:T(8,128)(2,1)S(1)}, u32[]{:S(2)}, u32[]{:S(2)}) async-start(bf16[8,16,128]{2,1,0:T(8,128)(2,1)} %get-tuple-element.17), calls=%async_computation | async-start | bytes 65536 | tf_op jit(solution)/shard_map/all_to_all | solution.py:503
  78.7 21.0 %copy-start.7 = (bf16[2048]{0:T(1024)(128)(2,1)S(1)}, bf16[2048]{0:T(1024)(128)(2,1)}, u32[]{:S(2)}) copy-start(bf16[2048]{0:T(1024)(128)(2,1)} %param.28) | copy-start | bytes 12292
  87.0 33.5 %copy-start.2 = (bf16[16,2048]{1,0:T(8,128)(2,1)S(1)}, bf16[16,2048]{1,0:T(8,128)(2,1)}, u32[]{:S(2)}) copy-start(bf16[16,2048]{1,0:T(8,128)(2,1)} %tok_ref.1) | copy-start | bytes 196612
  90.9 8.8 %collective-permute-start.3 = (bf16[16,104,1024]{2,1,0:T(8,128)(2,1)}, bf16[16,104,1024]{2,1,0:T(8,128)(2,1)}, u32[]{:S(2)}, u32[]{:S(2)}) collective-permute-start(bf16[16,104,1024]{2,1,0:T(8,128)(2,1)} %bitcast.16), channel_id=1, source_target_pairs={{0,1},{1,0},{2,3},{3,2},{4,5},{5,4},{6,7},{7,6},{8,9},{9,8},{10,11... | collective-permute-start | bytes 10223624 | tf_op jit(solution)/shard_map/ppermute | solution.py:531
  90.9 29.5 %all-to-all-start.1 = ((bf16[32,4,1024]{2,1,0:T(4,128)(2,1)}), bf16[32,4,1024]{2,1,0:T(4,128)(2,1)S(1)}, u32[]{:S(2)}, u32[]{:S(2)}) async-start(bf16[32,4,1024]{2,1,0:T(4,128)(2,1)} %get-tuple-element.19), calls=%async_computation.1 | async-start | bytes 524288 | tf_op jit(solution)/shard_map/all_to_all | solution.py:529
  99.7 2.0 %copy-start.1 = (bf16[1664,1024]{1,0:T(8,128)(2,1)S(1)}, bf16[1664,1024]{1,0:T(8,128)(2,1)}, u32[]{:S(2)}) copy-start(bf16[1664,1024]{1,0:T(8,128)(2,1)} %all-gather.3.cloned.1.call-done) | copy-start | bytes 10223620
  104.1 31.2 %copy-start.8 = (f32[16,4]{0,1:T(4,128)S(1)}, f32[16,4]{0,1:T(4,128)}, u32[]{:S(2)}) copy-start(f32[16,4]{0,1:T(4,128)} %param.33) | copy-start | bytes 772
  129.6 37.7 %all-to-all-start.2 = ((bf16[32,4,2048]{2,1,0:T(4,128)(2,1)}), bf16[32,4,2048]{2,1,0:T(4,128)(2,1)S(1)}, u32[]{:S(2)}, u32[]{:S(2)}) async-start(bf16[32,4,2048]{2,1,0:T(4,128)(2,1)} %get-tuple-element.23), calls=%async_computation.2 | async-start | bytes 1048576 | tf_op jit(solution)/shard_map/all_to_all | solution.py:550
Sparse Core Ops, SparseCore 0:
  10.0 80.9 all-gather.2

commit v8 on v7

--- a/solution.py
+++ b/solution.py
@@ -28,6 +28,48 @@
         * lax.rsqrt(jnp.mean(floats * floats, axis=-1, keepdims=True) + epsilon)
         * gain.astype(jnp.float32)
     )
+
+
+def pack_kernel(weight_hbm, tokens_hbm, routes_ref, o_hbm, name_buf, sem):
+    cols, depth = weight_hbm.shape
+    count, width = tokens_hbm.shape
+    copies = [pltpu.make_async_copy(weight_hbm, o_hbm.at[pl.ds(0, cols)], sem.at[0])]
+    for half in range(width // depth):
+        copies.append(
+            pltpu.make_async_copy(
+                tokens_hbm.at[:, pl.ds(half * depth, depth)],
+                o_hbm.at[pl.ds(cols + half * count, count)],
+                sem.at[1 + half],
+            )
+        )
+    for copy in copies:
+        copy.start()
+    named = routes_ref[...].astype(jnp.float32)
+    named = jnp.concatenate([named, jnp.full((name_buf.shape[0] - named.shape[0], count), -1.0)], axis=0)
+    rest = jnp.full((name_buf.shape[0], depth - count), -1.0, jnp.float32)
+    name_buf[...] = jnp.concatenate([named, rest], axis=1).astype(name_buf.dtype)
+    first = o_hbm.shape[0] - name_buf.shape[0]
+    copies.append(
+        pltpu.make_async_copy(name_buf, o_hbm.at[pl.ds(first, name_buf.shape[0])], sem.at[len(copies)])
+    )
+    copies[-1].start()
+    for copy in copies:
+        copy.wait()
+
+
+def pack(out_weight, tokens, routes):
+    depth, cols = out_weight.shape
+    count, width = tokens.shape
+    halves = width // depth
+    hbm = pl.BlockSpec(memory_space=pltpu.HBM)
+    return pl.pallas_call(
+        pack_kernel,
+        out_shape=jax.ShapeDtypeStruct((cols + halves * count + 8, depth), jnp.bfloat16),
+        in_specs=[hbm, hbm, pl.BlockSpec(memory_space=pltpu.VMEM)],
+        out_specs=hbm,
+        scratch_shapes=[pltpu.VMEM((8, depth), jnp.bfloat16), pltpu.SemaphoreType.DMA((2 + halves,))],
+        name="pack",
+    )(out_weight.T, tokens, routes.T)
 
 
 def query_kernel(place_ref, rows_ref, gain_ref, *refs):
@@ -493,15 +535,13 @@
 ):
     count = tokens.shape[0]
     topk = routes.shape[1]
-    depth = out_weight.shape[0]
-    named = jnp.pad(
-        routes.T.astype(jnp.bfloat16), ((0, 8 - topk), (0, depth - count)), constant_values=-1
-    )
-    packed = jnp.concatenate([out_weight.T, tokens[:, :depth], tokens[:, depth:], named], axis=0)
+    packed = pack(out_weight, tokens, routes)
     near_packed = lax.all_gather(packed, CHIPS, axis=0)
     part, normed = query_product(tokens, norm_gain, query_weight)
     queries = lax.all_to_all(part, "far", 0, 0, tiled=True)
-    new_keys = jnp.dot(normed, key_weight, preferred_element_type=jnp.float32).astype(jnp.bfloat16)
+    new_keys = jnp.dot(normed, key_weight, preferred_element_type=jnp.float32).astype(
+        jnp.bfloat16
+    )
     new_values = jnp.dot(normed, value_weight, preferred_element_type=jnp.float32).astype(
         jnp.bfloat16
     )

time: 179 us -> 183 us (1.022)
  Pallas kernels: 21.8 us -> 29.6 us
  other arithmetic: 3.59 us -> 1.29 us
    pallas_call x0 -> x1, Pallas kernels: none -> 7.85 us  [pack(): pl.pallas_call(pack_kernel, out_shape=jax.ShapeDtypeStruct((cols + halves...]
where the time goes in v8:
time: 183 us; the launch traced here: 180 us
  waiting for transfers between devices  63.2 us (35%)
  blocking collectives  34.4 us (19%)
  starting transfers between devices  31.2 us (17%)
  Pallas kernels  29.6 us (16%)
  between operations  13.6 us (7%)
  local copies, waits for them, and re-layouts  4.75 us (3%)
    all_gather x1, blocking collectives, query_product(): rows = lax.all_gather(tokens, 'far', axis=0, tiled=True)  34.4 us
    all_to_all x1, waiting for transfers between devices, local(): lax.all_to_all(results, EP, split_axis=0, concat_axis=0, tiled=True)  32 us
    all_to_all x1, waiting for transfers between devices, local(): lax.all_to_all(outgoing, EP, split_axis=0, concat_axis=0, tiled=True)  16.4 us
    all_to_all x1, waiting for transfers between devices, local(): queries = lax.all_to_all(part, 'far', 0, 0, tiled=True)  10.8 us
    pallas_call x1, Pallas kernels, expert(): pl.pallas_call(expert_kernel, out_shape=(jax.ShapeDtypeStruct((members, p...  9.13 us
    all_to_all x1, starting transfers between devices, local(): lax.all_to_all(outgoing, EP, split_axis=0, concat_axis=0, tiled=True)  8.68 us
    ppermute x3, starting transfers between devices, query_product(): lax.ppermute(shard, NEAR, [(i, i ^ d) for i in range(members)])  8.64 us
    pallas_call x1, Pallas kernels, attention(): pl.pallas_call(functools.partial(attention_kernel, together, 128, shard),...  8.28 us
  transfers between devices with their start and end apart: 8, of which 4 were waited for; matrix products, arithmetic and copies ran while one was open for 3% of the time, Pallas kernels for 7%

profile of v8, /device:TPU:196, one launch (start us, length us, event | category | flops | bytes accessed | tf_op | source)
XLA Modules:
  0.0 179.9 jit_solution(10518080021152314836)
XLA Ops:
  6.5 0.0 copy-start
  6.6 0.1 all-gather.3.cloned.1.call-start
  6.6 7.9 %pack.1 = bf16[104,1024]{1,0:T(8,128)(2,1)} custom-call(bf16[64,1024]{1,0:T(8,128)(2,1)} %bitcast.25, bf16[16,2048]{1,0:T(8,128)(2,1)} %tok_ref.1, s32[4,16]{1,0:T(4,128)} %bitcast.26), custom_call_target="tpu_custom_call" | custom-call | tf_op jit(solution)/shard_map/pack/pallas_call | solution.py:65
  14.5 0.1 all-gather.3.cloned.1.call-update
  14.5 0.1 collective-permute-start
  14.7 8.5 %collective-permute-start.1 = (bf16[32,2048]{1,0:T(8,128)(2,1)}, bf16[32,2048]{1,0:T(8,128)(2,1)S(1)}, u32[]{:S(2)}, u32[]{:S(2)}) collective-permute-start(bf16[32,2048]{1,0:T(8,128)(2,1)} %bitcast.19), channel_id=1, source_target_pairs={{0,2},{1,3},{2,0},{3,1},{4,6},{5,7},{6,4},{7,5},{8,10},{9,11},{10,... | collective-permute-start | bytes 393224 | tf_op jit(solution)/shard_map/ppermute | solution.py:95
  23.2 0.0 collective-permute-start.2
  23.2 0.7 reshape.29.gain_ref
  23.9 34.4 %all_gather.9.rows_ref = bf16[128,2048]{1,0:T(8,128)(2,1)S(1)} all-gather(bf16[16,2048]{1,0:T(8,128)(2,1)} %tok_ref.1), channel_id=1, replica_groups=mesh['grp'=4,'far'=8,'near'=2,'core'=2] {'far'}, dimensions={0}, use_global_device_ids=true | all-gather | bytes 589824 | tf_op jit(solution)/shard_map/all_gather | solution.py:96
  58.3 0.0 collective-permute-done.refs_1_
  58.3 0.0 collective-permute-done.1.refs_2_
  58.3 0.0 collective-permute-done.2.refs_3_
  58.3 0.0 copy-start.3
  58.3 0.9 copy-done.3
  59.2 1.1 query.1
  60.3 0.0 copy-done
  60.3 0.2 convolution_convert_fusion.1.nk_ref
  60.5 0.8 copy.29
  61.3 0.1 eq.20
  61.4 0.1 fusion
  61.5 0.1 reduce_window_sum.11
  61.6 0.2 select_reduce_fusion.1
  61.8 0.1 reshape.30
  61.8 0.1 copy.30
  61.9 8.2 %all-to-all-start = ((bf16[8,16,128]{2,1,0:T(8,128)(2,1)}), bf16[8,16,128]{2,1,0:T(8,128)(2,1)S(1)}, u32[]{:S(2)}, u32[]{:S(2)}) async-start(bf16[8,16,128]{2,1,0:T(8,128)(2,1)} %get-tuple-element.17), calls=%async_computation | async-start | bytes 65536 | tf_op jit(solution)/shard_map/all_to_all | solution.py:541
  70.1 0.7 multiply_add_fusion
  70.8 1.5 convolution_convert_fusion.nv_ref
  72.3 0.1 fusion.1
  72.4 0.1 copy.31
  72.5 10.8 %all-to-all-done.r_ref = bf16[8,16,128]{2,1,0:T(8,128)(2,1)S(1)} async-done(((bf16[8,16,128]{2,1,0:T(8,128)(2,1)}), bf16[8,16,128]{2,1,0:T(8,128)(2,1)S(1)}, u32[]{:S(2)}, u32[]{:S(2)}) %all-to-all-start) | async-done | bytes 32800 | tf_op jit(solution)/shard_map/all_to_all | solution.py:541
  83.3 0.0 copy-done.6
  83.4 0.0 copy-start.7
  83.4 8.3 %attention.1 = (bf16[16,1024]{1,0:T(8,128)(2,1)S(1)}, bf16[32,4,1024]{2,1,0:T(4,128)(2,1)}) custom-call(s32[1]{0:T(128)} %bitcast.4.member_ref, s32[16]{0:T(128)S(1)} %copy-done.4, f32[8]{0:T(128)S(1)} %copy-done.5, bf16[8,16,128]{2,1,0:T(8,128)(2,1)S(1)} %all-to-all-done.r_ref, bf16[16,256]{1,0:T(8,128)(2,1)S(1)} %convolution_convert_fusion.1.nk_ref, ...), custom_call_target="tpu_custom_call" | custom-call | tf_op jit(solution)/shard_map/attention/pallas_call | solution.py:279
  91.7 0.0 copy-start.2
  91.7 4.0 %all-gather.3.cloned.1.call-done = bf16[1664,1024]{1,0:T(8,128)(2,1)} async-done(((bf16[104,1024]{1,0:T(8,128)(2,1)}), bf16[1664,1024]{1,0:T(8,128)(2,1)}) %all-gather.3.cloned.1.call-update) | async-done | bytes 3407888 | tf_op jit(solution)/shard_map/all_gather | solution.py:539
  95.6 0.0 collective-permute-start.3
  95.6 8.7 %all-to-all-start.1 = ((bf16[32,4,1024]{2,1,0:T(4,128)(2,1)}), bf16[32,4,1024]{2,1,0:T(4,128)(2,1)S(1)}, u32[]{:S(2)}, u32[]{:S(2)}) async-start(bf16[32,4,1024]{2,1,0:T(4,128)(2,1)} %get-tuple-element.19), calls=%async_computation.1 | async-start | bytes 524288 | tf_op jit(solution)/shard_map/all_to_all | solution.py:569
  104.3 0.1 pad_add_fusion.where_ref.core_ref
  104.4 0.0 collective-permute-done.3.other_hbm
  104.4 2.0 %copy-done.1 = bf16[1664,1024]{1,0:T(8,128)(2,1)S(1)} copy-done((bf16[1664,1024]{1,0:T(8,128)(2,1)S(1)}, bf16[1664,1024]{1,0:T(8,128)(2,1)}, u32[]{:S(2)}) %copy-start.1) | copy-done | bytes 3407896
  106.4 2.4 %pick.1.rows_ref = bf16[128,2048]{1,0:T(8,128)(2,1)S(1)} custom-call(s32[2]{0:T(128)S(1)} %pad_add_fusion.where_ref.core_ref, bf16[16,104,1024]{2,1,0:T(8,128)(2,1)S(1)} %bitcast.17, bf16[16,104,1024]{2,1,0:T(8,128)(2,1)} %collective-permute-done.3.other_hbm), custom_call_target="tpu_custom_call" | custom-call | tf_op jit(solution)/shard_map/pick/pallas_call | solution.py:478
  108.8 0.0 copy-start.8
  108.8 16.4 %all-to-all-done.1.h_ref = bf16[32,4,1024]{2,1,0:T(4,128)(2,1)S(1)} async-done(((bf16[32,4,1024]{2,1,0:T(4,128)(2,1)}), bf16[32,4,1024]{2,1,0:T(4,128)(2,1)S(1)}, u32[]{:S(2)}, u32[]{:S(2)}) %all-to-all-start.1) | async-done | bytes 262176 | tf_op jit(solution)/shard_map/all_to_all | solution.py:569
  125.2 9.1 %expert.1 = (bf16[32,4,2048]{2,1,0:T(4,128)(2,1)}, bf16[16,2048]{1,0:T(8,128)(2,1)S(1)}) custom-call(s32[2]{0:T(128)S(1)} %pad_add_fusion.where_ref.core_ref, bf16[32,4,1024]{2,1,0:T(4,128)(2,1)S(1)} %all-to-all-done.1.h_ref, bf16[128,2048]{1,0:T(8,128)(2,1)S(1)} %pick.1.rows_ref, bf16[16,1024]{1,0:T(8,128)(2,1)S(1)} %get-tuple-element.22.own_ref, ...), custom_call_target="tpu_custom_call" | custom-call | tf_op jit(solution)/shard_map/expert/pallas_call | solution.py:385
  134.3 5.7 %all-to-all-start.2 = ((bf16[32,4,2048]{2,1,0:T(4,128)(2,1)}), bf16[32,4,2048]{2,1,0:T(4,128)(2,1)S(1)}, u32[]{:S(2)}, u32[]{:S(2)}) async-start(bf16[32,4,2048]{2,1,0:T(4,128)(2,1)} %get-tuple-element.23), calls=%async_computation.2 | async-start | bytes 1048576 | tf_op jit(solution)/shard_map/all_to_all | solution.py:590
  140.0 0.1 select_reduce_fusion.share_ref
  140.1 32.0 %all-to-all-done.2.rows_ref = bf16[32,4,2048]{2,1,0:T(4,128)(2,1)S(1)} async-done(((bf16[32,4,2048]{2,1,0:T(4,128)(2,1)}), bf16[32,4,2048]{2,1,0:T(4,128)(2,1)S(1)}, u32[]{:S(2)}, u32[]{:S(2)}) %all-to-all-start.2) | async-done | bytes 524320 | tf_op jit(solution)/shard_map/all_to_all | solution.py:590
  172.0 1.0 combine.1
  (11 shorter events, 0.0 us)
Async XLA Ops:
  6.5 53.7 %copy-start = (bf16[2048,256]{1,0:T(8,128)(2,1)S(1)}, bf16[2048,256]{1,0:T(8,128)(2,1)}, u32[]{:S(2)}) copy-start(bf16[2048,256]{1,0:T(8,128)(2,1)} %param.20) | copy-start | bytes 3145732
  6.6 76.8 %copy-start.6 = (bf16[128]{0:T(256)(128)(2,1)S(1)}, bf16[128]{0:T(256)(128)(2,1)}, u32[]{:S(2)}) copy-start(bf16[128]{0:T(256)(128)(2,1)} %param.23) | copy-start | bytes 772
  6.6 76.8 %copy-start.5 = (f32[8]{0:T(128)S(1)}, f32[8]{0:T(128)}, u32[]{:S(2)}) copy-start(f32[8]{0:T(128)} %lam_ref.1) | copy-start | bytes 100
  6.6 76.8 %copy-start.4 = (s32[16]{0:T(128)S(1)}, s32[16]{0:T(128)}, u32[]{:S(2)}) copy-start(s32[16]{0:T(128)} %lens_ref.1) | copy-start | bytes 196
  6.6 89.1 %all-gather.3.cloned.1.call-start = ((), (), s32[]{:S(2)}) async-start(), calls=%async_computation.3 | async-start | bytes 3620864 | tf_op jit(solution)/shard_map/all_gather | solution.py:539
  14.5 43.8 %collective-permute-start = (bf16[32,2048]{1,0:T(8,128)(2,1)}, bf16[32,2048]{1,0:T(8,128)(2,1)S(1)}, u32[]{:S(2)}, u32[]{:S(2)}) collective-permute-start(bf16[32,2048]{1,0:T(8,128)(2,1)} %bitcast.18), channel_id=1, source_target_pairs={{0,1},{1,0},{2,3},{3,2},{4,5},{5,4},{6,7},{7,6},{8,9},{9,8},{10,11... | collective-permute-start | bytes 393224 | tf_op jit(solution)/shard_map/ppermute | solution.py:95
  14.7 43.6 %collective-permute-start.1 = (bf16[32,2048]{1,0:T(8,128)(2,1)}, bf16[32,2048]{1,0:T(8,128)(2,1)S(1)}, u32[]{:S(2)}, u32[]{:S(2)}) collective-permute-start(bf16[32,2048]{1,0:T(8,128)(2,1)} %bitcast.19), channel_id=1, source_target_pairs={{0,2},{1,3},{2,0},{3,1},{4,6},{5,7},{6,4},{7,5},{8,10},{9,11},{10,... | collective-permute-start | bytes 393224 | tf_op jit(solution)/shard_map/ppermute | solution.py:95
  23.2 35.1 %collective-permute-start.2 = (bf16[32,2048]{1,0:T(8,128)(2,1)}, bf16[32,2048]{1,0:T(8,128)(2,1)S(1)}, u32[]{:S(2)}, u32[]{:S(2)}) collective-permute-start(bf16[32,2048]{1,0:T(8,128)(2,1)} %bitcast.20), channel_id=1, source_target_pairs={{0,3},{1,2},{2,1},{3,0},{4,7},{5,6},{6,5},{7,4},{8,11},{9,10},{10,... | collective-permute-start | bytes 393224 | tf_op jit(solution)/shard_map/ppermute | solution.py:95
  58.3 0.9 copy-start.3
  61.9 21.4 %all-to-all-start = ((bf16[8,16,128]{2,1,0:T(8,128)(2,1)}), bf16[8,16,128]{2,1,0:T(8,128)(2,1)S(1)}, u32[]{:S(2)}, u32[]{:S(2)}) async-start(bf16[8,16,128]{2,1,0:T(8,128)(2,1)} %get-tuple-element.17), calls=%async_computation | async-start | bytes 65536 | tf_op jit(solution)/shard_map/all_to_all | solution.py:541
  83.4 21.0 %copy-start.7 = (bf16[2048]{0:T(1024)(128)(2,1)S(1)}, bf16[2048]{0:T(1024)(128)(2,1)}, u32[]{:S(2)}) copy-start(bf16[2048]{0:T(1024)(128)(2,1)} %param.28) | copy-start | bytes 12292
  91.7 33.5 %copy-start.2 = (bf16[16,2048]{1,0:T(8,128)(2,1)S(1)}, bf16[16,2048]{1,0:T(8,128)(2,1)}, u32[]{:S(2)}) copy-start(bf16[16,2048]{1,0:T(8,128)(2,1)} %tok_ref.1) | copy-start | bytes 196612
  95.6 8.8 %collective-permute-start.3 = (bf16[16,104,1024]{2,1,0:T(8,128)(2,1)}, bf16[16,104,1024]{2,1,0:T(8,128)(2,1)}, u32[]{:S(2)}, u32[]{:S(2)}) collective-permute-start(bf16[16,104,1024]{2,1,0:T(8,128)(2,1)} %bitcast.15), channel_id=1, source_target_pairs={{0,1},{1,0},{2,3},{3,2},{4,5},{5,4},{6,7},{7,6},{8,9},{9,8},{10,11... | collective-permute-start | bytes 10223624 | tf_op jit(solution)/shard_map/ppermute | solution.py:571
  95.6 29.5 %all-to-all-start.1 = ((bf16[32,4,1024]{2,1,0:T(4,128)(2,1)}), bf16[32,4,1024]{2,1,0:T(4,128)(2,1)S(1)}, u32[]{:S(2)}, u32[]{:S(2)}) async-start(bf16[32,4,1024]{2,1,0:T(4,128)(2,1)} %get-tuple-element.19), calls=%async_computation.1 | async-start | bytes 524288 | tf_op jit(solution)/shard_map/all_to_all | solution.py:569
  104.4 2.0 %copy-start.1 = (bf16[1664,1024]{1,0:T(8,128)(2,1)S(1)}, bf16[1664,1024]{1,0:T(8,128)(2,1)}, u32[]{:S(2)}) copy-start(bf16[1664,1024]{1,0:T(8,128)(2,1)} %all-gather.3.cloned.1.call-done) | copy-start | bytes 10223620
  108.8 31.2 %copy-start.8 = (f32[16,4]{0,1:T(4,128)S(1)}, f32[16,4]{0,1:T(4,128)}, u32[]{:S(2)}) copy-start(f32[16,4]{0,1:T(4,128)} %param.33) | copy-start | bytes 772
  134.3 37.7 %all-to-all-start.2 = ((bf16[32,4,2048]{2,1,0:T(4,128)(2,1)}), bf16[32,4,2048]{2,1,0:T(4,128)(2,1)S(1)}, u32[]{:S(2)}, u32[]{:S(2)}) async-start(bf16[32,4,2048]{2,1,0:T(4,128)(2,1)} %get-tuple-element.23), calls=%async_computation.2 | async-start | bytes 1048576 | tf_op jit(solution)/shard_map/all_to_all | solution.py:590
Sparse Core Ops, SparseCore 0:
  14.7 80.9 all-gather.2

commit v9 on v7

--- a/solution.py
+++ b/solution.py
@@ -28,6 +28,34 @@
         * lax.rsqrt(jnp.mean(floats * floats, axis=-1, keepdims=True) + epsilon)
         * gain.astype(jnp.float32)
     )
+
+
+def pack_kernel(weight_ref, tokens_ref, routes_ref, o_ref):
+    cols, depth = weight_ref.shape
+    count, width = tokens_ref.shape
+    halves = width // depth
+    o_ref[pl.ds(0, cols)] = weight_ref[...]
+    for half in range(halves):
+        o_ref[pl.ds(cols + half * count, count)] = tokens_ref[:, pl.ds(half * depth, depth)]
+    first = cols + halves * count
+    named = routes_ref[...].astype(jnp.float32)
+    rows = o_ref.shape[0] - first
+    named = jnp.concatenate([named, jnp.full((rows - named.shape[0], count), -1.0)], axis=0)
+    rest = jnp.full((rows, depth - count), -1.0, jnp.float32)
+    o_ref[pl.ds(first, rows)] = jnp.concatenate([named, rest], axis=1).astype(o_ref.dtype)
+
+
+def pack(out_weight, tokens, routes):
+    depth, cols = out_weight.shape
+    count, width = tokens.shape
+    vmem = pl.BlockSpec(memory_space=pltpu.VMEM)
+    return pl.pallas_call(
+        pack_kernel,
+        out_shape=jax.ShapeDtypeStruct((cols + width // depth * count + 8, depth), jnp.bfloat16),
+        in_specs=[vmem] * 3,
+        out_specs=vmem,
+        name="pack",
+    )(out_weight.T, tokens, routes.T)
 
 
 def query_kernel(place_ref, rows_ref, gain_ref, *refs):
@@ -493,11 +521,7 @@
 ):
     count = tokens.shape[0]
     topk = routes.shape[1]
-    depth = out_weight.shape[0]
-    named = jnp.pad(
-        routes.T.astype(jnp.bfloat16), ((0, 8 - topk), (0, depth - count)), constant_values=-1
-    )
-    packed = jnp.concatenate([out_weight.T, tokens[:, :depth], tokens[:, depth:], named], axis=0)
+    packed = pack(out_weight, tokens, routes)
     near_packed = lax.all_gather(packed, CHIPS, axis=0)
     part, normed = query_product(tokens, norm_gain, query_weight)
     queries = lax.all_to_all(part, "far", 0, 0, tiled=True)

time: 179 us -> 177 us (0.989)
  other arithmetic: 3.59 us -> 1.29 us
where the time goes in v9:
time: 177 us; the launch traced here: 174 us
  waiting for transfers between devices  64.6 us (36%)
  blocking collectives  34.6 us (20%)
  starting transfers between devices  29.9 us (17%)
  Pallas kernels  23.5 us (13%)
  between operations  13.6 us (8%)
  local copies, waits for them, and re-layouts  4.75 us (3%)
    all_gather x1, blocking collectives, query_product(): rows = lax.all_gather(tokens, 'far', axis=0, tiled=True)  34.6 us
    all_to_all x1, waiting for transfers between devices, local(): lax.all_to_all(results, EP, split_axis=0, concat_axis=0, tiled=True)  32 us
    all_to_all x1, waiting for transfers between devices, local(): lax.all_to_all(outgoing, EP, split_axis=0, concat_axis=0, tiled=True)  16.4 us
    all_to_all x1, waiting for transfers between devices, local(): queries = lax.all_to_all(part, 'far', 0, 0, tiled=True)  10.8 us
    pallas_call x1, Pallas kernels, expert(): pl.pallas_call(expert_kernel, out_shape=(jax.ShapeDtypeStruct((members, p...  9.12 us
    ppermute x3, starting transfers between devices, query_product(): lax.ppermute(shard, NEAR, [(i, i ^ d) for i in range(members)])  8.64 us
    pallas_call x1, Pallas kernels, attention(): pl.pallas_call(functools.partial(attention_kernel, together, 128, shard),...  8.28 us
    all_to_all x1, starting transfers between devices, local(): lax.all_to_all(outgoing, EP, split_axis=0, concat_axis=0, tiled=True)  8.19 us
  transfers between devices with their start and end apart: 8, of which 4 were waited for; matrix products, arithmetic and copies ran while one was open for 3% of the time, Pallas kernels for 7%

profile of v9, /device:TPU:196, one launch (start us, length us, event | category | flops | bytes accessed | tf_op | source)
XLA Modules:
  0.0 173.9 jit_solution(1436203115203230671)
XLA Ops:
  6.5 0.0 copy-start
  6.6 0.1 all-gather.3.cloned.1.call-start
  6.6 1.7 pack.1
  8.3 0.1 all-gather.3.cloned.1.call-update
  8.4 0.1 collective-permute-start
  8.5 8.5 %collective-permute-start.1 = (bf16[32,2048]{1,0:T(8,128)(2,1)}, bf16[32,2048]{1,0:T(8,128)(2,1)S(1)}, u32[]{:S(2)}, u32[]{:S(2)}) collective-permute-start(bf16[32,2048]{1,0:T(8,128)(2,1)} %bitcast.19), channel_id=1, source_target_pairs={{0,2},{1,3},{2,0},{3,1},{4,6},{5,7},{6,4},{7,5},{8,10},{9,11},{10,... | collective-permute-start | bytes 393224 | tf_op jit(solution)/shard_map/ppermute | solution.py:81
  17.0 0.0 collective-permute-start.2
  17.0 0.7 reshape.29.gain_ref
  17.7 34.6 %all_gather.9.rows_ref = bf16[128,2048]{1,0:T(8,128)(2,1)S(1)} all-gather(bf16[16,2048]{1,0:T(8,128)(2,1)} %tok_ref.1), channel_id=1, replica_groups=mesh['grp'=4,'far'=8,'near'=2,'core'=2] {'far'}, dimensions={0}, use_global_device_ids=true | all-gather | bytes 589824 | tf_op jit(solution)/shard_map/all_gather | solution.py:82
  52.3 0.0 collective-permute-done.refs_1_
  52.3 0.0 collective-permute-done.1.refs_2_
  52.3 0.0 collective-permute-done.2.refs_3_
  52.3 0.0 copy-start.3
  52.3 0.9 copy-done.3
  53.2 1.1 query.1
  54.3 0.2 convolution_convert_fusion.1.nk_ref
  54.5 0.8 copy.29
  55.3 0.1 eq.20
  55.4 0.1 fusion
  55.5 0.1 reduce_window_sum.11
  55.6 0.2 select_reduce_fusion.1
  55.8 0.1 reshape.30
  55.8 0.1 copy.30
  55.9 7.4 %all-to-all-start = ((bf16[8,16,128]{2,1,0:T(8,128)(2,1)}), bf16[8,16,128]{2,1,0:T(8,128)(2,1)S(1)}, u32[]{:S(2)}, u32[]{:S(2)}) async-start(bf16[8,16,128]{2,1,0:T(8,128)(2,1)} %get-tuple-element.17), calls=%async_computation | async-start | bytes 65536 | tf_op jit(solution)/shard_map/all_to_all | solution.py:527
  63.3 0.7 multiply_add_fusion
  64.0 1.5 convolution_convert_fusion.nv_ref
  65.5 0.1 fusion.1
  65.6 0.1 copy.31
  65.7 10.8 %all-to-all-done.r_ref = bf16[8,16,128]{2,1,0:T(8,128)(2,1)S(1)} async-done(((bf16[8,16,128]{2,1,0:T(8,128)(2,1)}), bf16[8,16,128]{2,1,0:T(8,128)(2,1)S(1)}, u32[]{:S(2)}, u32[]{:S(2)}) %all-to-all-start) | async-done | bytes 32800 | tf_op jit(solution)/shard_map/all_to_all | solution.py:527
  76.5 0.0 copy-start.7
  76.6 8.3 %attention.1 = (bf16[16,1024]{1,0:T(8,128)(2,1)S(1)}, bf16[32,4,1024]{2,1,0:T(4,128)(2,1)}) custom-call(s32[1]{0:T(128)} %bitcast.4.member_ref, s32[16]{0:T(128)S(1)} %copy-done.4, f32[8]{0:T(128)S(1)} %copy-done.5, bf16[8,16,128]{2,1,0:T(8,128)(2,1)S(1)} %all-to-all-done.r_ref, bf16[16,256]{1,0:T(8,128)(2,1)S(1)} %convolution_convert_fusion.1.nk_ref, ...), custom_call_target="tpu_custom_call" | custom-call | tf_op jit(solution)/shard_map/attention/pallas_call | solution.py:265
  84.8 0.0 copy-start.2
  84.9 5.3 %all-gather.3.cloned.1.call-done = bf16[1664,1024]{1,0:T(8,128)(2,1)} async-done(((bf16[104,1024]{1,0:T(8,128)(2,1)}), bf16[1664,1024]{1,0:T(8,128)(2,1)}) %all-gather.3.cloned.1.call-update) | async-done | bytes 3407888 | tf_op jit(solution)/shard_map/all_gather | solution.py:525
  90.2 0.0 collective-permute-start.3
  90.2 8.2 %all-to-all-start.1 = ((bf16[32,4,1024]{2,1,0:T(4,128)(2,1)}), bf16[32,4,1024]{2,1,0:T(4,128)(2,1)S(1)}, u32[]{:S(2)}, u32[]{:S(2)}) async-start(bf16[32,4,1024]{2,1,0:T(4,128)(2,1)} %get-tuple-element.19), calls=%async_computation.1 | async-start | bytes 524288 | tf_op jit(solution)/shard_map/all_to_all | solution.py:553
  98.4 0.1 pad_add_fusion.where_ref.core_ref
  98.5 0.0 collective-permute-done.3.other_hbm
  98.5 2.0 %copy-done.1 = bf16[1664,1024]{1,0:T(8,128)(2,1)S(1)} copy-done((bf16[1664,1024]{1,0:T(8,128)(2,1)S(1)}, bf16[1664,1024]{1,0:T(8,128)(2,1)}, u32[]{:S(2)}) %copy-start.1) | copy-done | bytes 3407896
  100.4 2.3 %pick.1.rows_ref = bf16[128,2048]{1,0:T(8,128)(2,1)S(1)} custom-call(s32[2]{0:T(128)S(1)} %pad_add_fusion.where_ref.core_ref, bf16[16,104,1024]{2,1,0:T(8,128)(2,1)S(1)} %bitcast.17, bf16[16,104,1024]{2,1,0:T(8,128)(2,1)} %collective-permute-done.3.other_hbm), custom_call_target="tpu_custom_call" | custom-call | tf_op jit(solution)/shard_map/pick/pallas_call | solution.py:464
  102.8 0.0 copy-start.8
  102.8 16.4 %all-to-all-done.1.h_ref = bf16[32,4,1024]{2,1,0:T(4,128)(2,1)S(1)} async-done(((bf16[32,4,1024]{2,1,0:T(4,128)(2,1)}), bf16[32,4,1024]{2,1,0:T(4,128)(2,1)S(1)}, u32[]{:S(2)}, u32[]{:S(2)}) %all-to-all-start.1) | async-done | bytes 262176 | tf_op jit(solution)/shard_map/all_to_all | solution.py:553
  119.2 0.0 copy-done.2
  119.2 9.1 %expert.1 = (bf16[32,4,2048]{2,1,0:T(4,128)(2,1)}, bf16[16,2048]{1,0:T(8,128)(2,1)S(1)}) custom-call(s32[2]{0:T(128)S(1)} %pad_add_fusion.where_ref.core_ref, bf16[32,4,1024]{2,1,0:T(4,128)(2,1)S(1)} %all-to-all-done.1.h_ref, bf16[128,2048]{1,0:T(8,128)(2,1)S(1)} %pick.1.rows_ref, bf16[16,1024]{1,0:T(8,128)(2,1)S(1)} %get-tuple-element.22.own_ref, ...), custom_call_target="tpu_custom_call" | custom-call | tf_op jit(solution)/shard_map/expert/pallas_call | solution.py:371
  128.3 5.7 %all-to-all-start.2 = ((bf16[32,4,2048]{2,1,0:T(4,128)(2,1)}), bf16[32,4,2048]{2,1,0:T(4,128)(2,1)S(1)}, u32[]{:S(2)}, u32[]{:S(2)}) async-start(bf16[32,4,2048]{2,1,0:T(4,128)(2,1)} %get-tuple-element.23), calls=%async_computation.2 | async-start | bytes 1048576 | tf_op jit(solution)/shard_map/all_to_all | solution.py:574
  134.0 0.0 copy-done.8
  134.0 0.1 select_reduce_fusion.share_ref
  134.1 32.0 %all-to-all-done.2.rows_ref = bf16[32,4,2048]{2,1,0:T(4,128)(2,1)S(1)} async-done(((bf16[32,4,2048]{2,1,0:T(4,128)(2,1)}), bf16[32,4,2048]{2,1,0:T(4,128)(2,1)S(1)}, u32[]{:S(2)}, u32[]{:S(2)}) %all-to-all-start.2) | async-done | bytes 524320 | tf_op jit(solution)/shard_map/all_to_all | solution.py:574
  166.1 1.0 combine.1
  (11 shorter events, 0.0 us)
Async XLA Ops:
  6.5 47.7 %copy-start = (bf16[2048,256]{1,0:T(8,128)(2,1)S(1)}, bf16[2048,256]{1,0:T(8,128)(2,1)}, u32[]{:S(2)}) copy-start(bf16[2048,256]{1,0:T(8,128)(2,1)} %param.20) | copy-start | bytes 3145732
  6.6 70.0 %copy-start.6 = (bf16[128]{0:T(256)(128)(2,1)S(1)}, bf16[128]{0:T(256)(128)(2,1)}, u32[]{:S(2)}) copy-start(bf16[128]{0:T(256)(128)(2,1)} %param.23) | copy-start | bytes 772
  6.6 70.0 %copy-start.5 = (f32[8]{0:T(128)S(1)}, f32[8]{0:T(128)}, u32[]{:S(2)}) copy-start(f32[8]{0:T(128)} %lam_ref.1) | copy-start | bytes 100
  6.6 70.0 %copy-start.4 = (s32[16]{0:T(128)S(1)}, s32[16]{0:T(128)}, u32[]{:S(2)}) copy-start(s32[16]{0:T(128)} %lens_ref.1) | copy-start | bytes 196
  6.6 83.6 %all-gather.3.cloned.1.call-start = ((), (), s32[]{:S(2)}) async-start(), calls=%async_computation.3 | async-start | bytes 3620864 | tf_op jit(solution)/shard_map/all_gather | solution.py:525
  8.4 43.9 %collective-permute-start = (bf16[32,2048]{1,0:T(8,128)(2,1)}, bf16[32,2048]{1,0:T(8,128)(2,1)S(1)}, u32[]{:S(2)}, u32[]{:S(2)}) collective-permute-start(bf16[32,2048]{1,0:T(8,128)(2,1)} %bitcast.18), channel_id=1, source_target_pairs={{0,1},{1,0},{2,3},{3,2},{4,5},{5,4},{6,7},{7,6},{8,9},{9,8},{10,11... | collective-permute-start | bytes 393224 | tf_op jit(solution)/shard_map/ppermute | solution.py:81
  8.5 43.8 %collective-permute-start.1 = (bf16[32,2048]{1,0:T(8,128)(2,1)}, bf16[32,2048]{1,0:T(8,128)(2,1)S(1)}, u32[]{:S(2)}, u32[]{:S(2)}) collective-permute-start(bf16[32,2048]{1,0:T(8,128)(2,1)} %bitcast.19), channel_id=1, source_target_pairs={{0,2},{1,3},{2,0},{3,1},{4,6},{5,7},{6,4},{7,5},{8,10},{9,11},{10,... | collective-permute-start | bytes 393224 | tf_op jit(solution)/shard_map/ppermute | solution.py:81
  17.0 35.3 %collective-permute-start.2 = (bf16[32,2048]{1,0:T(8,128)(2,1)}, bf16[32,2048]{1,0:T(8,128)(2,1)S(1)}, u32[]{:S(2)}, u32[]{:S(2)}) collective-permute-start(bf16[32,2048]{1,0:T(8,128)(2,1)} %bitcast.20), channel_id=1, source_target_pairs={{0,3},{1,2},{2,1},{3,0},{4,7},{5,6},{6,5},{7,4},{8,11},{9,10},{10,... | collective-permute-start | bytes 393224 | tf_op jit(solution)/shard_map/ppermute | solution.py:81
  52.3 0.9 copy-start.3
  55.9 20.6 %all-to-all-start = ((bf16[8,16,128]{2,1,0:T(8,128)(2,1)}), bf16[8,16,128]{2,1,0:T(8,128)(2,1)S(1)}, u32[]{:S(2)}, u32[]{:S(2)}) async-start(bf16[8,16,128]{2,1,0:T(8,128)(2,1)} %get-tuple-element.17), calls=%async_computation | async-start | bytes 65536 | tf_op jit(solution)/shard_map/all_to_all | solution.py:527
  76.5 21.8 %copy-start.7 = (bf16[2048]{0:T(1024)(128)(2,1)S(1)}, bf16[2048]{0:T(1024)(128)(2,1)}, u32[]{:S(2)}) copy-start(bf16[2048]{0:T(1024)(128)(2,1)} %param.28) | copy-start | bytes 12292
  84.8 34.4 %copy-start.2 = (bf16[16,2048]{1,0:T(8,128)(2,1)S(1)}, bf16[16,2048]{1,0:T(8,128)(2,1)}, u32[]{:S(2)}) copy-start(bf16[16,2048]{1,0:T(8,128)(2,1)} %tok_ref.1) | copy-start | bytes 196612
  90.2 8.3 %collective-permute-start.3 = (bf16[16,104,1024]{2,1,0:T(8,128)(2,1)}, bf16[16,104,1024]{2,1,0:T(8,128)(2,1)}, u32[]{:S(2)}, u32[]{:S(2)}) collective-permute-start(bf16[16,104,1024]{2,1,0:T(8,128)(2,1)} %bitcast.15), channel_id=1, source_target_pairs={{0,1},{1,0},{2,3},{3,2},{4,5},{5,4},{6,7},{7,6},{8,9},{9,8},{10,11... | collective-permute-start | bytes 10223624 | tf_op jit(solution)/shard_map/ppermute | solution.py:555
  90.2 29.0 %all-to-all-start.1 = ((bf16[32,4,1024]{2,1,0:T(4,128)(2,1)}), bf16[32,4,1024]{2,1,0:T(4,128)(2,1)S(1)}, u32[]{:S(2)}, u32[]{:S(2)}) async-start(bf16[32,4,1024]{2,1,0:T(4,128)(2,1)} %get-tuple-element.19), calls=%async_computation.1 | async-start | bytes 524288 | tf_op jit(solution)/shard_map/all_to_all | solution.py:553
  98.5 2.0 %copy-start.1 = (bf16[1664,1024]{1,0:T(8,128)(2,1)S(1)}, bf16[1664,1024]{1,0:T(8,128)(2,1)}, u32[]{:S(2)}) copy-start(bf16[1664,1024]{1,0:T(8,128)(2,1)} %all-gather.3.cloned.1.call-done) | copy-start | bytes 10223620
  102.8 31.2 %copy-start.8 = (f32[16,4]{0,1:T(4,128)S(1)}, f32[16,4]{0,1:T(4,128)}, u32[]{:S(2)}) copy-start(f32[16,4]{0,1:T(4,128)} %param.33) | copy-start | bytes 772
  128.3 37.7 %all-to-all-start.2 = ((bf16[32,4,2048]{2,1,0:T(4,128)(2,1)}), bf16[32,4,2048]{2,1,0:T(4,128)(2,1)S(1)}, u32[]{:S(2)}, u32[]{:S(2)}) async-start(bf16[32,4,2048]{2,1,0:T(4,128)(2,1)} %get-tuple-element.23), calls=%async_computation.2 | async-start | bytes 1048576 | tf_op jit(solution)/shard_map/all_to_all | solution.py:574
Sparse Core Ops, SparseCore 0:
  9.0 81.0 all-gather.2
